TPU v7x, 512 devices: a whole 4x4x16 slice. The times are simulated.
512 devices in a mesh: sp: 64 (over z, y), tp: 8 (over x, core).
Axes of the slice: x: 4, y: 4, z: 16, core: 2. Of those that a mesh axis runs over, the one named last changes fastest.
Arguments:
- incoming_activity: bfloat16 [32768, 2048], P(('sp', 'tp')), may hold values from -6 to 6
- entry_standardize_factor: bfloat16 [2048], replicated, may hold values from 0.099609375 to 1.8984375
- recursive_entry_matrix: bfloat16 [2048, 2048], P(None, 'tp'), may hold values from -0.125 to 0.125
- final_switch_matrix: bfloat16 [2048, 2048], P(None, 'tp'), may hold values from -0.125 to 0.125
- averaging_entry_matrix: bfloat16 [2048, 1024], P(None, 'tp'), may hold values from -0.125 to 0.125
- percolumn_filter_coefficients: bfloat16 [4, 2048], P(None, 'tp'), may hold values from -3 to 3
- switch_tiled_matrices: bfloat16 [2, 2, 32, 64, 64], P(None, None, 'tp'), may hold values from -0.75 to 0.75
- prior_fading_odds: float32 [2, 2048], P(None, 'tp'), may hold values from 2.7 to 17
- speed_factors: float32 [2, 32768], P(None, 'sp'), may hold values from 0.4 to 2.5, as said below
- extra_fading_amounts: float32 [2, 32768], P(None, 'sp'), may hold values from -1.39 to 0, as said below
- averaging_cluster_matrices: bfloat16 [8, 128, 128], P('tp'), may hold values from -0.5 to 0.5
- averaging_feature_factor: bfloat16 [1024], P('tp'), may hold values from 0.099609375 to 1.8984375
- recursive_final_matrix: bfloat16 [2048, 2048], P('tp'), may hold values from -0.25 to 0.25
- averaging_final_matrix: bfloat16 [1024, 2048], P('tp'), may hold values from -0.1875 to 0.1875
Outputs:
- mixed: bfloat16 [32768, 2048], P(('sp', 'tp'))
Inputs may be any that keep to these rules, and one draw needn't show every extreme that they name: `speed_factors`: constant over each aligned block of 512 positions. `extra_fading_amounts`: each row has at most two nonzero entries.
All inputs are finite; a program needn't handle non-finite values.
Results may differ from a plain program's by a relative error of at most 0.017.
Values may be sent and summed in bfloat16 or wider, within the bound.
No kernel may reach another device: no remote copies, remote signals or barrier semaphores. Data moves between devices by JAX's collectives and lax.ppermute only.
A program may use at most 128 MiB of HBM per device.

v0:
```python
import jax
import jax.numpy as jnp
from jax import lax
from jax.sharding import PartitionSpec as P

FADING_FACTOR = 8.0
epsilon = 1e-06
span_rows = 16


def laid_out(tiles, dim):
    tiles = jnp.moveaxis(tiles, 0, dim)
    dims = tiles.shape
    return tiles.reshape(*dims[:dim], dims[dim] * dims[dim + 1], *dims[dim + 2 :])


def sent_to_all(value, axis):
    copies = jnp.broadcast_to(value, (lax.axis_size(axis), *value.shape))
    return lax.all_to_all(copies, axis, split_axis=0, concat_axis=0, tiled=True)


def gathered_copies(value, axis, dim):
    return laid_out(sent_to_all(value, axis), dim)


def padded(block, sides, width):
    for axis, dim in sides:
        count = lax.axis_size(axis)
        forward = [(i, i + 1) for i in range(count - 1)]
        backward = [(target, source) for source, target in forward]
        low = lax.ppermute(
            lax.slice_in_dim(block, block.shape[dim] - width, None, axis=dim), axis, forward
        )
        high = lax.ppermute(lax.slice_in_dim(block, 0, width, axis=dim), axis, backward)
        block = jnp.concatenate([low, block, high], axis=dim)
    return block


def gathered_once(value, axis):
    leaves = jax.tree.leaves(value)
    order = sorted(range(len(leaves)), key=lambda k: -leaves[k].size)
    width = (1, *leaves[order[0]].shape)[-1]
    lines = [
        jnp.pad(leaves[k].reshape(-1), (0, -leaves[k].size % width)).reshape(-1, width)
        for k in order
    ]
    both, at, found = (sent_to_all(jnp.concatenate(lines), axis), 0, {})
    for k, line in zip(order, lines):
        section = both[:, at : at + len(line)].reshape(len(both), -1)
        found[k] = section[:, : leaves[k].size].reshape(-1, *leaves[k].shape)
        at += len(line)
    numbers = iter(range(len(leaves)))
    return jax.tree.map(lambda _: found[next(numbers)], value)


def joined_by_halves(pieces, combine):
    while len(jax.tree.leaves(pieces)[0]) > 1:
        pieces = jax.vmap(combine)(
            *(jax.tree.map(lambda part: part[side::2], pieces) for side in (0, 1))
        )
    return jax.tree.map(lambda part: part[0], pieces)


def entering(value, axis, combine, identity, reverse):
    peers, position = (lax.axis_size(axis), lax.axis_index(axis))
    passed = jnp.arange(peers) > position if reverse else jnp.arange(peers) < position

    def kept(part, zero, own):
        part = jnp.where(
            passed.reshape(-1, *(1 for _ in own.shape)), part, jnp.asarray(zero, own.dtype)
        )
        return part[::-1] if reverse else part

    pieces = gathered_once(value, axis)
    return joined_by_halves(jax.tree.map(kept, pieces, identity, value), combine)


def combine(earlier, later):
    return (earlier[0] * later[0], later[0] * earlier[1] + later[1])


def product(left, right):
    return jnp.dot(left, right, preferred_element_type=jnp.float32)


def block_chain(log_keep, drive, backward):
    length, width = log_keep.shape
    count = length // span_rows
    logs = log_keep.reshape(count, span_rows, width)
    sources = drive.reshape(count, span_rows, width)
    running = jnp.cumsum(logs, axis=1)
    place = jnp.arange(span_rows, dtype=jnp.int32)
    if backward:
        running = running[:, -1:] - running + logs
        inside = place[None, :] >= place[:, None]
    else:
        inside = place[None, :] <= place[:, None]
    inside = inside[None, :, :, None]
    spread = running[:, :, None, :] - running[:, None, :, :]
    weights = jnp.where(inside, jnp.exp(jnp.where(inside, spread, 0.0)), 0.0)
    within = jnp.einsum("btsc,bsc->btc", weights, sources)
    decay = jnp.exp(running)
    ones = jnp.ones((1, width), jnp.float32)
    zeros = jnp.zeros((1, width), jnp.float32)
    if backward:
        ends = (decay[:, 0], within[:, 0])
        total_keep, total_state = lax.associative_scan(combine, ends, axis=0, reverse=True)
        prior_keep = jnp.concatenate([total_keep[1:], ones], axis=0)
        prior_state = jnp.concatenate([total_state[1:], zeros], axis=0)
    else:
        ends = (decay[:, -1], within[:, -1])
        total_keep, total_state = lax.associative_scan(combine, ends, axis=0)
        prior_keep = jnp.concatenate([ones, total_keep[:-1]], axis=0)
        prior_state = jnp.concatenate([zeros, total_state[:-1]], axis=0)
    keep_all = decay * prior_keep[:, None]
    local_all = within + decay * prior_state[:, None]
    return (keep_all.reshape(length, width), local_all.reshape(length, width))


def local(
    incoming_activity,
    entry_standardize_factor,
    recursive_entry_matrix,
    final_switch_matrix,
    averaging_entry_matrix,
    percolumn_filter_coefficients,
    switch_tiled_matrices,
    prior_fading_odds,
    speed_factors,
    extra_fading_amounts,
    averaging_cluster_matrices,
    averaging_feature_factor,
    recursive_final_matrix,
    averaging_final_matrix,
):
    state_width = recursive_entry_matrix.shape[1]
    pool_width = averaging_entry_matrix.shape[1]
    gain = entry_standardize_factor.astype(jnp.float32)
    values = gathered_copies(incoming_activity, "tp", 0).astype(jnp.float32)
    scaled = values * lax.rsqrt(jnp.mean(values * values, axis=1, keepdims=True) + epsilon)
    normed = (scaled * gain).astype(jnp.bfloat16)
    projected = jnp.concatenate(
        [
            product(normed, weight).astype(jnp.bfloat16)
            for weight in (recursive_entry_matrix, final_switch_matrix, averaging_entry_matrix)
        ],
        axis=1,
    )
    length = projected.shape[0]
    state_input = projected[:, :state_width]
    gate_input = projected[:, state_width : 2 * state_width]
    pool_input = projected[:, 2 * state_width :]
    conv_rows = padded(state_input, (("sp", 0),), 2).astype(jnp.float32)
    filtered = percolumn_filter_coefficients[0].astype(jnp.float32) * conv_rows[0:length]
    for shift in range(1, percolumn_filter_coefficients.shape[0]):
        filtered = (
            filtered
            + percolumn_filter_coefficients[shift].astype(jnp.float32)
            * conv_rows[shift : shift + length]
        )
    filtered = filtered.astype(jnp.bfloat16)
    filtered_wide = filtered.astype(jnp.float32)
    blocks_here = switch_tiled_matrices.shape[2]
    block_width = switch_tiled_matrices.shape[3]
    gate_sums = jnp.einsum(
        "tbi,dqbij->tdqbj",
        filtered.reshape(length, blocks_here, block_width),
        switch_tiled_matrices,
        preferred_element_type=jnp.float32,
    ).reshape(length, 2, 2, state_width)
    remember_switch = jax.nn.sigmoid(gate_sums[:, :, 0])
    inlet = jax.nn.sigmoid(gate_sums[:, :, 1])
    fading_speed = jax.nn.softplus(-prior_fading_odds)
    logarithmic_persistence = (
        -FADING_FACTOR
        * jnp.transpose(speed_factors)[:, :, None]
        * remember_switch
        * fading_speed[None]
        + jnp.transpose(extra_fading_amounts)[:, :, None]
    )
    drive = jnp.sqrt(-jnp.expm1(2.0 * logarithmic_persistence)) * inlet * filtered_wide[:, None, :]
    forward_keep, forward_local = block_chain(logarithmic_persistence[:, 0], drive[:, 0], False)
    backward_keep, backward_local = block_chain(logarithmic_persistence[:, 1], drive[:, 1], True)
    ones = jnp.ones((state_width,), jnp.float32)
    zeros = jnp.zeros((state_width,), jnp.float32)
    unused_front, forward_carry = entering(
        (forward_keep[-1], forward_local[-1]), "sp", combine, (ones, zeros), False
    )
    unused_back, backward_carry = entering(
        (backward_keep[0], backward_local[0]), "sp", combine, (ones, zeros), True
    )
    state_sum = (
        forward_local
        + forward_keep * forward_carry[None]
        + backward_local
        + backward_keep * backward_carry[None]
    )
    state_mix = (jax.nn.gelu(gate_input.astype(jnp.float32)) * state_sum).astype(jnp.bfloat16)
    pool_rows = padded(pool_input, (("sp", 0),), 8).astype(jnp.float32)
    spans = []
    level = pool_rows
    for step in range(4):
        shift = 1 << step
        level = level[:-shift] + level[shift:]
        spans.append(level)
    group_width = averaging_cluster_matrices.shape[1]
    local_groups = pool_width // group_width
    group_index = (
        lax.axis_index("tp") * local_groups + jnp.arange(pool_width, dtype=jnp.int32) // group_width
    )
    window_code = group_index % 4
    position = lax.axis_index("sp") * length + jnp.arange(length, dtype=jnp.int32)
    total_length = length * lax.axis_size("sp")
    window_sum = jnp.zeros((length, pool_width), jnp.float32)
    counted = jnp.ones((length, pool_width), jnp.float32)
    for code in range(4):
        half = 1 << code
        begin = 8 - half
        chosen = (window_code == code)[None, :]
        window_count = (
            jnp.minimum(position + half, total_length) - jnp.maximum(position - half, 0)
        ).astype(jnp.float32)[:, None]
        window_sum = jnp.where(chosen, spans[code][begin : begin + length], window_sum)
        counted = jnp.where(chosen, window_count, counted)
    pooled = (window_sum / counted - pool_rows[8 : 8 + length]).astype(jnp.bfloat16)
    grouped = jnp.einsum(
        "tgi,gij->tgj",
        pooled.reshape(length, local_groups, group_width),
        averaging_cluster_matrices,
        preferred_element_type=jnp.float32,
    ).reshape(length, pool_width)
    pool_mix = (grouped * averaging_feature_factor.astype(jnp.float32)).astype(jnp.bfloat16)
    joined = jnp.concatenate([state_mix, pool_mix], axis=1)
    moved = lax.all_to_all(joined, "tp", split_axis=0, concat_axis=1, tiled=True)
    stacked_weight = jnp.concatenate([recursive_final_matrix, averaging_final_matrix], axis=0)
    mixed = product(moved, lax.all_gather(stacked_weight, "tp", axis=0, tiled=True))
    return mixed.astype(jnp.bfloat16)


def solution(mesh):
    in_specs = (
        P(("sp", "tp"), None),
        P(),
        P(None, "tp"),
        P(None, "tp"),
        P(None, "tp"),
        P(None, "tp"),
        P(None, None, "tp", None, None),
        P(None, "tp"),
        P(None, "sp"),
        P(None, "sp"),
        P("tp", None, None),
        P("tp"),
        P("tp", None),
        P("tp", None),
    )
    out_specs = P(("sp", "tp"), None)
    return jax.shard_map(local, mesh=mesh, in_specs=in_specs, out_specs=out_specs, check_vma=False)
```

profile of v0, /device:TPU:1, one launch (start us, length us, event | category | flops | bytes accessed | tf_op | source)
XLA Modules:
  0.0 230.9 jit_solution(9454626966800306233)
XLA Ops:
  6.5 2.6 %broadcast_in_dim.169 = bf16[8,64,2048]{2,1,0:T(8,128)(2,1)} broadcast(bf16[64,2048]{1,0:T(8,128)(2,1)} %param.14), dimensions={1,2} | broadcast | bytes 2359296 | tf_op jit(solution)/shard_map/broadcast_in_dim | solution.py:18
  9.2 10.5 %all-to-all-start = ((bf16[8,64,2048]{2,1,0:T(8,128)(2,1)}), bf16[8,64,2048]{2,1,0:T(8,128)(2,1)S(1)}, u32[]{:S(2)}, u32[]{:S(2)}) async-start(bf16[8,64,2048]{2,1,0:T(8,128)(2,1)} %broadcast_in_dim.169), calls=%async_computation | async-start | bytes 4194304 | tf_op jit(solution)/shard_map/all_to_all | solution.py:19
  19.7 2.7 %pad_maximum_fusion = bf16[384,2048]{1,0:T(8,128)(2,1)} fusion(bf16[128,2048]{1,0:T(8,128)(2,1)} %param.27, bf16[256,2048]{1,0:T(8,128)(2,1)} %param.26), kind=kLoop, calls=%fused_computation.7 | loop fusion | flops 3145728 | bytes 3145728 | tf_op jit(solution)/shard_map/concatenate | solution.py:235
  29.1 17.3 %all-to-all-done = bf16[8,64,2048]{2,1,0:T(8,128)(2,1)S(1)} async-done(((bf16[8,64,2048]{2,1,0:T(8,128)(2,1)}), bf16[8,64,2048]{2,1,0:T(8,128)(2,1)S(1)}, u32[]{:S(2)}, u32[]{:S(2)}) %all-to-all-start) | async-done | bytes 2097184 | tf_op jit(solution)/shard_map/all_to_all | solution.py:19
  47.8 2.2 fusion.1
  54.7 4.6 %collective-permute-start.2 = (bf16[8,128]{1,0:T(8,128)(2,1)}, bf16[8,128]{1,0:T(8,128)(2,1)}, u32[]{:S(2)}, u32[]{:S(2)}) collective-permute-start(bf16[8,128]{1,0:T(8,128)(2,1)} %get-tuple-element.24), channel_id=1, source_target_pairs={{0,8},{8,16},{16,24},{24,32},{32,40},{40,48},{48,56},{56,64},{64,7... | collective-permute-start | bytes 6152 | tf_op jit(solution)/shard_map/ppermute | solution.py:31
  62.7 1.5 fusion.88
  67.9 2.2 copy.96
  70.1 2.2 fusion.87
  74.2 2.0 copy.137
  76.3 4.4 %multiply_reduce_fusion.1 = f32[32,256,16]{1,2,0:T(8,128)S(1)} fusion(f32[32,256,16]{1,2,0:T(8,128)} %bitcast.144, f32[32,16,256]{2,1,0:T(8,128)} %copy.98, pred[16,16]{1,0:T(8,128)(4,1)S(1)} %copy-done.37), kind=kLoop, calls=%fused_computation.1 | loop fusion | flops 10354688 | bytes 1573120
  88.4 2.1 copy.106
  91.9 2.4 %fusion.65 = (f32[32,16,256]{2,0,1:T(8,128)}, f32[32,16,256]{2,0,1:T(8,128)S(1)}, f32[32,16,256]{2,0,1:T(8,128)}) fusion(f32[32,16,256]{2,1,0:T(8,128)} %bitcast.125, f32[32,16,256]{2,0,1:T(8,128)S(1)} %fusion.34, f32[32,256]{1,0:T(8,128)S(1)} %slice_bitcast_fusion.2), kind=kLoop, calls=%fused_computation.209 | loop fusion | flops 262144 | bytes 2654208 | tf_op jit(solution)/shard_map/exp | solution.py:102
  96.2 2.1 copy.138
  98.2 4.2 %multiply_reduce_fusion = f32[32,256,16]{1,2,0:T(8,128)S(1)} fusion(f32[32,256,16]{1,2,0:T(8,128)} %bitcast.145, f32[32,16,256]{2,1,0:T(8,128)} %copy.109, pred[16,16]{1,0:T(8,128)(4,1)S(1)} %copy-done.36), kind=kLoop, calls=%fused_computation | loop fusion | flops 10354688 | bytes 1573120
  115.8 2.4 %broadcast_multiply_fusion = (f32[32,16,256]{2,0,1:T(8,128)S(1)}, f32[32,16,256]{2,0,1:T(8,128)}) fusion(f32[32,256]{1,0:T(8,128)S(1)} %concatenate.88, f32[32,16,256]{2,0,1:T(8,128)} %copy-done.4, f32[32,256]{1,0:T(8,128)S(1)} %concatenate.83, f32[32,256,16]{1,2,0:T(8,128)} %copy-done.11), kind=kLoop, calls=%fused_computation.73 | loop fusion | flops 393216 | bytes 2162688 | tf_op jit(solution)/shard_map/mul | solution.py:115
  119.9 2.0 copy.103
  124.6 2.1 copy.104
  128.3 1.6 multiply_add_fusion
  131.0 2.1 copy.112
  133.7 19.5 %all-to-all-start.1 = ((f32[64,2,256]{2,1,0:T(2,128)}), f32[64,2,256]{2,1,0:T(2,128)S(1)}, u32[]{:S(2)}, u32[]{:S(2)}) async-start(f32[64,2,256]{2,1,0:T(2,128)} %broadcast_in_dim.173), calls=%async_computation.1 | async-start | bytes 262144 | tf_op jit(solution)/shard_map/all_to_all | solution.py:19
  155.0 2.1 copy.115
  157.0 2.2 copy.113
  159.2 2.0 copy.114
  161.2 1.5 fusion.31
  164.6 2.0 fusion.3
  166.6 1.7 all-to-all-done.1
  168.9 13.1 %all-to-all-start.2 = ((f32[64,2,256]{2,1,0:T(2,128)}), f32[64,2,256]{2,1,0:T(2,128)S(1)}, u32[]{:S(2)}, u32[]{:S(2)}) async-start(f32[64,2,256]{2,1,0:T(2,128)} %broadcast_in_dim.178), calls=%async_computation.2 | async-start | bytes 262144 | tf_op jit(solution)/shard_map/all_to_all | solution.py:19
  183.3 13.8 %all-to-all-done.2 = f32[64,2,256]{2,1,0:T(2,128)S(1)} async-done(((f32[64,2,256]{2,1,0:T(2,128)}), f32[64,2,256]{2,1,0:T(2,128)S(1)}, u32[]{:S(2)}, u32[]{:S(2)}) %all-to-all-start.2) | async-done | bytes 131104 | tf_op jit(solution)/shard_map/all_to_all | solution.py:19
  198.7 2.8 %fusion.25 = bf16[512,256]{0,1:T(8,128)(2,1)S(1)} fusion(bf16[512,2048]{1,0:T(8,128)(2,1)S(1)} %fusion.1, bf16[2048,256]{1,0:T(8,128)(2,1)} %param.17, f32[512,256]{0,1:T(8,128)} %copy-done.5, f32[512,256]{0,1:T(8,128)} %copy.112, f32[512,256]{0,1:T(8,128)} %copy.104, f32[512,256]{0,1:T(8,128)} %copy.103, f32[256]{0:T(256)S(1)} %bitcast.147, ...), kind=kOutput, calls=%fused_computation.38 | convolution fusion | flops 539099136 | bytes 5507072 | tf_op jit(solution)/shard_map/dot_general | solution.py:83
  201.7 14.7 %all_to_all.34 = bf16[8,64,384]{2,1,0:T(8,128)(2,1)S(1)} all-to-all(bf16[8,64,384]{2,1,0:T(8,128)(2,1)S(1)} %bitcast.136), channel_id=1, replica_groups=mesh['sp'=64,'tp'=8] {'tp'}, dimensions={0} | all-to-all | bytes 786432 | tf_op jit(solution)/shard_map/all_to_all | solution.py:234
  216.5 7.6 %convolution_convert_fusion = bf16[64,2048]{1,0:T(8,128)(2,1)} fusion(bf16[64,3072]{1,0:T(8,128)(2,1)S(1)} %bitcast.126, bf16[3072,2048]{1,0:T(8,128)(2,1)} %all-gather.2.cloned.1.call-done), kind=kOutput, calls=%fused_computation.6 | convolution fusion | flops 805437440 | bytes 13238272 | tf_op jit(solution)/shard_map/dot_general | solution.py:83
  (361 shorter events, 60.4 us)
Async XLA Ops:
  6.5 43.5 %copy-start = (bf16[2048,256]{1,0:T(8,128)(2,1)S(1)}, bf16[2048,256]{1,0:T(8,128)(2,1)}, u32[]{:S(2)}) copy-start(bf16[2048,256]{1,0:T(8,128)(2,1)} %param.16) | copy-start | bytes 3145732
  9.1 13.3 %copy-start.24 = (bf16[2048]{0:T(1024)(128)(2,1)S(1)}, bf16[2048]{0:T(1024)(128)(2,1)}, u32[]{:S(2)}) copy-start(bf16[2048]{0:T(1024)(128)(2,1)} %param.15) | copy-start | bytes 12292
  9.1 13.3 %copy-start.15 = (bf16[2,2,4,64,64]{4,3,2,1,0:T(8,128)(2,1)S(1)}, bf16[2,2,4,64,64]{4,3,2,1,0:T(8,128)(2,1)}, u32[]{:S(2)}) copy-start(bf16[2,2,4,64,64]{4,3,2,1,0:T(8,128)(2,1)} %param.20) | copy-start | bytes 393220
  9.1 14.1 %copy-start.38 = (bf16[128]{0:T(256)(128)(2,1)S(1)}, bf16[128]{0:T(256)(128)(2,1)}, u32[]{:S(2)}) copy-start(bf16[128]{0:T(256)(128)(2,1)} %param.25) | copy-start | bytes 772
  9.1 18.7 %copy-start.33 = (f32[2,256]{1,0:T(2,128)S(1)}, f32[2,256]{1,0:T(2,128)}, u32[]{:S(2)}) copy-start(f32[2,256]{1,0:T(2,128)} %param.21) | copy-start | bytes 6148
  9.1 19.3 %copy-start.17 = (bf16[4,256]{1,0:T(4,128)(2,1)S(1)}, bf16[4,256]{1,0:T(4,128)(2,1)}, u32[]{:S(2)}) copy-start(bf16[4,256]{1,0:T(4,128)(2,1)} %param.19) | copy-start | bytes 6148
  9.2 19.9 %copy-start.29 = (f32[2,512]{1,0:T(2,128)S(1)}, f32[2,512]{1,0:T(2,128)}, u32[]{:S(2)}) copy-start(f32[2,512]{1,0:T(2,128)} %param.22) | copy-start | bytes 12292
  9.2 37.3 %all-to-all-start = ((bf16[8,64,2048]{2,1,0:T(8,128)(2,1)}), bf16[8,64,2048]{2,1,0:T(8,128)(2,1)S(1)}, u32[]{:S(2)}, u32[]{:S(2)}) async-start(bf16[8,64,2048]{2,1,0:T(8,128)(2,1)} %broadcast_in_dim.169), calls=%async_computation | async-start | bytes 4194304 | tf_op jit(solution)/shard_map/all_to_all | solution.py:19
  19.7 196.8 %all-gather.2.cloned.1.call-start = ((), (), s32[]{:S(2)}) async-start(), calls=%async_computation.4 | async-start | bytes 14155776 | tf_op jit(solution)/shard_map/all_gather | solution.py:236
  50.0 10.6 %copy-start.22 = (f32[1,256]{1,0:T(1,128)S(1)}, f32[1,256]{1,0:T(1,128)}, u32[]{:S(2)}) copy-start(f32[1,256]{1,0:T(1,128)} %get-tuple-element.88) | copy-start | bytes 3076
  50.0 10.6 %copy-start.23 = (f32[1,256]{1,0:T(1,128)S(1)}, f32[1,256]{1,0:T(1,128)}, u32[]{:S(2)}) copy-start(f32[1,256]{1,0:T(1,128)} %get-tuple-element.89) | copy-start | bytes 3076
  50.8 9.8 %collective-permute-start = (bf16[2,256]{1,0:T(2,128)(2,1)S(1)}, bf16[2,256]{1,0:T(2,128)(2,1)S(1)}, u32[]{:S(2)}, u32[]{:S(2)}) collective-permute-start(bf16[2,256]{1,0:T(2,128)(2,1)S(1)} %get-tuple-element.18), channel_id=1, source_target_pairs={{0,8},{8,16},{16,24},{24,32},{32,40},{40,48},{48,56},{56,64},{64,7... | collective-permute-start | bytes 3080 | tf_op jit(solution)/shard_map/ppermute | solution.py:31
  52.1 8.5 %collective-permute-start.1 = (bf16[2,256]{1,0:T(2,128)(2,1)S(1)}, bf16[2,256]{1,0:T(2,128)(2,1)S(1)}, u32[]{:S(2)}, u32[]{:S(2)}) collective-permute-start(bf16[2,256]{1,0:T(2,128)(2,1)S(1)} %get-tuple-element.19), channel_id=1, source_target_pairs={{8,0},{16,8},{24,16},{32,24},{40,32},{48,40},{56,48},{64,56},{72,6... | collective-permute-start | bytes 3080 | tf_op jit(solution)/shard_map/ppermute | solution.py:34
  54.7 109.0 %collective-permute-start.2 = (bf16[8,128]{1,0:T(8,128)(2,1)}, bf16[8,128]{1,0:T(8,128)(2,1)}, u32[]{:S(2)}, u32[]{:S(2)}) collective-permute-start(bf16[8,128]{1,0:T(8,128)(2,1)} %get-tuple-element.24), channel_id=1, source_target_pairs={{0,8},{8,16},{16,24},{24,32},{32,40},{40,48},{48,56},{56,64},{64,7... | collective-permute-start | bytes 6152 | tf_op jit(solution)/shard_map/ppermute | solution.py:31
  59.2 104.4 %collective-permute-start.3 = (bf16[8,128]{1,0:T(8,128)(2,1)}, bf16[8,128]{1,0:T(8,128)(2,1)}, u32[]{:S(2)}, u32[]{:S(2)}) collective-permute-start(bf16[8,128]{1,0:T(8,128)(2,1)} %get-tuple-element.25), channel_id=1, source_target_pairs={{8,0},{16,8},{24,16},{32,24},{40,32},{48,40},{56,48},{64,56},{72,6... | collective-permute-start | bytes 6152 | tf_op jit(solution)/shard_map/ppermute | solution.py:34
  66.6 9.7 %copy-start.37 = (pred[16,16]{1,0:T(8,128)(4,1)S(1)}, pred[16,16]{1,0:T(8,128)(4,1)}, u32[]{:S(2)}) copy-start(pred[16,16]{1,0:T(8,128)(4,1)} %iota_compare_fusion.1) | copy-start | bytes 772
  81.5 16.7 %copy-start.36 = (pred[16,16]{1,0:T(8,128)(4,1)S(1)}, pred[16,16]{1,0:T(8,128)(4,1)}, u32[]{:S(2)}) copy-start(pred[16,16]{1,0:T(8,128)(4,1)} %iota_compare_fusion) | copy-start | bytes 772
  111.3 15.4 %copy-start.18 = (f32[2,256]{1,0:T(2,128)S(1)}, f32[2,256]{1,0:T(2,128)}, u32[]{:S(2)}) copy-start(f32[2,256]{1,0:T(2,128)} %slice.745) | copy-start | bytes 6148
  111.3 15.4 %copy-start.19 = (f32[2,256]{1,0:T(2,128)S(1)}, f32[2,256]{1,0:T(2,128)}, u32[]{:S(2)}) copy-start(f32[2,256]{1,0:T(2,128)} %slice.746) | copy-start | bytes 6148
  112.0 14.7 %copy-start.20 = (f32[2,256]{1,0:T(2,128)S(1)}, f32[2,256]{1,0:T(2,128)}, u32[]{:S(2)}) copy-start(f32[2,256]{1,0:T(2,128)} %slice.744) | copy-start | bytes 6148
  112.7 14.0 %copy-start.21 = (f32[2,256]{1,0:T(2,128)S(1)}, f32[2,256]{1,0:T(2,128)}, u32[]{:S(2)}) copy-start(f32[2,256]{1,0:T(2,128)} %slice.748) | copy-start | bytes 6148
  114.9 12.0 %copy-start.28 = (f32[1,256]{1,0:T(1,128)S(1)}, f32[1,256]{1,0:T(1,128)}, u32[]{:S(2)}) copy-start(f32[1,256]{1,0:T(1,128)} %slice.894) | copy-start | bytes 3076
  114.9 12.1 %copy-start.27 = (f32[1,256]{1,0:T(1,128)S(1)}, f32[1,256]{1,0:T(1,128)}, u32[]{:S(2)}) copy-start(f32[1,256]{1,0:T(1,128)} %slice.877) | copy-start | bytes 3076
  115.0 12.2 %copy-start.26 = (f32[1,256]{1,0:T(1,128)S(1)}, f32[1,256]{1,0:T(1,128)}, u32[]{:S(2)}) copy-start(f32[1,256]{1,0:T(1,128)} %slice.876) | copy-start | bytes 3076
  115.0 12.2 %copy-start.25 = (f32[1,256]{1,0:T(1,128)S(1)}, f32[1,256]{1,0:T(1,128)}, u32[]{:S(2)}) copy-start(f32[1,256]{1,0:T(1,128)} %slice.893) | copy-start | bytes 3076
  126.7 6.3 %copy-start.30 = (f32[1,256]{1,0:T(1,128)S(1)}, f32[1,256]{1,0:T(1,128)}, u32[]{:S(2)}) copy-start(f32[1,256]{1,0:T(1,128)} %slice.862) | copy-start | bytes 3076
  126.8 6.3 %copy-start.31 = (f32[1,256]{1,0:T(1,128)S(1)}, f32[1,256]{1,0:T(1,128)}, u32[]{:S(2)}) copy-start(f32[1,256]{1,0:T(1,128)} %slice.863) | copy-start | bytes 3076
  133.7 34.5 %all-to-all-start.1 = ((f32[64,2,256]{2,1,0:T(2,128)}), f32[64,2,256]{2,1,0:T(2,128)S(1)}, u32[]{:S(2)}, u32[]{:S(2)}) async-start(f32[64,2,256]{2,1,0:T(2,128)} %broadcast_in_dim.173), calls=%async_computation.1 | async-start | bytes 262144 | tf_op jit(solution)/shard_map/all_to_all | solution.py:19
  157.0 7.5 %copy-start.34 = (f32[512]{0:T(512)S(1)}, f32[512]{0:T(512)}, u32[]{:S(2)}) copy-start(f32[512]{0:T(512)} %get-tuple-element.100) | copy-start | bytes 6148
  157.0 7.5 %copy-start.35 = (f32[512]{0:T(512)S(1)}, f32[512]{0:T(512)}, u32[]{:S(2)}) copy-start(f32[512]{0:T(512)} %get-tuple-element.101) | copy-start | bytes 6148
  168.9 28.1 %all-to-all-start.2 = ((f32[64,2,256]{2,1,0:T(2,128)}), f32[64,2,256]{2,1,0:T(2,128)S(1)}, u32[]{:S(2)}, u32[]{:S(2)}) async-start(f32[64,2,256]{2,1,0:T(2,128)} %broadcast_in_dim.178), calls=%async_computation.2 | async-start | bytes 262144 | tf_op jit(solution)/shard_map/all_to_all | solution.py:19
  182.9 18.5 %copy-start.16 = (bf16[512,128]{0,1:T(8,128)(2,1)S(1)}, bf16[512,128]{0,1:T(8,128)(2,1)}, u32[]{:S(2)}) copy-start(bf16[512,128]{0,1:T(8,128)(2,1)} %fusion.3) | copy-start | bytes 393220
  (15 other events, 21.3 us)
Sparse Core Ops, SparseCore 0:
  22.6 76.5 all-gather.1
where the time goes:
time: 233 us; the launch traced here: 231 us
  local copies, waits for them, and re-layouts  63.2 us (27%)
  starting transfers between devices  51.5 us (22%)
  other arithmetic  38.7 us (17%)
  waiting for transfers between devices  32.8 us (14%)
  matrix products  15.2 us (7%)
  blocking collectives  14.7 us (6%)
  between operations  14.7 us (6%)
    all_to_all x3, starting transfers between devices, sent_to_all(): return lax.all_to_all(copies, axis, split_axis=0, concat_axis=0, tiled=True)  43.1 us
    all_to_all x3, waiting for transfers between devices, sent_to_all(): return lax.all_to_all(copies, axis, split_axis=0, concat_axis=0, tiled=True)  32.8 us
    unnamed x85, local copies, waits for them, and re-layouts  14.9 us
    all_to_all x1, blocking collectives, local(): lax.all_to_all(joined, 'tp', split_axis=0, concat_axis=1, tiled=True)  14.7 us
    dot_general x4, matrix products, product(): return jnp.dot(left, right, preferred_element_type=jnp.float32)  11.8 us
    unnamed x2, other arithmetic  8.65 us
    slice x34, local copies, waits for them, and re-layouts, block_chain(): lax.associative_scan(combine, ends, axis=0, reverse=True)  6.76 us
    slice x28, local copies, waits for them, and re-layouts, block_chain(): total_keep, total_state = lax.associative_scan(combine, ends, axis=0)  6.4 us
  transfers between devices with their start and end apart: 8, of which 3 were waited for; matrix products, arithmetic and copies ran while one was open for 42% of the time, Pallas kernels for 0%

commit v1 on v0

v1 whole, which is shorter than its diff:
```python
import jax
import jax.numpy as jnp
from jax import lax
from jax.experimental import pallas as pl
from jax.experimental.pallas import tpu as pltpu
from jax.sharding import PartitionSpec as P

FADING_FACTOR = 8.0
epsilon = 1e-06

SEG = 8
STEP = 64
ROWS = SEG * STEP
EDGE = 8
WIDE = 2048
CH = 256
PC = 128
F32 = jnp.float32
BF16 = jnp.bfloat16
VMEM = pltpu.VMEM


def vspecs(n):
    return [pl.BlockSpec(memory_space=VMEM)] * n


def params():
    return pltpu.CompilerParams(vmem_limit_bytes=48 * 1024 * 1024)


def cost(flops, nbytes, trans=0):
    return pl.CostEstimate(flops=flops, bytes_accessed=nbytes, transcendentals=trans)


def dot(a, b):
    return jnp.dot(a, b, preferred_element_type=F32)


def normalize(read, write, gain_ref, rows):
    total = jnp.zeros((rows, 128), F32)
    for k in range(WIDE // 128):
        v = read(k * 128).astype(F32)
        total = total + v * v
    inv = lax.rsqrt(jnp.sum(total, axis=1, keepdims=True) * (1.0 / WIDE) + epsilon)
    for k in range(WIDE // 128):
        v = read(k * 128).astype(F32)
        gain = gain_ref[0:1, k * 128 : (k + 1) * 128].astype(F32)
        write(k * 128, ((v * inv) * gain).astype(BF16))


def normalize_shards(x_ref, gain_ref, out_ref):
    def one(i, _):
        base = pl.multiple_of(i * STEP, STEP)

        def read(lane):
            return x_ref[i, :, lane : lane + 128]

        def write(lane, v):
            out_ref[pl.ds(base, STEP), lane : lane + 128] = v

        normalize(read, write, gain_ref, STEP)
        return 0

    lax.fori_loop(0, 4, one, 0)


def project_kernel(x_ref, gain_ref, ws_ref, wg_ref, wp_ref, y_ref, xn_ref):
    normalize_shards(x_ref, gain_ref, xn_ref)
    xn = xn_ref[...]
    y_ref[:, 0:256] = dot(xn, ws_ref[...]).astype(BF16)
    y_ref[:, 256:512] = dot(xn, wg_ref[...]).astype(BF16)
    y_ref[:, 512:640] = dot(xn, wp_ref[...]).astype(BF16)


def gates_kernel(
    x_ref, h1_ref, h2_ref, yo_ref, gain_ref, ws_ref, wg_ref, wp_ref, perm_ref, conv_ref, bd_ref,
    half_rate_ref, extra_ref,
    kd_ref, gate_ref, pool_ref, seg_ref, send_ref,
    xn_ref, y_ref, s_ref, f_ref, g_ref,
):
    normalize_shards(x_ref, gain_ref, xn_ref)
    for n, ref in enumerate((h1_ref, h2_ref)):
        base = 256 + n * EDGE

        def read(lane, ref=ref):
            return ref[:, lane : lane + 128]

        def write(lane, v, base=base):
            xn_ref[base : base + EDGE, lane : lane + 128] = v

        normalize(read, write, gain_ref, EDGE)
    y_ref[0:256, :] = yo_ref[...]
    xn = xn_ref[...]
    y_ref[256:528, 0:256] = dot(xn, ws_ref[...]).astype(BF16)
    y_ref[256:528, 256:512] = dot(xn, wg_ref[...]).astype(BF16)
    y_ref[256:528, 512:640] = dot(xn, wp_ref[...]).astype(BF16)
    lo = (EDGE - 2) * SEG
    s_ref[...] = dot(perm_ref[lo : lo + 67 * SEG, :], y_ref[:, 0:256])
    mid = EDGE * SEG
    gate_ref[...] = dot(perm_ref[mid : mid + ROWS, :], y_ref[:, 256:512])
    pool_ref[...] = dot(perm_ref[...], y_ref[:, 512:640])
    taps = conv_ref[...].astype(F32)

    def conv(i, _):
        base = pl.multiple_of(i * 64, 64)
        value = taps[0:1] * s_ref[pl.ds(base, 64), :]
        for k in range(1, 4):
            value = value + taps[k : k + 1] * s_ref[pl.ds(base + 8 * k, 64), :]
        f_ref[pl.ds(base, 64), :] = value.astype(BF16)
        return 0

    lax.fori_loop(0, ROWS // 64, conv, 0)
    f = f_ref[...]
    for k in range(4):
        g_ref[:, k * 256 : (k + 1) * 256] = dot(f, bd_ref[:, k * 256 : (k + 1) * 256])

    def chunk(i, carry):
        base = pl.multiple_of(i * 64, 64)
        rows = pl.ds(base, 64)
        out = []
        for lt in range(2):
            hf, lf, hb, pb, lb = carry[lt]
            lanes = slice(lt * 128, lt * 128 + 128)
            wide = f_ref[rows, lanes].astype(F32)
            for d in range(2):
                col = d * 512 + lt * 128
                half = half_rate_ref[d : d + 1, lanes]
                recall = jnp.tanh(0.5 * g_ref[rows, col : col + 128])
                inlet = 0.5 * jnp.tanh(0.5 * g_ref[rows, col + 256 : col + 384]) + 0.5
                log_keep = half * recall + half + extra_ref[d, rows, :]
                keep = jnp.exp(log_keep)
                gap = (1.0 + keep * keep) * jnp.tanh(-log_keep)
                drive = gap * lax.rsqrt(jnp.maximum(gap, 1e-37)) * (inlet * wide)
                kd_ref[2 * d, rows, lanes] = keep
                kd_ref[2 * d + 1, rows, lanes] = drive
                for j in range(8):
                    kj = keep[8 * j : 8 * j + 8]
                    uj = drive[8 * j : 8 * j + 8]
                    lj = log_keep[8 * j : 8 * j + 8]
                    if d == 0:
                        hf = kj * hf + uj
                        lf = lf + lj
                    else:
                        hb = hb + pb * uj
                        pb = pb * kj
                        lb = lb + lj
            out.append((hf, lf, hb, pb, lb))
        return tuple(out)

    zero = jnp.zeros((SEG, 128), F32)
    one = jnp.ones((SEG, 128), F32)
    totals = lax.fori_loop(0, ROWS // 64, chunk, tuple((zero, zero, zero, one, zero) for _ in range(2)))
    row = lax.broadcasted_iota(jnp.int32, (SEG, 128), 0)
    send = jnp.zeros((SEG, 128), F32)
    for lt in range(2):
        hf, lf, hb, pb, lb = totals[lt]
        lanes = slice(lt * 128, lt * 128 + 128)
        for d, (log_total, state) in enumerate(((lf, hf), (lb, hb))):
            factor = jnp.exp(log_total)
            for shift in (1, 2, 4):
                move = shift if d == 0 else SEG - shift
                inside = (row >= shift) if d == 0 else (row < SEG - shift)
                earlier_factor = jnp.where(inside, pltpu.roll(factor, move, 0), 1.0)
                earlier_state = jnp.where(inside, pltpu.roll(state, move, 0), 0.0)
                state = factor * earlier_state + state
                factor = factor * earlier_factor
            move = 1 if d == 0 else SEG - 1
            inside = (row >= 1) if d == 0 else (row < SEG - 1)
            seg_ref[2 * d, :, lanes] = jnp.where(inside, pltpu.roll(factor, move, 0), 1.0)
            seg_ref[2 * d + 1, :, lanes] = jnp.where(inside, pltpu.roll(state, move, 0), 0.0)
            end = SEG - 1 if d == 0 else 0
            whole_log = jnp.sum(log_total, axis=0, keepdims=True)
            whole_state = jnp.sum(jnp.where(row == end, state, 0.0), axis=0, keepdims=True)
            send = jnp.where(row == 4 * d + lt, whole_log, send)
            send = jnp.where(row == 4 * d + 2 + lt, whole_state, send)
    packed = send.astype(BF16)
    send_ref[...] = jnp.broadcast_to(packed[None], send_ref.shape)


def pooling_kernel(gate_ref, pool_ref, inverse_ref, code_ref, cluster_ref, factor_ref, act_ref, mix_ref, p_ref):
    def gelu(i, _):
        rows = pl.ds(pl.multiple_of(i * 64, 64), 64)
        v = gate_ref[rows, :]
        inner = 0.7978845608028654 * (v + 0.044715 * (v * v * v))
        act_ref[rows, :] = v * (0.5 * (1.0 + jnp.tanh(inner)))
        return 0

    lax.fori_loop(0, ROWS // 64, gelu, 0)
    code = code_ref[0]

    def windows(i, _):
        base = pl.multiple_of(i * 64, 64)
        level = pool_ref[pl.ds(base, 64 + 2 * EDGE * SEG), :]
        centre = level[EDGE * SEG : EDGE * SEG + 64]
        chosen = jnp.zeros((64, PC), F32)
        for k in range(4):
            shift = SEG << k
            size = level.shape[0] - shift
            level = level[:size] + level[shift:]
            begin = (EDGE - (1 << k)) * SEG
            chosen = jnp.where(code == k, level[begin : begin + 64], chosen)
        rows = pl.ds(base, 64)
        p_ref[rows, :] = (chosen * inverse_ref[rows, :] - centre).astype(BF16)
        return 0

    lax.fori_loop(0, ROWS // 64, windows, 0)
    grouped = dot(p_ref[...], cluster_ref[...])
    mix_ref[...] = (grouped * factor_ref[...].astype(F32)).astype(BF16)


def states_kernel(
    got_ref, after_ref, valid_ref, seg_ref, kd_ref, act_ref, pool_mix_ref, back_ref,
    send_ref, own_ref,
    hf_ref, hb_ref, mix_ref,
):
    got = got_ref[...].reshape(-1, 128)
    sums = dot(after_ref[...], got)
    terms = jnp.exp(sums) * valid_ref[...] * got.astype(F32)
    carry = jnp.sum(terms.reshape(-1, SEG, 128), axis=0)
    begin = []
    for lt in range(2):
        lanes = slice(lt * 128, lt * 128 + 128)
        for d in range(2):
            r = 4 * d + 2 + lt
            begin.append(seg_ref[2 * d, :, lanes] * carry[r : r + 1] + seg_ref[2 * d + 1, :, lanes])

    def walk(i, carry):
        hf0, hb0, hf1, hb1 = carry
        for k in range(8):
            f = pl.ds(pl.multiple_of((i * 8 + k) * SEG, SEG), SEG)
            b = pl.ds(pl.multiple_of((STEP - 1 - i * 8 - k) * SEG, SEG), SEG)
            hf0 = kd_ref[0, f, 0:128] * hf0 + kd_ref[1, f, 0:128]
            hf1 = kd_ref[0, f, 128:256] * hf1 + kd_ref[1, f, 128:256]
            hb0 = kd_ref[2, b, 0:128] * hb0 + kd_ref[3, b, 0:128]
            hb1 = kd_ref[2, b, 128:256] * hb1 + kd_ref[3, b, 128:256]
            hf_ref[f, 0:128] = hf0
            hf_ref[f, 128:256] = hf1
            hb_ref[b, 0:128] = hb0
            hb_ref[b, 128:256] = hb1
        return hf0, hb0, hf1, hb1

    lax.fori_loop(0, STEP // 8, walk, tuple(begin))

    def mixing(i, _):
        rows = pl.ds(pl.multiple_of(i * 64, 64), 64)
        mix_ref[rows, 0:CH] = (act_ref[rows, :] * (hf_ref[rows, :] + hb_ref[rows, :])).astype(BF16)
        return 0

    lax.fori_loop(0, ROWS // 64, mixing, 0)
    mix_ref[:, CH : CH + PC] = pool_mix_ref[...]
    mix = mix_ref[...]
    send_ref[...] = dot(back_ref[0:256, :], mix).astype(BF16)
    own_ref[...] = dot(back_ref[256:512, :], mix).astype(BF16)


def output_kernel(own_ref, got_ref, wr_ref, wp_ref, vr_ref, vp_ref, out_ref):
    own_state = own_ref[:, 0:CH]
    own_pool = own_ref[:, CH : CH + PC]
    got_state = got_ref[:, 0:CH]
    got_pool = got_ref[:, CH : CH + PC]
    for k in range(4):
        lanes = slice(k * 512, k * 512 + 512)
        value = dot(own_state, wr_ref[:, lanes]) + dot(got_state, vr_ref[:, lanes])
        value = value + dot(own_pool, wp_ref[:, lanes]) + dot(got_pool, vp_ref[:, lanes])
        value = value.astype(BF16)
        for x in range(4):
            out_ref[x, :, lanes] = value[x * STEP : (x + 1) * STEP]


def local(
    incoming_activity,
    entry_standardize_factor,
    recursive_entry_matrix,
    final_switch_matrix,
    averaging_entry_matrix,
    percolumn_filter_coefficients,
    switch_tiled_matrices,
    prior_fading_odds,
    speed_factors,
    extra_fading_amounts,
    averaging_cluster_matrices,
    averaging_feature_factor,
    recursive_final_matrix,
    averaging_final_matrix,
):
    blocks = lax.axis_size("sp")
    place = lax.axis_index("sp")
    column = lax.axis_index("tp")
    core = column % 2
    same_core = [[0, 2, 4, 6], [1, 3, 5, 7]]
    sibling = [(k, k ^ 1) for k in range(8)]

    def exchange(v):
        return lax.all_to_all(
            v, "tp", split_axis=0, concat_axis=0, tiled=True, axis_index_groups=same_core
        )

    def edge_pairs(cross):
        pairs = []
        for sp in range(blocks):
            for tp in range(8):
                to = sp + 1 if tp % 2 else sp - 1
                if 0 <= to < blocks:
                    pairs.append((sp * 8 + tp, to * 8 + (tp ^ cross)))
        return pairs

    x_own = exchange(jnp.broadcast_to(incoming_activity, (4, *incoming_activity.shape)))
    edge = lax.dynamic_slice(
        x_own, (3 * core, (STEP - EDGE) * core, 0), (1, EDGE, WIDE)
    ).reshape(EDGE, WIDE)
    edge_same = lax.ppermute(edge, ("sp", "tp"), edge_pairs(0))
    edge_cross = lax.ppermute(edge, ("sp", "tp"), edge_pairs(1))
    x_sibling = lax.ppermute(x_own, "tp", sibling)
    sibling_recursive = lax.ppermute(recursive_final_matrix, "tp", sibling)
    sibling_averaging = lax.ppermute(averaging_final_matrix, "tp", sibling)

    wide_row = jnp.arange((STEP + 2 * EDGE) * SEG, dtype=jnp.int32)
    t = (wide_row % SEG) * STEP + wide_row // SEG - EDGE
    shard = t // STEP
    held = jnp.where(shard % 2 == core, 0, 256) + (shard // 2) * STEP + t % STEP
    before = jnp.where(core == 1, 512, 520)
    held = jnp.where(t < 0, before + t + EDGE, held)
    held = jnp.where(t >= ROWS, (1032 - before) + t - ROWS, held)
    perm = (held[:, None] == jnp.arange(528, dtype=jnp.int32)[None, :]).astype(BF16)
    out_row = jnp.arange(ROWS, dtype=jnp.int32)
    parity = jnp.where(out_row < 256, 1 - core, core)
    source = (out_row % STEP) * SEG + 2 * ((out_row % 256) // STEP) + parity
    back = (source[:, None] == jnp.arange(ROWS, dtype=jnp.int32)[None, :]).astype(BF16)

    entry = jnp.arange(blocks * SEG, dtype=jnp.int32)
    p, r = entry[:, None] // SEG, entry[:, None] % SEG
    q, r2 = entry[None, :] // SEG, entry[None, :] % SEG
    between = jnp.where(r < 4, (q > p) & (q < place), (q < p) & (q > place))
    after = (between & (r2 == r - 2) & (r % 4 >= 2)).astype(BF16)
    valid = jnp.where(r < 4, p < place, p > place) & (r % 4 >= 2)
    valid = jnp.broadcast_to(valid.astype(F32), (blocks * SEG, 128))

    eye = jnp.eye(4, dtype=BF16)
    maps = jnp.transpose(switch_tiled_matrices, (2, 3, 0, 1, 4))
    maps = (maps[:, :, :, :, None, :] * eye[:, None, None, None, :, None]).reshape(CH, 4 * CH)
    half_rate = (-0.5 * FADING_FACTOR) * speed_factors[:, :1] * jax.nn.softplus(-prior_fading_odds)
    extra = jnp.transpose(extra_fading_amounts.reshape(2, SEG, STEP), (0, 2, 1)).reshape(2, ROWS, 1)
    extra = jnp.broadcast_to(extra, (2, ROWS, 128))
    window_code = column % 4
    reach = jnp.left_shift(1, window_code)
    mid_row = jnp.arange(ROWS, dtype=jnp.int32)
    position = place * ROWS + (mid_row % SEG) * STEP + mid_row // SEG
    count = jnp.minimum(position + reach, ROWS * blocks) - jnp.maximum(position - reach, 0)
    inverse = jnp.broadcast_to((1.0 / count.astype(F32))[:, None], (ROWS, PC))
    gain = entry_standardize_factor.reshape(1, WIDE)
    entry_weights = (recursive_entry_matrix, final_switch_matrix, averaging_entry_matrix)

    y_own = pl.pallas_call(
        project_kernel,
        out_shape=jax.ShapeDtypeStruct((256, 640), BF16),
        in_specs=vspecs(5),
        out_specs=pl.BlockSpec(memory_space=VMEM),
        scratch_shapes=[VMEM((256, WIDE), BF16)],
        compiler_params=params(),
        cost_estimate=cost(2 * 256 * WIDE * 640, 4_000_000),
        name="project",
    )(x_own, gain, *entry_weights)

    kd, gate, pool, seg, send = pl.pallas_call(
        gates_kernel,
        out_shape=(
            jax.ShapeDtypeStruct((4, ROWS, CH), F32),
            jax.ShapeDtypeStruct((ROWS, CH), F32),
            jax.ShapeDtypeStruct((ROWS + 2 * EDGE * SEG, PC), F32),
            jax.ShapeDtypeStruct((4, SEG, CH), F32),
            jax.ShapeDtypeStruct((blocks, SEG, 128), BF16),
        ),
        in_specs=vspecs(13),
        out_specs=tuple(vspecs(5)),
        scratch_shapes=[
            VMEM((272, WIDE), BF16),
            VMEM((528, 640), BF16),
            VMEM((67 * SEG, CH), F32),
            VMEM((ROWS, CH), BF16),
            VMEM((ROWS, 4 * CH), F32),
        ],
        compiler_params=params(),
        cost_estimate=cost(4 * 272 * WIDE * 640, 8_000_000, 1_000_000),
        name="gates",
    )(
        x_sibling, edge_same, edge_cross, y_own, gain, *entry_weights, perm,
        percolumn_filter_coefficients, maps, half_rate, extra,
    )

    got = lax.all_to_all(send, "sp", split_axis=0, concat_axis=0, tiled=True)

    act, pool_mix = pl.pallas_call(
        pooling_kernel,
        out_shape=(
            jax.ShapeDtypeStruct((ROWS, CH), F32),
            jax.ShapeDtypeStruct((ROWS, PC), BF16),
        ),
        in_specs=[*vspecs(3), pl.BlockSpec(memory_space=pltpu.SMEM), *vspecs(2)],
        out_specs=tuple(vspecs(2)),
        scratch_shapes=[VMEM((ROWS, PC), BF16)],
        compiler_params=params(),
        cost_estimate=cost(1_000_000_000, 2_000_000, 200_000),
        name="pooling",
    )(
        gate, pool, inverse, window_code.reshape(1), averaging_cluster_matrices.reshape(PC, PC),
        averaging_feature_factor.reshape(1, PC),
    )

    mix_send, mix_own = pl.pallas_call(
        states_kernel,
        out_shape=(
            jax.ShapeDtypeStruct((256, CH + PC), BF16),
            jax.ShapeDtypeStruct((256, CH + PC), BF16),
        ),
        in_specs=vspecs(8),
        out_specs=tuple(vspecs(2)),
        scratch_shapes=[
            VMEM((ROWS, CH), F32),
            VMEM((ROWS, CH), F32),
            VMEM((ROWS, CH + PC), BF16),
        ],
        compiler_params=params(),
        cost_estimate=cost(1_000_000_000, 4_000_000, 100_000),
        name="states",
    )(got, after, valid, seg, kd, act, pool_mix, back)

    mix_got = lax.ppermute(mix_send, "tp", sibling)

    partial = pl.pallas_call(
        output_kernel,
        out_shape=jax.ShapeDtypeStruct((4, STEP, WIDE), BF16),
        in_specs=vspecs(6),
        out_specs=pl.BlockSpec(memory_space=VMEM),
        compiler_params=params(),
        cost_estimate=cost(4 * 256 * 384 * WIDE, 5_000_000),
        name="output",
    )(
        mix_own, mix_got, recursive_final_matrix, averaging_final_matrix, sibling_recursive,
        sibling_averaging,
    )
    moved = exchange(partial)
    return jnp.sum(moved.astype(F32), axis=0).astype(BF16)


def solution(mesh):
    in_specs = (
        P(("sp", "tp"), None),
        P(),
        P(None, "tp"),
        P(None, "tp"),
        P(None, "tp"),
        P(None, "tp"),
        P(None, None, "tp", None, None),
        P(None, "tp"),
        P(None, "sp"),
        P(None, "sp"),
        P("tp", None, None),
        P("tp"),
        P("tp", None),
        P("tp", None),
    )
    out_specs = P(("sp", "tp"), None)
    return jax.shard_map(local, mesh=mesh, in_specs=in_specs, out_specs=out_specs, check_vma=False)
```

time: 233 us -> 113 us (0.48)
  local copies, waits for them, and re-layouts: 63.2 us -> 10.8 us
  other arithmetic: 38.7 us -> 5.11 us
  waiting for transfers between devices: 32.8 us -> 13.8 us
  matrix products: 15.2 us -> 0 us
  between operations: 14.7 us -> 0.5 us
  Pallas kernels: 0 us -> 13.6 us
  blocking collectives: 14.7 us -> 17.2 us
    slice x125 -> x0, local copies, waits for them, and re-layouts: 22.1 us -> none  [the longest x34 6.76 us: block_chain(): lax.associative_scan(combine, ends, axis=0, reverse=True)]
    all_to_all x3 -> x2, waiting for transfers between devices: 32.8 us -> 11.8 us  [the longest x1 11.8 us: local(): got = lax.all_to_all(send, 'sp', split_axis=0, concat_axis=0, tiled=True)]
    all_to_all x3 -> x2, starting transfers between devices: 43.1 us -> 25.2 us  [the longest x1 20.2 us: local(): got = lax.all_to_all(send, 'sp', split_axis=0, concat_axis=0, tiled=True)]
    ppermute x4 -> x6, starting transfers between devices: 8.41 us -> 26 us  [the longest x1 7.44 us: local(): sibling_recursive = lax.ppermute(recursive_final_matrix, 'tp', sibling)]
    dot_general x5 -> x0, matrix products: 13.8 us -> none  [the longest x4 11.8 us: product(): return jnp.dot(left, right, preferred_element_type=jnp.float32)]
    pallas_call x0 -> x5, Pallas kernels: none -> 13.6 us  [the longest x1 6.97 us: local(): pl.pallas_call(gates_kernel, out_shape=(jax.ShapeDtypeStruct((4, ROWS, CH...]
    unnamed x85 -> x38, local copies, waits for them, and re-layouts: 14.9 us -> 4.62 us
    unnamed x2 -> x0, other arithmetic: 8.65 us -> none
  transfers between devices with their start and end apart: 8 -> 8, of which waited for: 3 -> 3; matrix products, arithmetic and copies ran while one was open for 42% -> 7% of each run, Pallas kernels for 0% -> 9%
where the time goes in v1:
time: 113 us; the launch traced here: 112 us
  starting transfers between devices  51.2 us (45%)
  blocking collectives  17.2 us (15%)
  waiting for transfers between devices  13.8 us (12%)
  Pallas kernels  13.6 us (12%)
  local copies, waits for them, and re-layouts  10.8 us (10%)
  other arithmetic  5.11 us (5%)
    all_to_all x1, starting transfers between devices, local(): got = lax.all_to_all(send, 'sp', split_axis=0, concat_axis=0, tiled=True)  20.2 us
    all_to_all x1, blocking collectives, exchange(): lax.all_to_all(v, 'tp', split_axis=0, concat_axis=0, tiled=True, axis_ind...  17.2 us
    all_to_all x1, waiting for transfers between devices, local(): got = lax.all_to_all(send, 'sp', split_axis=0, concat_axis=0, tiled=True)  11.8 us
    ppermute x1, starting transfers between devices, local(): sibling_recursive = lax.ppermute(recursive_final_matrix, 'tp', sibling)  7.44 us
    pallas_call x1, Pallas kernels, local(): pl.pallas_call(gates_kernel, out_shape=(jax.ShapeDtypeStruct((4, ROWS, CH...  6.97 us
    ppermute x1, starting transfers between devices, local(): x_sibling = lax.ppermute(x_own, 'tp', sibling)  6.14 us
    all_to_all x1, starting transfers between devices, exchange(): lax.all_to_all(v, 'tp', split_axis=0, concat_axis=0, tiled=True, axis_ind...  4.96 us
    ppermute x1, starting transfers between devices, local(): mix_got = lax.ppermute(mix_send, 'tp', sibling)  4.92 us
  transfers between devices with their start and end apart: 8, of which 3 were waited for; matrix products, arithmetic and copies ran while one was open for 7% of the time, Pallas kernels for 9%

profile of v1, /device:TPU:1, one launch (start us, length us, event | category | flops | bytes accessed | tf_op | source)
XLA Modules:
  0.0 112.2 jit_solution(1694233087730534489)
XLA Ops:
  0.0 2.1 %broadcast_in_dim.32 = bf16[4,64,2048]{2,1,0:T(8,128)(2,1)} broadcast(bf16[64,2048]{1,0:T(8,128)(2,1)} %param.14), dimensions={1,2} | broadcast | bytes 1310720 | tf_op jit(solution)/shard_map/broadcast_in_dim | solution.py:307
  2.1 5.0 %all-to-all-start = ((bf16[4,64,2048]{2,1,0:T(8,128)(2,1)}), bf16[4,64,2048]{2,1,0:T(8,128)(2,1)S(1)}, u32[]{:S(2)}, u32[]{:S(2)}) async-start(bf16[4,64,2048]{2,1,0:T(8,128)(2,1)} %broadcast_in_dim.32), calls=%async_computation | async-start | bytes 2097152 | tf_op jit(solution)/shard_map/all_to_all | solution.py:294
  7.1 7.4 %collective-permute-start.4 = (bf16[256,2048]{1,0:T(8,128)(2,1)}, bf16[256,2048]{1,0:T(8,128)(2,1)}, u32[]{:S(2)}, u32[]{:S(2)}) collective-permute-start(bf16[256,2048]{1,0:T(8,128)(2,1)} %wr_ref.1), channel_id=1, source_target_pairs={{0,1},{1,0},{2,3},{3,2},{4,5},{5,4},{6,7},{7,6},{8,9},{9,8},{10,11... | collective-permute-start | bytes 3145736 | tf_op jit(solution)/shard_map/ppermute | solution.py:314
  14.5 1.9 %collective-permute-start.5 = (bf16[128,2048]{1,0:T(8,128)(2,1)}, bf16[128,2048]{1,0:T(8,128)(2,1)}, u32[]{:S(2)}, u32[]{:S(2)}) collective-permute-start(bf16[128,2048]{1,0:T(8,128)(2,1)} %wp_ref.5), channel_id=1, source_target_pairs={{0,1},{1,0},{2,3},{3,2},{4,5},{5,4},{6,7},{7,6},{8,9},{9,8},{10,11... | collective-permute-start | bytes 1572872 | tf_op jit(solution)/shard_map/ppermute | solution.py:315
  16.5 0.3 copy.17
  16.8 0.8 multiply_reduce_fusion
  17.7 1.5 %broadcast_multiply_fusion = bf16[4,64,2,2,4,64]{5,4,3,2,1,0:T(4,128)(2,1)} fusion(bf16[4,4]{1,0:T(4,128)(2,1)S(1)} %fusion.44, bf16[4,64,2,2,64]{4,3,2,1,0:T(2,128)(2,1)S(1)} %copy.17), kind=kLoop, calls=%fused_computation.5 | loop fusion | flops 262144 | bytes 655392 | tf_op jit(solution)/shard_map/mul | solution.py:340
  19.2 6.1 %collective-permute-start = (bf16[4,64,2048]{2,1,0:T(8,128)(2,1)S(1)}, bf16[4,64,2048]{2,1,0:T(8,128)(2,1)}, u32[]{:S(2)}, u32[]{:S(2)}) collective-permute-start(bf16[4,64,2048]{2,1,0:T(8,128)(2,1)S(1)} %all-to-all-done.x_ref), channel_id=1, source_target_pairs={{0,1},{1,0},{2,3},{3,2},{4,5},{5,4},{6,7},{7,6},{8,9},{9,8},{10,11... | collective-permute-start | bytes 3145736 | tf_op jit(solution)/shard_map/ppermute | solution.py:313
  25.4 3.1 %mul.90.bd_ref = bf16[256,1024]{1,0:T(8,128)(2,1)} reshape(bf16[4,64,2,2,4,64]{5,4,3,2,1,0:T(4,128)(2,1)} %broadcast_multiply_fusion) | data formatting | bytes 1048576 | tf_op jit(solution)/shard_map/mul | solution.py:340
  28.8 1.4 %and_convert_fusion.after_ref = bf16[512,512]{1,0:T(8,128)(2,1)} fusion(s32[512]{0:T(512)S(1)} %get-tuple-element.26, s32[512]{0:T(512)S(1)} %get-tuple-element.25, s32[512]{0:T(512)S(1)} %broadcast_add_fusion, pred[512]{0:T(512)(128)(4,1)S(1)} %get-tuple-element.27, pred[512]{0:T(512)(128)(4,1)S(1)} %broadcast_compare_fusion.2, ...), kind=kLoop, calls=%fused_computation.4 | loop fusion | flops 2359296 | bytes 532480 | tf_op jit(solution)/shard_map/convert_element_type | solution.py:334
  30.2 0.2 fusion.perm_ref
  30.5 3.0 %collective-permute-start.1 = (bf16[8,2048]{1,0:T(8,128)(2,1)S(1)}, bf16[8,2048]{1,0:T(8,128)(2,1)S(1)}, u32[]{:S(2)}, u32[]{:S(2)}) collective-permute-start(bf16[8,2048]{1,0:T(8,128)(2,1)S(1)} %dynamic-slice_bitcast_fusion), channel_id=1, source_target_pairs={{1,9},{3,11},{5,13},{7,15},{8,0},{9,17},{10,2},{11,19},{12,4},{13,... | collective-permute-start | bytes 98312 | tf_op jit(solution)/shard_map/ppermute | solution.py:311
  33.5 2.6 %collective-permute-start.2 = (bf16[8,2048]{1,0:T(8,128)(2,1)S(1)}, bf16[8,2048]{1,0:T(8,128)(2,1)S(1)}, u32[]{:S(2)}, u32[]{:S(2)}) collective-permute-start(bf16[8,2048]{1,0:T(8,128)(2,1)S(1)} %dynamic-slice_bitcast_fusion), channel_id=1, source_target_pairs={{1,8},{3,10},{5,12},{7,14},{8,1},{9,16},{10,3},{11,18},{12,5},{13,... | collective-permute-start | bytes 98312 | tf_op jit(solution)/shard_map/ppermute | solution.py:312
  36.1 1.7 %project.1.yo_ref = bf16[256,640]{1,0:T(8,128)(2,1)S(1)} custom-call(bf16[4,64,2048]{2,1,0:T(8,128)(2,1)S(1)} %all-to-all-done.x_ref, bf16[1,2048]{1,0:T(2,128)(2,1)S(1)} %reshape.317.gain_ref, bf16[2048,256]{1,0:T(8,128)(2,1)S(1)} %copy-done, bf16[2048,256]{1,0:T(8,128)(2,1)S(1)} %copy-done.1, bf16[2048,128]{1,0:T(8,128)(2,1)S(1)} %copy-done.2), custom_call_target="tpu_custom_call" | custom-call | flops 671088640 | bytes 4000000 | tf_op jit(solution)/shard_map/project/pallas_call | solution.py:353
  37.8 0.9 collective-permute-done.2.h2_ref
  38.7 0.2 broadcast_in_dim.56.extra_ref
  38.9 7.0 %gates.1 = (f32[4,512,256]{2,1,0:T(8,128)}, f32[512,256]{1,0:T(8,128)S(1)}, f32[640,128]{1,0:T(8,128)S(1)}, f32[4,8,256]{2,1,0:T(8,128)S(1)}, bf16[64,8,128]{2,1,0:T(8,128)(2,1)}) custom-call(bf16[4,64,2048]{2,1,0:T(8,128)(2,1)} %collective-permute-done.x_ref, bf16[8,2048]{1,0:T(8,128)(2,1)S(1)} %collective-permute-done.1.h1_ref, ...), custom_call_target="tpu_custom_call" | custom-call | flops 1426063360 | bytes 8000000 | tf_op jit(solution)/shard_map/gates/pallas_call | solution.py:364
  45.9 0.7 copy-done.11
  46.6 20.2 %all-to-all-start.1 = ((bf16[64,8,128]{2,1,0:T(8,128)(2,1)}), bf16[64,8,128]{2,1,0:T(8,128)(2,1)S(1)}, u32[]{:S(2)}, u32[]{:S(2)}) async-start(bf16[64,8,128]{2,1,0:T(8,128)(2,1)} %get-tuple-element.14), calls=%async_computation.1 | async-start | bytes 262144 | tf_op jit(solution)/shard_map/all_to_all | solution.py:390
  66.9 0.2 fusion.1.back_ref
  67.3 1.0 copy-done.10
  68.3 1.0 copy-done.12
  69.3 0.6 pooling.1
  69.9 0.8 copy-done.6
  70.7 11.8 %all-to-all-done.1.got_ref = bf16[64,8,128]{2,1,0:T(8,128)(2,1)S(1)} async-done(((bf16[64,8,128]{2,1,0:T(8,128)(2,1)}), bf16[64,8,128]{2,1,0:T(8,128)(2,1)S(1)}, u32[]{:S(2)}, u32[]{:S(2)}) %all-to-all-start.1) | async-done | bytes 131104 | tf_op jit(solution)/shard_map/all_to_all | solution.py:390
  82.6 1.0 copy-done.7
  83.6 1.4 %states.1 = (bf16[256,384]{1,0:T(8,128)(2,1)S(1)}, bf16[256,384]{1,0:T(8,128)(2,1)S(1)}) custom-call(bf16[64,8,128]{2,1,0:T(8,128)(2,1)S(1)} %all-to-all-done.1.got_ref, bf16[512,512]{1,0:T(8,128)(2,1)S(1)} %copy-done.5, f32[512,128]{1,0:T(8,128)S(1)} %broadcast_in_dim.58.valid_ref, f32[4,8,256]{2,1,0:T(8,128)S(1)} %get-tuple-element.15.seg_ref, ...), custom_call_target="tpu_custom_call" | custom-call | flops 1000000000 | bytes 4000000 | tf_op jit(solution)/shard_map/states/pallas_call | solution.py:409
  85.0 4.9 %collective-permute-start.3 = (bf16[256,384]{1,0:T(8,128)(2,1)S(1)}, bf16[256,384]{1,0:T(8,128)(2,1)S(1)}, u32[]{:S(2)}, u32[]{:S(2)}) collective-permute-start(bf16[256,384]{1,0:T(8,128)(2,1)S(1)} %get-tuple-element.22), channel_id=1, source_target_pairs={{0,1},{1,0},{2,3},{3,2},{4,5},{5,4},{6,7},{7,6},{8,9},{9,8},{10,11... | collective-permute-start | bytes 589832 | tf_op jit(solution)/shard_map/ppermute | solution.py:427
  89.9 1.0 collective-permute-done.3.got_ref
  91.0 3.1 %output.1 = bf16[4,64,2048]{2,1,0:T(8,128)(2,1)S(1)} custom-call(bf16[256,384]{1,0:T(8,128)(2,1)S(1)} %get-tuple-element.21.own_ref, bf16[256,384]{1,0:T(8,128)(2,1)S(1)} %collective-permute-done.3.got_ref, bf16[256,2048]{1,0:T(8,128)(2,1)} %wr_ref.1, bf16[128,2048]{1,0:T(8,128)(2,1)} %wp_ref.5, bf16[256,2048]{1,0:T(8,128)(2,1)} %collective-permute-done.4.vr_ref, ...), custom_call_target="tpu_custom_call" | custom-call | flops 805306368 | bytes 5000000 | tf_op jit(solution)/shard_map/output/pallas_call | solution.py:429
  94.1 17.2 %all_to_all.15 = bf16[4,64,2048]{2,1,0:T(8,128)(2,1)S(1)} all-to-all(bf16[4,64,2048]{2,1,0:T(8,128)(2,1)S(1)} %output.1), channel_id=1, replica_groups={{0,2,4,6},{1,3,5,7},{8,10,12,14},{9,11,13,15},{16,18,20,22},{17,19,21,2..., dimensions={0} | all-to-all | bytes 2097152 | tf_op jit(solution)/shard_map/all_to_all | solution.py:294
  111.3 0.9 reduce_sum.12
  (55 shorter events, 0.8 us)
Async XLA Ops:
  0.0 16.5 %copy-start.15 = (bf16[2,2,4,64,64]{4,3,2,1,0:T(8,128)(2,1)S(1)}, bf16[2,2,4,64,64]{4,3,2,1,0:T(8,128)(2,1)}, u32[]{:S(2)}) copy-start(bf16[2,2,4,64,64]{4,3,2,1,0:T(8,128)(2,1)} %param.20) | copy-start | bytes 393220
  2.1 23.3 %copy-start.16 = (bf16[2048]{0:T(1024)(128)(2,1)S(1)}, bf16[2048]{0:T(1024)(128)(2,1)}, u32[]{:S(2)}) copy-start(bf16[2048]{0:T(1024)(128)(2,1)} %param.15) | copy-start | bytes 12292
  2.1 17.1 %all-to-all-start = ((bf16[4,64,2048]{2,1,0:T(8,128)(2,1)}), bf16[4,64,2048]{2,1,0:T(8,128)(2,1)S(1)}, u32[]{:S(2)}, u32[]{:S(2)}) async-start(bf16[4,64,2048]{2,1,0:T(8,128)(2,1)} %broadcast_in_dim.32), calls=%async_computation | async-start | bytes 2097152 | tf_op jit(solution)/shard_map/all_to_all | solution.py:294
  7.1 82.9 %collective-permute-start.4 = (bf16[256,2048]{1,0:T(8,128)(2,1)}, bf16[256,2048]{1,0:T(8,128)(2,1)}, u32[]{:S(2)}, u32[]{:S(2)}) collective-permute-start(bf16[256,2048]{1,0:T(8,128)(2,1)} %wr_ref.1), channel_id=1, source_target_pairs={{0,1},{1,0},{2,3},{3,2},{4,5},{5,4},{6,7},{7,6},{8,9},{9,8},{10,11... | collective-permute-start | bytes 3145736 | tf_op jit(solution)/shard_map/ppermute | solution.py:314
  14.5 75.4 %collective-permute-start.5 = (bf16[128,2048]{1,0:T(8,128)(2,1)}, bf16[128,2048]{1,0:T(8,128)(2,1)}, u32[]{:S(2)}, u32[]{:S(2)}) collective-permute-start(bf16[128,2048]{1,0:T(8,128)(2,1)} %wp_ref.5), channel_id=1, source_target_pairs={{0,1},{1,0},{2,3},{3,2},{4,5},{5,4},{6,7},{7,6},{8,9},{9,8},{10,11... | collective-permute-start | bytes 1572872 | tf_op jit(solution)/shard_map/ppermute | solution.py:315
  16.5 12.0 %copy-start.17 = (f32[2,512]{1,0:T(2,128)S(1)}, f32[2,512]{1,0:T(2,128)}, u32[]{:S(2)}) copy-start(f32[2,512]{1,0:T(2,128)} %param.23) | copy-start | bytes 12292
  16.8 12.0 %copy-start.18 = (f32[2,256]{1,0:T(2,128)S(1)}, f32[2,256]{1,0:T(2,128)}, u32[]{:S(2)}) copy-start(f32[2,256]{1,0:T(2,128)} %param.21) | copy-start | bytes 6148
  19.2 16.9 %copy-start = (bf16[2048,256]{1,0:T(8,128)(2,1)S(1)}, bf16[2048,256]{1,0:T(8,128)(2,1)}, u32[]{:S(2)}) copy-start(bf16[2048,256]{1,0:T(8,128)(2,1)} %ws_ref.3) | copy-start | bytes 3145732
  19.2 16.9 %copy-start.1 = (bf16[2048,256]{1,0:T(8,128)(2,1)S(1)}, bf16[2048,256]{1,0:T(8,128)(2,1)}, u32[]{:S(2)}) copy-start(bf16[2048,256]{1,0:T(8,128)(2,1)} %wg_ref.3) | copy-start | bytes 3145732
  19.2 19.5 %collective-permute-start = (bf16[4,64,2048]{2,1,0:T(8,128)(2,1)S(1)}, bf16[4,64,2048]{2,1,0:T(8,128)(2,1)}, u32[]{:S(2)}, u32[]{:S(2)}) collective-permute-start(bf16[4,64,2048]{2,1,0:T(8,128)(2,1)S(1)} %all-to-all-done.x_ref), channel_id=1, source_target_pairs={{0,1},{1,0},{2,3},{3,2},{4,5},{5,4},{6,7},{7,6},{8,9},{9,8},{10,11... | collective-permute-start | bytes 3145736 | tf_op jit(solution)/shard_map/ppermute | solution.py:313
  28.8 7.3 %copy-start.2 = (bf16[2048,128]{1,0:T(8,128)(2,1)S(1)}, bf16[2048,128]{1,0:T(8,128)(2,1)}, u32[]{:S(2)}) copy-start(bf16[2048,128]{1,0:T(8,128)(2,1)} %wp_ref.4) | copy-start | bytes 1572868
  30.4 8.5 %copy-start.3 = (bf16[256,1024]{1,0:T(8,128)(2,1)S(1)}, bf16[256,1024]{1,0:T(8,128)(2,1)}, u32[]{:S(2)}) copy-start(bf16[256,1024]{1,0:T(8,128)(2,1)} %mul.90.bd_ref) | copy-start | bytes 1572868
  30.4 8.5 %copy-start.8 = (bf16[4,256]{1,0:T(4,128)(2,1)S(1)}, bf16[4,256]{1,0:T(4,128)(2,1)}, u32[]{:S(2)}) copy-start(bf16[4,256]{1,0:T(4,128)(2,1)} %conv_ref.1) | copy-start | bytes 6148
  30.5 7.3 %collective-permute-start.1 = (bf16[8,2048]{1,0:T(8,128)(2,1)S(1)}, bf16[8,2048]{1,0:T(8,128)(2,1)S(1)}, u32[]{:S(2)}, u32[]{:S(2)}) collective-permute-start(bf16[8,2048]{1,0:T(8,128)(2,1)S(1)} %dynamic-slice_bitcast_fusion), channel_id=1, source_target_pairs={{1,9},{3,11},{5,13},{7,15},{8,0},{9,17},{10,2},{11,19},{12,4},{13,... | collective-permute-start | bytes 98312 | tf_op jit(solution)/shard_map/ppermute | solution.py:311
  33.5 5.2 %collective-permute-start.2 = (bf16[8,2048]{1,0:T(8,128)(2,1)S(1)}, bf16[8,2048]{1,0:T(8,128)(2,1)S(1)}, u32[]{:S(2)}, u32[]{:S(2)}) collective-permute-start(bf16[8,2048]{1,0:T(8,128)(2,1)S(1)} %dynamic-slice_bitcast_fusion), channel_id=1, source_target_pairs={{1,8},{3,10},{5,12},{7,14},{8,1},{9,16},{10,3},{11,18},{12,5},{13,... | collective-permute-start | bytes 98312 | tf_op jit(solution)/shard_map/ppermute | solution.py:312
  38.9 28.3 %copy-start.13 = (bf16[1,128,128]{2,1,0:T(8,128)(2,1)S(1)}, bf16[1,128,128]{2,1,0:T(8,128)(2,1)}, u32[]{:S(2)}) copy-start(bf16[1,128,128]{2,1,0:T(8,128)(2,1)} %param.24) | copy-start | bytes 98308
  38.9 28.3 %copy-start.14 = (bf16[128]{0:T(256)(128)(2,1)S(1)}, bf16[128]{0:T(256)(128)(2,1)}, u32[]{:S(2)}) copy-start(bf16[128]{0:T(256)(128)(2,1)} %param.25) | copy-start | bytes 772
  45.9 0.7 copy-start.11
  46.6 20.6 %copy-start.9 = (f32[512,256]{1,0:T(8,128)}, f32[512,256]{1,0:T(8,128)S(1)}, u32[]{:S(2)}) copy-start(f32[512,256]{1,0:T(8,128)S(1)} %get-tuple-element.17.gate_ref) | copy-start | bytes 1572868
  46.6 35.8 %all-to-all-start.1 = ((bf16[64,8,128]{2,1,0:T(8,128)(2,1)}), bf16[64,8,128]{2,1,0:T(8,128)(2,1)S(1)}, u32[]{:S(2)}, u32[]{:S(2)}) async-start(bf16[64,8,128]{2,1,0:T(8,128)(2,1)} %get-tuple-element.14), calls=%async_computation.1 | async-start | bytes 262144 | tf_op jit(solution)/shard_map/all_to_all | solution.py:390
  67.2 1.0 copy-start.10
  68.3 1.0 copy-start.12
  69.3 13.3 %copy-start.4 = (f32[4,512,256]{2,1,0:T(8,128)S(1)}, f32[4,512,256]{2,1,0:T(8,128)}, u32[]{:S(2)}) copy-start(f32[4,512,256]{2,1,0:T(8,128)} %get-tuple-element.16.kd_ref) | copy-start | bytes 6291460
  69.3 13.3 %copy-start.5 = (bf16[512,512]{1,0:T(8,128)(2,1)S(1)}, bf16[512,512]{1,0:T(8,128)(2,1)}, u32[]{:S(2)}) copy-start(bf16[512,512]{1,0:T(8,128)(2,1)} %and_convert_fusion.after_ref) | copy-start | bytes 1572868
  69.8 0.8 copy-start.6
  82.6 1.0 copy-start.7
  85.0 6.0 %collective-permute-start.3 = (bf16[256,384]{1,0:T(8,128)(2,1)S(1)}, bf16[256,384]{1,0:T(8,128)(2,1)S(1)}, u32[]{:S(2)}, u32[]{:S(2)}) collective-permute-start(bf16[256,384]{1,0:T(8,128)(2,1)S(1)} %get-tuple-element.22), channel_id=1, source_target_pairs={{0,1},{1,0},{2,3},{3,2},{4,5},{5,4},{6,7},{7,6},{8,9},{9,8},{10,11... | collective-permute-start | bytes 589832 | tf_op jit(solution)/shard_map/ppermute | solution.py:427

commit v2 on v1

v2 whole, which is shorter than its diff:
```python
import jax
import jax.numpy as jnp
from jax import lax
from jax.experimental import pallas as pl
from jax.experimental.pallas import tpu as pltpu
from jax.sharding import PartitionSpec as P

FADING_FACTOR = 8.0
epsilon = 1e-06

SEG = 8
STEP = 64
ROWS = SEG * STEP
EDGE = 8
WIDE = 2048
CH = 256
PC = 128
F32 = jnp.float32
BF16 = jnp.bfloat16
VMEM = pltpu.VMEM
HBM = pltpu.HBM
DMA = pltpu.SemaphoreType.DMA
PITCH = STEP + 3 * EDGE


def vspecs(n):
    return [pl.BlockSpec(memory_space=VMEM)] * n


def hspecs(n):
    return [pl.BlockSpec(memory_space=HBM)] * n


def kept(*arrays):
    return [pltpu.with_memory_space_constraint(array, HBM) for array in arrays]


def params(mebibytes):
    return pltpu.CompilerParams(vmem_limit_bytes=mebibytes * 1024 * 1024)


def cost(flops, nbytes, trans=0):
    return pl.CostEstimate(flops=flops, bytes_accessed=nbytes, transcendentals=trans)


def dot(a, b):
    return jnp.dot(a, b, preferred_element_type=F32)


def normalize(read, write, gain_ref, rows):
    total = jnp.zeros((rows, 128), F32)
    for k in range(WIDE // 128):
        v = read(k * 128).astype(F32)
        total = total + v * v
    inv = lax.rsqrt(jnp.sum(total, axis=1, keepdims=True) * (1.0 / WIDE) + epsilon)
    for k in range(WIDE // 128):
        v = read(k * 128).astype(F32)
        gain = gain_ref[0:1, k * 128 : (k + 1) * 128].astype(F32)
        write(k * 128, ((v * inv) * gain).astype(BF16))


def normalize_shards(x_ref, gain_ref, out_ref):
    def one(i, _):
        base = pl.multiple_of(i * STEP, STEP)

        def read(lane):
            return x_ref[i, :, lane : lane + 128]

        def write(lane, v):
            out_ref[pl.ds(base, STEP), lane : lane + 128] = v

        normalize(read, write, gain_ref, STEP)
        return 0

    lax.fori_loop(0, 4, one, 0)


def spread_kernel(x_ref, out_ref, held_ref, in_sem, out_sem):
    load = pltpu.make_async_copy(x_ref, held_ref, in_sem)
    load.start()
    load.wait()
    copies = [pltpu.make_async_copy(held_ref, out_ref.at[k], out_sem.at[k]) for k in range(4)]
    for copy in copies:
        copy.start()
    for copy in copies:
        copy.wait()


def tables_kernel(maps_ref, extra_ref, bd_ref, spread_ref):
    bd_ref[...] = jnp.zeros_like(bd_ref)
    blank = jnp.zeros((64, 64), BF16)
    for d in range(2):
        for q in range(2):
            for b in range(4):
                block = maps_ref[d, q, b]
                tile = jnp.concatenate([block, blank] if b % 2 == 0 else [blank, block], axis=1)
                col = (d * 2 + q) * CH + (b // 2) * 128
                bd_ref[b * 64 : b * 64 + 64, col : col + 128] = tile
    for d in range(2):
        for j in range(STEP):
            spread_ref[d, j * SEG : (j + 1) * SEG, :] = jnp.broadcast_to(
                extra_ref[d, :, j : j + 1], (SEG, 128)
            )


def project_kernel(x_ref, gain_ref, ws_ref, wg_ref, wp_ref, y_ref, xn_ref):
    normalize_shards(x_ref, gain_ref, xn_ref)
    xn = xn_ref[...]
    y_ref[:, 0:256] = dot(xn, ws_ref[...]).astype(BF16)
    y_ref[:, 256:512] = dot(xn, wg_ref[...]).astype(BF16)
    y_ref[:, 512:640] = dot(xn, wp_ref[...]).astype(BF16)


def gates_kernel(
    at_ref, x_ref, h1_ref, h2_ref, yo_ref, gain_ref, ws_ref, wg_ref, wp_ref, conv_ref, bd_ref,
    half_rate_ref, extra_ref,
    kd_out, gate_out, pool_out, seg_out, send_ref,
    x_held, xn_ref, y_ref, f_ref, g_ref, kd_ref, gate_ref, pool_ref, seg_ref,
    x_sem, kd_sem, gate_sem, pool_sem, seg_sem,
):
    core = lax.rem(at_ref[1], 2)
    loads = [pltpu.make_async_copy(x_ref.at[x], x_held.at[x], x_sem.at[x]) for x in range(4)]
    for load in loads:
        load.start()
    for x in range(4):
        base = pl.multiple_of((2 * x + core) * PITCH + EDGE, 8)
        for k in range(5):
            tile = yo_ref[x * STEP : (x + 1) * STEP, k * 128 : (k + 1) * 128]
            y_ref[k, pl.ds(base, STEP), :] = tile.astype(F32)
    for n, ref in enumerate((h1_ref, h2_ref)):
        base = 256 + n * EDGE

        def read_edge(lane, ref=ref):
            return ref[:, lane : lane + 128]

        def write_edge(lane, v, base=base):
            xn_ref[base : base + EDGE, lane : lane + 128] = v

        normalize(read_edge, write_edge, gain_ref, EDGE)
    for x in range(4):
        loads[x].wait()

        def read(lane, x=x):
            return x_held[x, :, lane : lane + 128]

        def write(lane, v, x=x):
            xn_ref[x * STEP : (x + 1) * STEP, lane : lane + 128] = v

        normalize(read, write, gain_ref, STEP)
    xn = xn_ref[...]
    first = 0
    for w_ref in (ws_ref, wg_ref, wp_ref):
        value = dot(xn, w_ref[...]).astype(BF16).astype(F32)
        for n in range(w_ref.shape[1] // 128):
            k = first + n
            tile = value[:, n * 128 : (n + 1) * 128]
            for x in range(4):
                base = pl.multiple_of((2 * x + 1 - core) * PITCH + EDGE, 8)
                y_ref[k, pl.ds(base, STEP), :] = tile[x * STEP : (x + 1) * STEP]
            if k in (0, 1, 4):
                one, two = tile[256 : 256 + EDGE], tile[256 + EDGE : 256 + 2 * EDGE]
                y_ref[k, 0:EDGE, :] = jnp.where(core == 1, one, two)
                end = (SEG - 1) * PITCH + EDGE + STEP
                y_ref[k, end : end + EDGE, :] = jnp.where(core == 1, two, one)
                for s in range(SEG - 1):
                    low, high = s * PITCH, (s + 1) * PITCH
                    y_ref[k, high : high + EDGE, :] = y_ref[k, low + STEP : low + STEP + EDGE, :]
                    y_ref[k, low + EDGE + STEP : low + 2 * EDGE + STEP, :] = y_ref[
                        k, high + EDGE : high + 2 * EDGE, :
                    ]
        first += w_ref.shape[1] // 128

    def at(k, j):
        return y_ref[k, pl.ds(j + EDGE, SEG, stride=PITCH), :]

    taps = conv_ref[...].astype(F32)

    def conv(i, _):
        rows = pl.ds(pl.multiple_of(i * 64, 64), 64)
        for lt in range(2):
            lanes = slice(lt * 128, lt * 128 + 128)
            near = [at(lt, i * 8 + j - 2) for j in range(11)]
            out = []
            for j in range(8):
                value = taps[0:1, lanes] * near[j]
                for k in range(1, 4):
                    value = value + taps[k : k + 1, lanes] * near[j + k]
                out.append(value)
            f_ref[rows, lanes] = jnp.concatenate(out, axis=0).astype(BF16)
            gate = [at(2 + lt, i * 8 + j) for j in range(8)]
            gate_ref[rows, lanes] = jnp.concatenate(gate, axis=0).astype(BF16)
        return 0

    lax.fori_loop(0, STEP // 8, conv, 0)
    gate_copy = pltpu.make_async_copy(gate_ref, gate_out, gate_sem)
    gate_copy.start()

    def pools(i, _):
        rows = pl.ds(pl.multiple_of(i * 64, 64), 64)
        tiles = [at(4, i * 8 + j - EDGE) for j in range(8)]
        pool_ref[rows, :] = jnp.concatenate(tiles, axis=0).astype(BF16)
        return 0

    lax.fori_loop(0, (STEP + 2 * EDGE) // 8, pools, 0)
    pool_copy = pltpu.make_async_copy(pool_ref, pool_out, pool_sem)
    pool_copy.start()
    f = f_ref[...]
    for k in range(4):
        g_ref[:, k * 256 : (k + 1) * 256] = dot(f, bd_ref[:, k * 256 : (k + 1) * 256])

    def chunk(i, carry):
        rows = pl.ds(pl.multiple_of(i * 64, 64), 64)
        out = []
        for lt in range(2):
            hf, lf, hb, pb, lb = carry[lt]
            lanes = slice(lt * 128, lt * 128 + 128)
            wide = f_ref[rows, lanes].astype(F32)
            for d in range(2):
                col = d * 512 + lt * 128
                half = half_rate_ref[d : d + 1, lanes]
                recall = jnp.tanh(0.5 * g_ref[rows, col : col + 128])
                inlet = 0.5 * jnp.tanh(0.5 * g_ref[rows, col + 256 : col + 384]) + 0.5
                log_keep = half * recall + half + extra_ref[d, rows, :]
                keep = jnp.exp(log_keep)
                gap = (1.0 + keep * keep) * jnp.tanh(-log_keep)
                drive = gap * lax.rsqrt(jnp.maximum(gap, 1e-37)) * (inlet * wide)
                kd_ref[2 * d, rows, lanes] = keep
                kd_ref[2 * d + 1, rows, lanes] = drive
                for j in range(8):
                    kj = keep[8 * j : 8 * j + 8]
                    uj = drive[8 * j : 8 * j + 8]
                    lj = log_keep[8 * j : 8 * j + 8]
                    if d == 0:
                        hf = kj * hf + uj
                        lf = lf + lj
                    else:
                        hb = hb + pb * uj
                        pb = pb * kj
                        lb = lb + lj
            out.append((hf, lf, hb, pb, lb))
        return tuple(out)

    zero = jnp.zeros((SEG, 128), F32)
    one = jnp.ones((SEG, 128), F32)
    totals = tuple((zero, zero, zero, one, zero) for _ in range(2))
    kd_copies = []
    for part in range(4):
        totals = lax.fori_loop(2 * part, 2 * part + 2, chunk, totals)
        rows = slice(part * 128, part * 128 + 128)
        copy = pltpu.make_async_copy(
            kd_ref.at[:, rows, :], kd_out.at[:, rows, :], kd_sem.at[part]
        )
        copy.start()
        kd_copies.append(copy)
    row = lax.broadcasted_iota(jnp.int32, (SEG, 128), 0)
    send = jnp.zeros((SEG, 128), F32)
    for lt in range(2):
        hf, lf, hb, _, lb = totals[lt]
        lanes = slice(lt * 128, lt * 128 + 128)
        for d, (log_total, state) in enumerate(((lf, hf), (lb, hb))):
            factor = jnp.exp(log_total)
            for shift in (1, 2, 4):
                move = shift if d == 0 else SEG - shift
                inside = (row >= shift) if d == 0 else (row < SEG - shift)
                earlier_factor = jnp.where(inside, pltpu.roll(factor, move, 0), 1.0)
                earlier_state = jnp.where(inside, pltpu.roll(state, move, 0), 0.0)
                state = factor * earlier_state + state
                factor = factor * earlier_factor
            move = 1 if d == 0 else SEG - 1
            inside = (row >= 1) if d == 0 else (row < SEG - 1)
            seg_ref[2 * d, :, lanes] = jnp.where(inside, pltpu.roll(factor, move, 0), 1.0)
            seg_ref[2 * d + 1, :, lanes] = jnp.where(inside, pltpu.roll(state, move, 0), 0.0)
            end = SEG - 1 if d == 0 else 0
            whole_log = jnp.sum(log_total, axis=0, keepdims=True)
            whole_state = jnp.sum(jnp.where(row == end, state, 0.0), axis=0, keepdims=True)
            send = jnp.where(row == 4 * d + lt, whole_log, send)
            send = jnp.where(row == 4 * d + 2 + lt, whole_state, send)
    seg_copy = pltpu.make_async_copy(seg_ref, seg_out, seg_sem)
    seg_copy.start()
    packed = send.astype(BF16)
    send_ref[...] = jnp.broadcast_to(packed[None], send_ref.shape)
    for copy in (gate_copy, pool_copy, seg_copy, *kd_copies):
        copy.wait()


def pooling_kernel(at_ref, pool_ref, cluster_ref, factor_ref, mix_ref, p_ref):
    place, column = at_ref[0], at_ref[1]
    total = at_ref[2]
    code = lax.rem(column, 4)

    def windows(i, _):
        base = pl.multiple_of(i * 64, 64)
        level = pool_ref[pl.ds(base, 64 + 2 * EDGE * SEG), :].astype(F32)
        centre = level[EDGE * SEG : EDGE * SEG + 64]
        chosen = jnp.zeros((64, PC), F32)
        for k in range(4):
            shift = SEG << k
            size = level.shape[0] - shift
            level = level[:size] + level[shift:]
            begin = (EDGE - (1 << k)) * SEG
            chosen = jnp.where(code == k, level[begin : begin + 64], chosen)
        row = base + lax.broadcasted_iota(jnp.int32, (64, PC), 0)
        position = place * ROWS + (row & 7) * STEP + (row >> 3)
        reach = jnp.left_shift(1, code)
        count = jnp.minimum(position + reach, total) - jnp.maximum(position - reach, 0)
        p_ref[pl.ds(base, 64), :] = (chosen / count.astype(F32) - centre).astype(BF16)
        return 0

    lax.fori_loop(0, ROWS // 64, windows, 0)
    grouped = dot(p_ref[...], cluster_ref[...])
    mix_ref[...] = (grouped * factor_ref[...].astype(F32)).astype(BF16)


def states_kernel(
    at_ref, got_ref, seg_ref, kd_ref, gate_ref, pool_mix_ref,
    send_ref, own_ref,
    hf_ref, hb_ref, mix_ref,
):
    place = at_ref[0]
    core = lax.rem(at_ref[1], 2)
    blocks = got_ref.shape[0]

    def arriving(i, carry):
        ahead, behind = carry
        for k in range(2):
            p = i * 2 + k
            v = got_ref[p].astype(F32)
            ahead = jnp.where(p < place, jnp.exp(pltpu.roll(v, 2, 0)) * ahead + v, ahead)
            p = blocks - 1 - p
            v = got_ref[p].astype(F32)
            behind = jnp.where(p > place, jnp.exp(pltpu.roll(v, 2, 0)) * behind + v, behind)
        return ahead, behind

    zero = jnp.zeros((SEG, 128), F32)
    carry = lax.fori_loop(0, blocks // 2, arriving, (zero, zero), unroll=min(8, blocks // 2))
    begin = []
    for lt in range(2):
        lanes = slice(lt * 128, lt * 128 + 128)
        for d in range(2):
            r = 4 * d + 2 + lt
            begin.append(
                seg_ref[2 * d, :, lanes] * carry[d][r : r + 1] + seg_ref[2 * d + 1, :, lanes]
            )

    def walk(i, carry):
        hf0, hb0, hf1, hb1 = carry
        for k in range(8):
            f = pl.ds(pl.multiple_of((i * 8 + k) * SEG, SEG), SEG)
            b = pl.ds(pl.multiple_of((STEP - 1 - i * 8 - k) * SEG, SEG), SEG)
            hf0 = kd_ref[0, f, 0:128] * hf0 + kd_ref[1, f, 0:128]
            hf1 = kd_ref[0, f, 128:256] * hf1 + kd_ref[1, f, 128:256]
            hb0 = kd_ref[2, b, 0:128] * hb0 + kd_ref[3, b, 0:128]
            hb1 = kd_ref[2, b, 128:256] * hb1 + kd_ref[3, b, 128:256]
            hf_ref[f, 0:128] = hf0
            hf_ref[f, 128:256] = hf1
            hb_ref[b, 0:128] = hb0
            hb_ref[b, 128:256] = hb1
        return hf0, hb0, hf1, hb1

    lax.fori_loop(0, STEP // 8, walk, tuple(begin))

    def mixing(i, _):
        rows = pl.ds(pl.multiple_of(i * 64, 64), 64)
        for lt in range(2):
            lanes = slice(lt * 128, lt * 128 + 128)
            v = gate_ref[rows, lanes].astype(F32)
            inner = 0.7978845608028654 * (v + 0.044715 * (v * v * v))
            act = v * (0.5 * (1.0 + jnp.tanh(inner)))
            mix_ref[lt, rows, :] = act * (hf_ref[rows, lanes] + hb_ref[rows, lanes])
        mix_ref[2, rows, :] = pool_mix_ref[rows, :].astype(F32)
        return 0

    lax.fori_loop(0, ROWS // 64, mixing, 0)
    for x in range(4):
        rows = slice(x * STEP, (x + 1) * STEP)
        for k in range(3):
            lanes = slice(k * 128, k * 128 + 128)
            there = mix_ref[k, pl.ds(2 * x + 1 - core, STEP, stride=SEG), :]
            send_ref[rows, lanes] = there.astype(BF16)
            here = mix_ref[k, pl.ds(2 * x + core, STEP, stride=SEG), :]
            own_ref[rows, lanes] = here.astype(BF16)


def output_kernel(
    own_ref, got_ref, wr_hbm, wp_hbm, vr_hbm, vp_hbm, out_ref, wr_ref, wp_ref, vr_ref, vp_ref, sem
):
    pairs = ((wr_hbm, wr_ref), (wp_hbm, wp_ref), (vr_hbm, vr_ref), (vp_hbm, vp_ref))
    copies = []
    for k in range(4):
        lanes = slice(k * 512, k * 512 + 512)
        copies.append(
            [
                pltpu.make_async_copy(source.at[:, lanes], target.at[:, lanes], sem.at[k, n])
                for n, (source, target) in enumerate(pairs)
            ]
        )
        for copy in copies[k]:
            copy.start()
    own_state = own_ref[:, 0:CH]
    own_pool = own_ref[:, CH : CH + PC]
    got_state = got_ref[:, 0:CH]
    got_pool = got_ref[:, CH : CH + PC]
    for k in range(4):
        lanes = slice(k * 512, k * 512 + 512)
        for copy in copies[k]:
            copy.wait()
        value = dot(own_state, wr_ref[:, lanes]) + dot(got_state, vr_ref[:, lanes])
        value = value + dot(own_pool, wp_ref[:, lanes]) + dot(got_pool, vp_ref[:, lanes])
        value = value.astype(BF16)
        for x in range(4):
            out_ref[x, :, lanes] = value[x * STEP : (x + 1) * STEP]


def local(
    incoming_activity,
    entry_standardize_factor,
    recursive_entry_matrix,
    final_switch_matrix,
    averaging_entry_matrix,
    percolumn_filter_coefficients,
    switch_tiled_matrices,
    prior_fading_odds,
    speed_factors,
    extra_fading_amounts,
    averaging_cluster_matrices,
    averaging_feature_factor,
    recursive_final_matrix,
    averaging_final_matrix,
):
    blocks = lax.axis_size("sp")
    place = lax.axis_index("sp")
    column = lax.axis_index("tp")
    core = column % 2
    same_core = [[0, 2, 4, 6], [1, 3, 5, 7]]
    sibling = [(k, k ^ 1) for k in range(8)]

    def exchange(v):
        return lax.all_to_all(
            v, "tp", split_axis=0, concat_axis=0, tiled=True, axis_index_groups=same_core
        )

    def edge_pairs(cross):
        pairs = []
        for sp in range(blocks):
            for tp in range(8):
                to = sp + 1 if tp % 2 else sp - 1
                if 0 <= to < blocks:
                    pairs.append((sp * 8 + tp, to * 8 + (tp ^ cross)))
        return pairs

    spread = pl.pallas_call(
        spread_kernel,
        out_shape=HBM((4, STEP, WIDE), BF16),
        in_specs=hspecs(1),
        out_specs=pl.BlockSpec(memory_space=HBM),
        scratch_shapes=[VMEM((STEP, WIDE), BF16), DMA, DMA((4,))],
        compiler_params=params(2),
        cost_estimate=cost(0, 1_300_000),
        name="spread",
    )(*kept(incoming_activity))
    spread, *later = lax.optimization_barrier(
        (spread, switch_tiled_matrices, recursive_final_matrix, averaging_final_matrix)
    )
    x_own = exchange(spread)
    at = jnp.stack([place, column, jnp.asarray(blocks * ROWS)]).astype(jnp.int32)
    half_rate = (-0.5 * FADING_FACTOR) * speed_factors[:, :1] * jax.nn.softplus(-prior_fading_odds)
    gain = entry_standardize_factor.reshape(1, WIDE)
    smem = pl.BlockSpec(memory_space=pltpu.SMEM)
    maps, extra = pl.pallas_call(
        tables_kernel,
        out_shape=(
            HBM((CH, 4 * CH), BF16),
            HBM((2, ROWS, 128), F32),
        ),
        in_specs=vspecs(2),
        out_specs=tuple(vspecs(2)),
        compiler_params=params(4),
        cost_estimate=cost(1_000_000, 2_000_000),
        name="tables",
    )(later[0], extra_fading_amounts.reshape(2, SEG, STEP))
    sibling_recursive = lax.ppermute(later[1], "tp", sibling)
    sibling_averaging = lax.ppermute(later[2], "tp", sibling)
    x_own, maps, extra, half_rate, gain, at, sibling_recursive, sibling_averaging = (
        lax.optimization_barrier(
            (x_own, maps, extra, half_rate, gain, at, sibling_recursive, sibling_averaging)
        )
    )
    edge = lax.dynamic_slice(
        x_own, (3 * core, (STEP - EDGE) * core, 0), (1, EDGE, WIDE)
    ).reshape(EDGE, WIDE)
    edge_same = lax.ppermute(edge, ("sp", "tp"), edge_pairs(0))
    edge_cross = lax.ppermute(edge, ("sp", "tp"), edge_pairs(1))
    x_sibling = lax.ppermute(x_own, "tp", sibling)
    entry_weights = (recursive_entry_matrix, final_switch_matrix, averaging_entry_matrix)

    y_own = pl.pallas_call(
        project_kernel,
        out_shape=jax.ShapeDtypeStruct((256, 640), BF16),
        in_specs=vspecs(5),
        out_specs=pl.BlockSpec(memory_space=VMEM),
        scratch_shapes=[VMEM((256, WIDE), BF16)],
        compiler_params=params(8),
        cost_estimate=cost(2 * 256 * WIDE * 640, 4_000_000),
        name="project",
    )(x_own, gain, *entry_weights)

    kd, gate, pool, seg, send = pl.pallas_call(
        gates_kernel,
        out_shape=(
            HBM((4, ROWS, CH), F32),
            HBM((ROWS, CH), BF16),
            HBM((ROWS + 2 * EDGE * SEG, PC), BF16),
            HBM((4, SEG, CH), F32),
            jax.ShapeDtypeStruct((blocks, SEG, 128), BF16),
        ),
        in_specs=[smem, *hspecs(1), *vspecs(11)],
        out_specs=(*hspecs(4), *vspecs(1)),
        scratch_shapes=[
            VMEM((4, STEP, WIDE), BF16),
            VMEM((272, WIDE), BF16),
            VMEM((5, SEG * PITCH, 128), F32),
            VMEM((ROWS, CH), BF16),
            VMEM((ROWS, 4 * CH), F32),
            VMEM((4, ROWS, CH), F32),
            VMEM((ROWS, CH), BF16),
            VMEM((ROWS + 2 * EDGE * SEG, PC), BF16),
            VMEM((4, SEG, CH), F32),
            DMA((4,)),
            DMA((4,)),
            DMA,
            DMA,
            DMA,
        ],
        compiler_params=params(20),
        cost_estimate=cost(4 * 272 * WIDE * 640, 8_000_000, 1_000_000),
        name="gates",
    )(
        at, *kept(x_sibling), edge_same, edge_cross, y_own, gain, *entry_weights,
        percolumn_filter_coefficients, maps, half_rate, extra,
    )

    got = lax.all_to_all(send, "sp", split_axis=0, concat_axis=0, tiled=True)

    pool_mix = pl.pallas_call(
        pooling_kernel,
        out_shape=jax.ShapeDtypeStruct((ROWS, PC), BF16),
        in_specs=[smem, *vspecs(3)],
        out_specs=pl.BlockSpec(memory_space=VMEM),
        scratch_shapes=[VMEM((ROWS, PC), BF16)],
        compiler_params=params(4),
        cost_estimate=cost(1_000_000_000, 2_000_000, 200_000),
        name="pooling",
    )(
        at, pool, averaging_cluster_matrices.reshape(PC, PC),
        averaging_feature_factor.reshape(1, PC),
    )

    mix_send, mix_own = pl.pallas_call(
        states_kernel,
        out_shape=(
            jax.ShapeDtypeStruct((256, CH + PC), BF16),
            jax.ShapeDtypeStruct((256, CH + PC), BF16),
        ),
        in_specs=[smem, *vspecs(5)],
        out_specs=tuple(vspecs(2)),
        scratch_shapes=[
            VMEM((ROWS, CH), F32),
            VMEM((ROWS, CH), F32),
            VMEM((3, ROWS, 128), F32),
        ],
        compiler_params=params(8),
        cost_estimate=cost(1_000_000_000, 4_000_000, 100_000),
        name="states",
    )(at, got, seg, kd, gate, pool_mix)

    mix_got = lax.ppermute(mix_send, "tp", sibling)

    partial = pl.pallas_call(
        output_kernel,
        out_shape=jax.ShapeDtypeStruct((4, STEP, WIDE), BF16),
        in_specs=[*vspecs(2), *hspecs(4)],
        out_specs=pl.BlockSpec(memory_space=VMEM),
        scratch_shapes=[
            VMEM((CH, WIDE), BF16),
            VMEM((PC, WIDE), BF16),
            VMEM((CH, WIDE), BF16),
            VMEM((PC, WIDE), BF16),
            DMA((4, 4)),
        ],
        compiler_params=params(10),
        cost_estimate=cost(4 * 256 * 384 * WIDE, 5_000_000),
        name="output",
    )(
        mix_own,
        mix_got,
        *kept(recursive_final_matrix, averaging_final_matrix, sibling_recursive, sibling_averaging),
    )
    moved = exchange(partial)
    return jnp.sum(moved.astype(F32), axis=0).astype(BF16)


def solution(mesh):
    in_specs = (
        P(("sp", "tp"), None),
        P(),
        P(None, "tp"),
        P(None, "tp"),
        P(None, "tp"),
        P(None, "tp"),
        P(None, None, "tp", None, None),
        P(None, "tp"),
        P(None, "sp"),
        P(None, "sp"),
        P("tp", None, None),
        P("tp"),
        P("tp", None),
        P("tp", None),
    )
    out_specs = P(("sp", "tp"), None)


    return jax.shard_map(local, mesh=mesh, in_specs=in_specs, out_specs=out_specs, check_vma=False)
```

time: 113 us -> 107 us (0.947)
  waiting for transfers between devices: 13.8 us -> 24.9 us
  starting transfers between devices: 51.2 us -> 42.1 us
  local copies, waits for them, and re-layouts: 10.8 us -> 2.11 us
  Pallas kernels: 13.6 us -> 17.6 us
  other arithmetic: 5.11 us -> 1.85 us
    all_to_all x1, waiting for transfers between devices: 0.01 us -> 10.9 us  [exchange(): lax.all_to_all(v, 'tp', split_axis=0, concat_axis=0, tiled=True, axis_ind...]
    all_to_all x1, starting transfers between devices: 20.2 us -> 16.2 us  [local(): got = lax.all_to_all(send, 'sp', split_axis=0, concat_axis=0, tiled=True)]
    pallas_call x2 -> x4, Pallas kernels: 7.54 us -> 11.4 us  [the longest x1 6.99 us: local(): pl.pallas_call(gates_kernel, out_shape=(HBM((4, ROWS, CH), F32), HBM((ROW...]
    ppermute x1, starting transfers between devices: 6.14 us -> 2.77 us  [local(): x_sibling = lax.ppermute(x_own, 'tp', sibling)]
    mul x1 -> x0, local copies, waits for them, and re-layouts: 3.05 us -> none  [local(): maps[:, :, :, :, None, :] * eye[:, None, None, None, :, None]]
    broadcast_in_dim x5 -> x0, local copies, waits for them, and re-layouts: 2.64 us -> none  [the longest x1 2.1 us: local(): jnp.broadcast_to(incoming_activity, (4, *incoming_activity.shape))]
    unnamed x38 -> x34, local copies, waits for them, and re-layouts: 4.62 us -> 2.01 us
    convert_element_type x5 -> x0, other arithmetic: 1.72 us -> none  [the longest x1 1.36 us: local(): after = (between & (r2 == r - 2) & (r % 4 >= 2)).astype(BF16)]
  transfers between devices with their start and end apart: 8 -> 8, of which waited for: 3 -> 3; matrix products, arithmetic and copies ran while one was open for 7% -> 1% of each run, Pallas kernels for 9% -> 4%
where the time goes in v2:
time: 107 us; the launch traced here: 106 us
  starting transfers between devices  42.1 us (39%)
  waiting for transfers between devices  24.9 us (23%)
  Pallas kernels  17.6 us (16%)
  blocking collectives  17.2 us (16%)
  local copies, waits for them, and re-layouts  2.11 us (2%)
  other arithmetic  1.85 us (2%)
    all_to_all x1, blocking collectives, exchange(): lax.all_to_all(v, 'tp', split_axis=0, concat_axis=0, tiled=True, axis_ind...  17.2 us
    all_to_all x1, starting transfers between devices, local(): got = lax.all_to_all(send, 'sp', split_axis=0, concat_axis=0, tiled=True)  16.2 us
    all_to_all x1, waiting for transfers between devices, local(): got = lax.all_to_all(send, 'sp', split_axis=0, concat_axis=0, tiled=True)  13 us
    all_to_all x1, waiting for transfers between devices, exchange(): lax.all_to_all(v, 'tp', split_axis=0, concat_axis=0, tiled=True, axis_ind...  10.9 us
    ppermute x1, starting transfers between devices, local(): sibling_recursive = lax.ppermute(later[1], 'tp', sibling)  8.73 us
    pallas_call x1, Pallas kernels, local(): pl.pallas_call(gates_kernel, out_shape=(HBM((4, ROWS, CH), F32), HBM((ROW...  6.99 us
    ppermute x1, starting transfers between devices, local(): mix_got = lax.ppermute(mix_send, 'tp', sibling)  5.72 us
    all_to_all x1, starting transfers between devices, exchange(): lax.all_to_all(v, 'tp', split_axis=0, concat_axis=0, tiled=True, axis_ind...  3.53 us
  transfers between devices with their start and end apart: 8, of which 3 were waited for; matrix products, arithmetic and copies ran while one was open for 1% of the time, Pallas kernels for 4%

profile of v2, /device:TPU:1, one launch (start us, length us, event | category | flops | bytes accessed | tf_op | source)
XLA Modules:
  0.0 106.2 jit_solution(3143569991958823105)
XLA Ops:
  0.0 2.1 %spread.1 = bf16[4,64,2048]{2,1,0:T(8,128)(2,1)} custom-call(bf16[64,2048]{1,0:T(8,128)(2,1)} %x_ref.1), custom_call_target="tpu_custom_call" | custom-call | bytes 1300000 | tf_op jit(solution)/shard_map/spread/pallas_call | solution.py:451
  2.2 8.7 %collective-permute-start = (bf16[256,2048]{1,0:T(8,128)(2,1)}, bf16[256,2048]{1,0:T(8,128)(2,1)}, u32[]{:S(2)}, u32[]{:S(2)}) collective-permute-start(bf16[256,2048]{1,0:T(8,128)(2,1)} %wr_hbm.1), channel_id=1, source_target_pairs={{0,1},{1,0},{2,3},{3,2},{4,5},{5,4},{6,7},{7,6},{8,9},{9,8},{10,11... | collective-permute-start | bytes 3145736 | tf_op jit(solution)/shard_map/ppermute | solution.py:481
  10.9 3.5 %all-to-all-start = ((bf16[4,64,2048]{2,1,0:T(8,128)(2,1)}), bf16[4,64,2048]{2,1,0:T(8,128)(2,1)S(1)}, u32[]{:S(2)}, u32[]{:S(2)}) async-start(bf16[4,64,2048]{2,1,0:T(8,128)(2,1)} %spread.1), calls=%async_computation | async-start | bytes 2097152 | tf_op jit(solution)/shard_map/all_to_all | solution.py:438
  14.5 1.9 %collective-permute-start.1 = (bf16[128,2048]{1,0:T(8,128)(2,1)}, bf16[128,2048]{1,0:T(8,128)(2,1)}, u32[]{:S(2)}, u32[]{:S(2)}) collective-permute-start(bf16[128,2048]{1,0:T(8,128)(2,1)} %wp_hbm.1), channel_id=1, source_target_pairs={{0,1},{1,0},{2,3},{3,2},{4,5},{5,4},{6,7},{7,6},{8,9},{9,8},{10,11... | collective-permute-start | bytes 1572872 | tf_op jit(solution)/shard_map/ppermute | solution.py:482
  16.4 0.1 reshape.15.extra_ref
  16.5 1.2 %tables.1 = (bf16[256,1024]{1,0:T(8,128)(2,1)}, f32[2,512,128]{2,1,0:T(8,128)}) custom-call(bf16[2,2,4,64,64]{4,3,2,1,0:T(8,128)(2,1)S(1)} %copy-done.4, f32[2,8,64]{2,1,0:T(8,128)S(1)} %reshape.15.extra_ref), custom_call_target="tpu_custom_call" | custom-call | flops 1000000 | bytes 2000000 | tf_op jit(solution)/shard_map/tables/pallas_call | solution.py:469
  17.8 0.1 pad_add_fusion.at_ref
  17.8 0.8 multiply_reduce_fusion
  18.6 0.1 fusion.half_rate_ref
  18.7 10.9 %all-to-all-done.x_ref = bf16[4,64,2048]{2,1,0:T(8,128)(2,1)S(1)} async-done(((bf16[4,64,2048]{2,1,0:T(8,128)(2,1)}), bf16[4,64,2048]{2,1,0:T(8,128)(2,1)S(1)}, u32[]{:S(2)}, u32[]{:S(2)}) %all-to-all-start) | async-done | bytes 1048608 | tf_op jit(solution)/shard_map/all_to_all | solution.py:438
  29.6 0.0 collective-permute-done.vr_hbm
  29.6 2.8 %collective-permute-start.2 = (bf16[4,64,2048]{2,1,0:T(8,128)(2,1)S(1)}, bf16[4,64,2048]{2,1,0:T(8,128)(2,1)}, u32[]{:S(2)}, u32[]{:S(2)}) collective-permute-start(bf16[4,64,2048]{2,1,0:T(8,128)(2,1)S(1)} %all-to-all-done.x_ref), channel_id=1, source_target_pairs={{0,1},{1,0},{2,3},{3,2},{4,5},{5,4},{6,7},{7,6},{8,9},{9,8},{10,11... | collective-permute-start | bytes 3145736 | tf_op jit(solution)/shard_map/ppermute | solution.py:493
  32.4 1.9 %collective-permute-start.4 = (bf16[8,2048]{1,0:T(8,128)(2,1)S(1)}, bf16[8,2048]{1,0:T(8,128)(2,1)S(1)}, u32[]{:S(2)}, u32[]{:S(2)}) collective-permute-start(bf16[8,2048]{1,0:T(8,128)(2,1)S(1)} %dynamic-slice_bitcast_fusion), channel_id=1, source_target_pairs={{1,8},{3,10},{5,12},{7,14},{8,1},{9,16},{10,3},{11,18},{12,5},{13,... | collective-permute-start | bytes 98312 | tf_op jit(solution)/shard_map/ppermute | solution.py:492
  34.4 1.3 %collective-permute-start.3 = (bf16[8,2048]{1,0:T(8,128)(2,1)S(1)}, bf16[8,2048]{1,0:T(8,128)(2,1)S(1)}, u32[]{:S(2)}, u32[]{:S(2)}) collective-permute-start(bf16[8,2048]{1,0:T(8,128)(2,1)S(1)} %dynamic-slice_bitcast_fusion), channel_id=1, source_target_pairs={{1,9},{3,11},{5,13},{7,15},{8,0},{9,17},{10,2},{11,19},{12,4},{13,... | collective-permute-start | bytes 98312 | tf_op jit(solution)/shard_map/ppermute | solution.py:491
  35.7 0.0 copy-start.2
  35.7 1.0 copy-done.2
  36.7 1.7 %project.1.yo_ref = bf16[256,640]{1,0:T(8,128)(2,1)S(1)} custom-call(bf16[4,64,2048]{2,1,0:T(8,128)(2,1)S(1)} %all-to-all-done.x_ref, bf16[1,2048]{1,0:T(2,128)(2,1)S(1)} %reshape.16.gain_ref, bf16[2048,256]{1,0:T(8,128)(2,1)S(1)} %copy-done, bf16[2048,256]{1,0:T(8,128)(2,1)S(1)} %copy-done.1, bf16[2048,128]{1,0:T(8,128)(2,1)S(1)} %copy-done.2), custom_call_target="tpu_custom_call" | custom-call | flops 671088640 | bytes 4000000 | tf_op jit(solution)/shard_map/project/pallas_call | solution.py:496
  38.4 0.0 copy-start.7
  38.4 0.0 copy-start.9
  38.4 0.0 collective-permute-done.3.h1_ref
  38.5 7.0 %gates.1 = (f32[4,512,256]{2,1,0:T(8,128)}, bf16[512,256]{1,0:T(8,128)(2,1)}, bf16[640,128]{1,0:T(8,128)(2,1)}, f32[4,8,256]{2,1,0:T(8,128)}, bf16[64,8,128]{2,1,0:T(8,128)(2,1)}) custom-call(s32[3]{0:T(128)S(1)} %pad_add_fusion.at_ref, bf16[4,64,2048]{2,1,0:T(8,128)(2,1)} %collective-permute-done.2.x_ref, ...), custom_call_target="tpu_custom_call" | custom-call | flops 1426063360 | bytes 8000000 | tf_op jit(solution)/shard_map/gates/pallas_call | solution.py:507
  45.5 0.0 copy-start.11
  45.5 16.2 %all-to-all-start.1 = ((bf16[64,8,128]{2,1,0:T(8,128)(2,1)}), bf16[64,8,128]{2,1,0:T(8,128)(2,1)S(1)}, u32[]{:S(2)}, u32[]{:S(2)}) async-start(bf16[64,8,128]{2,1,0:T(8,128)(2,1)} %get-tuple-element.38), calls=%async_computation.1 | async-start | bytes 262144 | tf_op jit(solution)/shard_map/all_to_all | solution.py:542
  61.8 0.9 copy-done.12
  62.7 1.1 %pooling.1.pool_mix_ref = bf16[512,128]{1,0:T(8,128)(2,1)S(1)} custom-call(s32[3]{0:T(128)S(1)} %pad_add_fusion.at_ref, bf16[640,128]{1,0:T(8,128)(2,1)S(1)} %copy-done.12, bf16[128,128]{1,0:T(8,128)(2,1)S(1)} %bitcast.6, bf16[1,128]{1,0:T(2,128)(2,1)S(1)} %bitcast.7), custom_call_target="tpu_custom_call" | custom-call | flops 1000000000 | bytes 2000000 | tf_op jit(solution)/shard_map/pooling/pallas_call | solution.py:544
  63.8 13.0 %all-to-all-done.1.got_ref = bf16[64,8,128]{2,1,0:T(8,128)(2,1)S(1)} async-done(((bf16[64,8,128]{2,1,0:T(8,128)(2,1)}), bf16[64,8,128]{2,1,0:T(8,128)(2,1)S(1)}, u32[]{:S(2)}, u32[]{:S(2)}) %all-to-all-start.1) | async-done | bytes 131104 | tf_op jit(solution)/shard_map/all_to_all | solution.py:542
  76.7 1.5 %states.1 = (bf16[256,384]{1,0:T(8,128)(2,1)S(1)}, bf16[256,384]{1,0:T(8,128)(2,1)S(1)}) custom-call(s32[3]{0:T(128)S(1)} %pad_add_fusion.at_ref, bf16[64,8,128]{2,1,0:T(8,128)(2,1)S(1)} %all-to-all-done.1.got_ref, f32[4,8,256]{2,1,0:T(8,128)S(1)} %copy-done.13, f32[4,512,256]{2,1,0:T(8,128)S(1)} %copy-done.10, bf16[512,256]{1,0:T(8,128)(2,1)S(1)} %copy-done.11, ...), custom_call_target="tpu_custom_call" | custom-call | flops 1000000000 | bytes 4000000 | tf_op jit(solution)/shard_map/states/pallas_call | solution.py:558
  78.2 5.7 %collective-permute-start.5 = (bf16[256,384]{1,0:T(8,128)(2,1)S(1)}, bf16[256,384]{1,0:T(8,128)(2,1)S(1)}, u32[]{:S(2)}, u32[]{:S(2)}) collective-permute-start(bf16[256,384]{1,0:T(8,128)(2,1)S(1)} %get-tuple-element.44), channel_id=1, source_target_pairs={{0,1},{1,0},{2,3},{3,2},{4,5},{5,4},{6,7},{7,6},{8,9},{9,8},{10,11... | collective-permute-start | bytes 589832 | tf_op jit(solution)/shard_map/ppermute | solution.py:576
  83.9 1.0 collective-permute-done.5.got_ref
  85.0 3.1 %output.1 = bf16[4,64,2048]{2,1,0:T(8,128)(2,1)S(1)} custom-call(bf16[256,384]{1,0:T(8,128)(2,1)S(1)} %get-tuple-element.43.own_ref, bf16[256,384]{1,0:T(8,128)(2,1)S(1)} %collective-permute-done.5.got_ref, bf16[256,2048]{1,0:T(8,128)(2,1)} %wr_hbm.1, bf16[128,2048]{1,0:T(8,128)(2,1)} %wp_hbm.1, bf16[256,2048]{1,0:T(8,128)(2,1)} %collective-permute-done.vr_hbm, ...), custom_call_target="tpu_custom_call" | custom-call | flops 805306368 | bytes 5000000 | tf_op jit(solution)/shard_map/output/pallas_call | solution.py:578
  88.0 17.2 %all_to_all.15 = bf16[4,64,2048]{2,1,0:T(8,128)(2,1)S(1)} all-to-all(bf16[4,64,2048]{2,1,0:T(8,128)(2,1)S(1)} %output.1), channel_id=1, replica_groups={{0,2,4,6},{1,3,5,7},{8,10,12,14},{9,11,13,15},{16,18,20,22},{17,19,21,2..., dimensions={0} | all-to-all | bytes 2097152 | tf_op jit(solution)/shard_map/all_to_all | solution.py:438
  105.3 0.9 reduce_sum.12
  (33 shorter events, 0.1 us)
Async XLA Ops:
  0.0 16.5 %copy-start.4 = (bf16[2,2,4,64,64]{4,3,2,1,0:T(8,128)(2,1)S(1)}, bf16[2,2,4,64,64]{4,3,2,1,0:T(8,128)(2,1)}, u32[]{:S(2)}) copy-start(bf16[2,2,4,64,64]{4,3,2,1,0:T(8,128)(2,1)} %maps_ref) | copy-start | bytes 393220
  0.0 16.4 %copy-start.14 = (bf16[2048]{0:T(1024)(128)(2,1)S(1)}, bf16[2048]{0:T(1024)(128)(2,1)}, u32[]{:S(2)}) copy-start(bf16[2048]{0:T(1024)(128)(2,1)} %param.15) | copy-start | bytes 12292
  0.0 16.4 %copy-start.15 = (f32[2,512]{1,0:T(2,128)S(1)}, f32[2,512]{1,0:T(2,128)}, u32[]{:S(2)}) copy-start(f32[2,512]{1,0:T(2,128)} %param.23) | copy-start | bytes 12292
  0.0 18.6 %copy-start.16 = (f32[2,256]{1,0:T(2,128)S(1)}, f32[2,256]{1,0:T(2,128)}, u32[]{:S(2)}) copy-start(f32[2,256]{1,0:T(2,128)} %param.21) | copy-start | bytes 6148
  0.0 35.6 %copy-start.1 = (bf16[2048,256]{1,0:T(8,128)(2,1)S(1)}, bf16[2048,256]{1,0:T(8,128)(2,1)}, u32[]{:S(2)}) copy-start(bf16[2048,256]{1,0:T(8,128)(2,1)} %wg_ref.3) | copy-start | bytes 3145732
  0.0 35.6 %copy-start = (bf16[2048,256]{1,0:T(8,128)(2,1)S(1)}, bf16[2048,256]{1,0:T(8,128)(2,1)}, u32[]{:S(2)}) copy-start(bf16[2048,256]{1,0:T(8,128)(2,1)} %ws_ref.3) | copy-start | bytes 3145732
  2.2 27.4 %collective-permute-start = (bf16[256,2048]{1,0:T(8,128)(2,1)}, bf16[256,2048]{1,0:T(8,128)(2,1)}, u32[]{:S(2)}, u32[]{:S(2)}) collective-permute-start(bf16[256,2048]{1,0:T(8,128)(2,1)} %wr_hbm.1), channel_id=1, source_target_pairs={{0,1},{1,0},{2,3},{3,2},{4,5},{5,4},{6,7},{7,6},{8,9},{9,8},{10,11... | collective-permute-start | bytes 3145736 | tf_op jit(solution)/shard_map/ppermute | solution.py:481
  10.9 18.7 %all-to-all-start = ((bf16[4,64,2048]{2,1,0:T(8,128)(2,1)}), bf16[4,64,2048]{2,1,0:T(8,128)(2,1)S(1)}, u32[]{:S(2)}, u32[]{:S(2)}) async-start(bf16[4,64,2048]{2,1,0:T(8,128)(2,1)} %spread.1), calls=%async_computation | async-start | bytes 2097152 | tf_op jit(solution)/shard_map/all_to_all | solution.py:438
  14.5 4.2 %collective-permute-start.1 = (bf16[128,2048]{1,0:T(8,128)(2,1)}, bf16[128,2048]{1,0:T(8,128)(2,1)}, u32[]{:S(2)}, u32[]{:S(2)}) collective-permute-start(bf16[128,2048]{1,0:T(8,128)(2,1)} %wp_hbm.1), channel_id=1, source_target_pairs={{0,1},{1,0},{2,3},{3,2},{4,5},{5,4},{6,7},{7,6},{8,9},{9,8},{10,11... | collective-permute-start | bytes 1572872 | tf_op jit(solution)/shard_map/ppermute | solution.py:482
  17.8 20.7 %copy-start.8 = (bf16[4,256]{1,0:T(4,128)(2,1)S(1)}, bf16[4,256]{1,0:T(4,128)(2,1)}, u32[]{:S(2)}) copy-start(bf16[4,256]{1,0:T(4,128)(2,1)} %conv_ref.1) | copy-start | bytes 6148
  29.6 8.8 %collective-permute-start.2 = (bf16[4,64,2048]{2,1,0:T(8,128)(2,1)S(1)}, bf16[4,64,2048]{2,1,0:T(8,128)(2,1)}, u32[]{:S(2)}, u32[]{:S(2)}) collective-permute-start(bf16[4,64,2048]{2,1,0:T(8,128)(2,1)S(1)} %all-to-all-done.x_ref), channel_id=1, source_target_pairs={{0,1},{1,0},{2,3},{3,2},{4,5},{5,4},{6,7},{7,6},{8,9},{9,8},{10,11... | collective-permute-start | bytes 3145736 | tf_op jit(solution)/shard_map/ppermute | solution.py:493
  32.4 6.0 %collective-permute-start.4 = (bf16[8,2048]{1,0:T(8,128)(2,1)S(1)}, bf16[8,2048]{1,0:T(8,128)(2,1)S(1)}, u32[]{:S(2)}, u32[]{:S(2)}) collective-permute-start(bf16[8,2048]{1,0:T(8,128)(2,1)S(1)} %dynamic-slice_bitcast_fusion), channel_id=1, source_target_pairs={{1,8},{3,10},{5,12},{7,14},{8,1},{9,16},{10,3},{11,18},{12,5},{13,... | collective-permute-start | bytes 98312 | tf_op jit(solution)/shard_map/ppermute | solution.py:492
  34.4 4.1 %collective-permute-start.3 = (bf16[8,2048]{1,0:T(8,128)(2,1)S(1)}, bf16[8,2048]{1,0:T(8,128)(2,1)S(1)}, u32[]{:S(2)}, u32[]{:S(2)}) collective-permute-start(bf16[8,2048]{1,0:T(8,128)(2,1)S(1)} %dynamic-slice_bitcast_fusion), channel_id=1, source_target_pairs={{1,9},{3,11},{5,13},{7,15},{8,0},{9,17},{10,2},{11,19},{12,4},{13,... | collective-permute-start | bytes 98312 | tf_op jit(solution)/shard_map/ppermute | solution.py:491
  35.7 1.0 copy-start.2
  36.7 1.7 %copy-start.3 = (bf16[2048,128]{1,0:T(8,128)(2,1)S(1)}, bf16[2048,128]{1,0:T(8,128)(2,1)}, u32[]{:S(2)}) copy-start(bf16[2048,128]{1,0:T(8,128)(2,1)} %wp_ref.3) | copy-start | bytes 1572868
  36.7 1.7 %copy-start.5 = (bf16[256,1024]{1,0:T(8,128)(2,1)S(1)}, bf16[256,1024]{1,0:T(8,128)(2,1)}, u32[]{:S(2)}) copy-start(bf16[256,1024]{1,0:T(8,128)(2,1)} %get-tuple-element.35.bd_ref) | copy-start | bytes 1572868
  36.7 1.8 %copy-start.6 = (f32[2,512,128]{2,1,0:T(8,128)S(1)}, f32[2,512,128]{2,1,0:T(8,128)}, u32[]{:S(2)}) copy-start(f32[2,512,128]{2,1,0:T(8,128)} %get-tuple-element.37.extra_ref) | copy-start | bytes 1572868
  38.4 23.3 %copy-start.7 = (bf16[1,128,128]{2,1,0:T(8,128)(2,1)S(1)}, bf16[1,128,128]{2,1,0:T(8,128)(2,1)}, u32[]{:S(2)}) copy-start(bf16[1,128,128]{2,1,0:T(8,128)(2,1)} %param.24) | copy-start | bytes 98308
  38.4 23.3 %copy-start.9 = (bf16[128]{0:T(256)(128)(2,1)S(1)}, bf16[128]{0:T(256)(128)(2,1)}, u32[]{:S(2)}) copy-start(bf16[128]{0:T(256)(128)(2,1)} %param.25) | copy-start | bytes 772
  45.5 31.2 %copy-start.10 = (f32[4,512,256]{2,1,0:T(8,128)S(1)}, f32[4,512,256]{2,1,0:T(8,128)}, u32[]{:S(2)}) copy-start(f32[4,512,256]{2,1,0:T(8,128)} %get-tuple-element.40.kd_ref) | copy-start | bytes 6291460
  45.5 31.2 %copy-start.11 = (bf16[512,256]{1,0:T(8,128)(2,1)S(1)}, bf16[512,256]{1,0:T(8,128)(2,1)}, u32[]{:S(2)}) copy-start(bf16[512,256]{1,0:T(8,128)(2,1)} %get-tuple-element.41.gate_ref) | copy-start | bytes 786436
  45.5 31.2 %all-to-all-start.1 = ((bf16[64,8,128]{2,1,0:T(8,128)(2,1)}), bf16[64,8,128]{2,1,0:T(8,128)(2,1)S(1)}, u32[]{:S(2)}, u32[]{:S(2)}) async-start(bf16[64,8,128]{2,1,0:T(8,128)(2,1)} %get-tuple-element.38), calls=%async_computation.1 | async-start | bytes 262144 | tf_op jit(solution)/shard_map/all_to_all | solution.py:542
  61.7 0.9 copy-start.12
  62.7 14.1 %copy-start.13 = (f32[4,8,256]{2,1,0:T(8,128)S(1)}, f32[4,8,256]{2,1,0:T(8,128)}, u32[]{:S(2)}) copy-start(f32[4,8,256]{2,1,0:T(8,128)} %get-tuple-element.39.seg_ref) | copy-start | bytes 98308
  78.2 6.8 %collective-permute-start.5 = (bf16[256,384]{1,0:T(8,128)(2,1)S(1)}, bf16[256,384]{1,0:T(8,128)(2,1)S(1)}, u32[]{:S(2)}, u32[]{:S(2)}) collective-permute-start(bf16[256,384]{1,0:T(8,128)(2,1)S(1)} %get-tuple-element.44), channel_id=1, source_target_pairs={{0,1},{1,0},{2,3},{3,2},{4,5},{5,4},{6,7},{7,6},{8,9},{9,8},{10,11... | collective-permute-start | bytes 589832 | tf_op jit(solution)/shard_map/ppermute | solution.py:576

commit v3 on v2

--- a/solution.py
+++ b/solution.py
@@ -59,31 +59,14 @@
         write(k * 128, ((v * inv) * gain).astype(BF16))
 
 
-def normalize_shards(x_ref, gain_ref, out_ref):
-    def one(i, _):
-        base = pl.multiple_of(i * STEP, STEP)
-
-        def read(lane):
-            return x_ref[i, :, lane : lane + 128]
-
-        def write(lane, v):
-            out_ref[pl.ds(base, STEP), lane : lane + 128] = v
-
-        normalize(read, write, gain_ref, STEP)
-        return 0
-
-    lax.fori_loop(0, 4, one, 0)
-
-
-def spread_kernel(x_ref, out_ref, held_ref, in_sem, out_sem):
-    load = pltpu.make_async_copy(x_ref, held_ref, in_sem)
-    load.start()
-    load.wait()
-    copies = [pltpu.make_async_copy(held_ref, out_ref.at[k], out_sem.at[k]) for k in range(4)]
-    for copy in copies:
-        copy.start()
-    for copy in copies:
-        copy.wait()
+def normalize_shard(x_ref, gain_ref, out_ref, base):
+    def read(lane):
+        return x_ref[:, lane : lane + 128]
+
+    def write(lane, v):
+        out_ref[base : base + x_ref.shape[0], lane : lane + 128] = v
+
+    normalize(read, write, gain_ref, x_ref.shape[0])
 
 
 def tables_kernel(maps_ref, extra_ref, bd_ref, spread_ref):
@@ -103,83 +86,76 @@
             )
 
 
-def project_kernel(x_ref, gain_ref, ws_ref, wg_ref, wp_ref, y_ref, xn_ref):
-    normalize_shards(x_ref, gain_ref, xn_ref)
-    xn = xn_ref[...]
-    y_ref[:, 0:256] = dot(xn, ws_ref[...]).astype(BF16)
-    y_ref[:, 256:512] = dot(xn, wg_ref[...]).astype(BF16)
-    y_ref[:, 512:640] = dot(xn, wp_ref[...]).astype(BF16)
+def placing(at_ref):
+    core = lax.rem(at_ref[1], 2)
+    chip = lax.div(at_ref[1], 2)
+
+    def place(y_ref, k, tile, edges):
+        for n in range(8):
+            parity = core if n < 4 else 1 - core
+            segment = 2 * lax.rem(chip + (0, 3, 1, 2)[n % 4], 4) + parity
+            rows = pl.ds(pl.multiple_of(segment * PITCH + EDGE, 8), STEP)
+            y_ref[k, rows, :] = tile[n * STEP : (n + 1) * STEP]
+        if edges:
+            one, two = tile[ROWS : ROWS + EDGE], tile[ROWS + EDGE : ROWS + 2 * EDGE]
+            y_ref[k, 0:EDGE, :] = jnp.where(core == 1, one, two)
+            end = (SEG - 1) * PITCH + EDGE + STEP
+            y_ref[k, end : end + EDGE, :] = jnp.where(core == 1, two, one)
+            for s in range(SEG - 1):
+                low, high = s * PITCH, (s + 1) * PITCH
+                y_ref[k, high : high + EDGE, :] = y_ref[k, low + STEP : low + STEP + EDGE, :]
+                y_ref[k, low + EDGE + STEP : low + 2 * EDGE + STEP, :] = y_ref[
+                    k, high + EDGE : high + 2 * EDGE, :
+                ]
+
+    def take(y_ref, k, j):
+        return y_ref[k, pl.ds(j + EDGE, SEG, stride=PITCH), :]
+
+    return place, take
 
 
 def gates_kernel(
-    at_ref, x_ref, h1_ref, h2_ref, yo_ref, gain_ref, ws_ref, wg_ref, wp_ref, conv_ref, bd_ref,
-    half_rate_ref, extra_ref,
-    kd_out, gate_out, pool_out, seg_out, send_ref,
-    x_held, xn_ref, y_ref, f_ref, g_ref, kd_ref, gate_ref, pool_ref, seg_ref,
-    x_sem, kd_sem, gate_sem, pool_sem, seg_sem,
+    at_ref, x_hbm, xb_ref, xc_ref, xd_ref, sa_ref, sb_ref, sc_ref, sd_ref, h1_ref, h2_ref, gain_ref,
+    rate_ref, ws_hbm, conv_hbm, bd_hbm, speed_hbm, extra_hbm,
+    kd_out, xn_out, seg_out, send_out,
+    x_ref, ws_ref, conv_ref, bd_ref, speed_ref, extra_ref,
+    xn_ref, y_ref, f_ref, g_ref, kd_ref, seg_ref, send_ref,
+    x_sem, ws_sem, table_sem, kd_sem, xn_sem, seg_sem, send_sem,
 ):
-    core = lax.rem(at_ref[1], 2)
-    loads = [pltpu.make_async_copy(x_ref.at[x], x_held.at[x], x_sem.at[x]) for x in range(4)]
-    for load in loads:
+    place, take = placing(at_ref)
+    x_load = pltpu.make_async_copy(x_hbm, x_ref, x_sem)
+    x_load.start()
+    ws_load = pltpu.make_async_copy(ws_hbm, ws_ref, ws_sem)
+    ws_load.start()
+    tables = ((conv_hbm, conv_ref), (bd_hbm, bd_ref), (speed_hbm, speed_ref), (extra_hbm, extra_ref))
+    table_loads = [
+        pltpu.make_async_copy(source, target, table_sem.at[n])
+        for n, (source, target) in enumerate(tables)
+    ]
+    for load in table_loads:
         load.start()
-    for x in range(4):
-        base = pl.multiple_of((2 * x + core) * PITCH + EDGE, 8)
-        for k in range(5):
-            tile = yo_ref[x * STEP : (x + 1) * STEP, k * 128 : (k + 1) * 128]
-            y_ref[k, pl.ds(base, STEP), :] = tile.astype(F32)
+    shards = (xb_ref, xc_ref, xd_ref, sa_ref, sb_ref, sc_ref, sd_ref)
+    for n, ref in enumerate(shards):
+        normalize_shard(ref, gain_ref, xn_ref, (n + 1) * STEP)
     for n, ref in enumerate((h1_ref, h2_ref)):
-        base = 256 + n * EDGE
-
-        def read_edge(lane, ref=ref):
-            return ref[:, lane : lane + 128]
-
-        def write_edge(lane, v, base=base):
-            xn_ref[base : base + EDGE, lane : lane + 128] = v
-
-        normalize(read_edge, write_edge, gain_ref, EDGE)
-    for x in range(4):
-        loads[x].wait()
-
-        def read(lane, x=x):
-            return x_held[x, :, lane : lane + 128]
-
-        def write(lane, v, x=x):
-            xn_ref[x * STEP : (x + 1) * STEP, lane : lane + 128] = v
-
-        normalize(read, write, gain_ref, STEP)
-    xn = xn_ref[...]
-    first = 0
-    for w_ref in (ws_ref, wg_ref, wp_ref):
-        value = dot(xn, w_ref[...]).astype(BF16).astype(F32)
-        for n in range(w_ref.shape[1] // 128):
-            k = first + n
-            tile = value[:, n * 128 : (n + 1) * 128]
-            for x in range(4):
-                base = pl.multiple_of((2 * x + 1 - core) * PITCH + EDGE, 8)
-                y_ref[k, pl.ds(base, STEP), :] = tile[x * STEP : (x + 1) * STEP]
-            if k in (0, 1, 4):
-                one, two = tile[256 : 256 + EDGE], tile[256 + EDGE : 256 + 2 * EDGE]
-                y_ref[k, 0:EDGE, :] = jnp.where(core == 1, one, two)
-                end = (SEG - 1) * PITCH + EDGE + STEP
-                y_ref[k, end : end + EDGE, :] = jnp.where(core == 1, two, one)
-                for s in range(SEG - 1):
-                    low, high = s * PITCH, (s + 1) * PITCH
-                    y_ref[k, high : high + EDGE, :] = y_ref[k, low + STEP : low + STEP + EDGE, :]
-                    y_ref[k, low + EDGE + STEP : low + 2 * EDGE + STEP, :] = y_ref[
-                        k, high + EDGE : high + 2 * EDGE, :
-                    ]
-        first += w_ref.shape[1] // 128
-
-    def at(k, j):
-        return y_ref[k, pl.ds(j + EDGE, SEG, stride=PITCH), :]
-
+        normalize_shard(ref, gain_ref, xn_ref, ROWS + n * EDGE)
+    x_load.wait()
+    normalize_shard(x_ref, gain_ref, xn_ref, 0)
+    xn_copy = pltpu.make_async_copy(xn_ref, xn_out, xn_sem)
+    xn_copy.start()
+    ws_load.wait()
+    value = dot(xn_ref[...], ws_ref[...]).astype(BF16).astype(F32)
+    for k in range(2):
+        place(y_ref, k, value[:, k * 128 : (k + 1) * 128], True)
+    for load in table_loads:
+        load.wait()
     taps = conv_ref[...].astype(F32)
 
     def conv(i, _):
         rows = pl.ds(pl.multiple_of(i * 64, 64), 64)
         for lt in range(2):
             lanes = slice(lt * 128, lt * 128 + 128)
-            near = [at(lt, i * 8 + j - 2) for j in range(11)]
+            near = [take(y_ref, lt, i * 8 + j - 2) for j in range(11)]
             out = []
             for j in range(8):
                 value = taps[0:1, lanes] * near[j]
@@ -187,23 +163,9 @@
                     value = value + taps[k : k + 1, lanes] * near[j + k]
                 out.append(value)
             f_ref[rows, lanes] = jnp.concatenate(out, axis=0).astype(BF16)
-            gate = [at(2 + lt, i * 8 + j) for j in range(8)]
-            gate_ref[rows, lanes] = jnp.concatenate(gate, axis=0).astype(BF16)
         return 0
 
     lax.fori_loop(0, STEP // 8, conv, 0)
-    gate_copy = pltpu.make_async_copy(gate_ref, gate_out, gate_sem)
-    gate_copy.start()
-
-    def pools(i, _):
-        rows = pl.ds(pl.multiple_of(i * 64, 64), 64)
-        tiles = [at(4, i * 8 + j - EDGE) for j in range(8)]
-        pool_ref[rows, :] = jnp.concatenate(tiles, axis=0).astype(BF16)
-        return 0
-
-    lax.fori_loop(0, (STEP + 2 * EDGE) // 8, pools, 0)
-    pool_copy = pltpu.make_async_copy(pool_ref, pool_out, pool_sem)
-    pool_copy.start()
     f = f_ref[...]
     for k in range(4):
         g_ref[:, k * 256 : (k + 1) * 256] = dot(f, bd_ref[:, k * 256 : (k + 1) * 256])
@@ -217,7 +179,7 @@
             wide = f_ref[rows, lanes].astype(F32)
             for d in range(2):
                 col = d * 512 + lt * 128
-                half = half_rate_ref[d : d + 1, lanes]
+                half = half_rate[d][:, lanes]
                 recall = jnp.tanh(0.5 * g_ref[rows, col : col + 128])
                 inlet = 0.5 * jnp.tanh(0.5 * g_ref[rows, col + 256 : col + 384]) + 0.5
                 log_keep = half * recall + half + extra_ref[d, rows, :]
@@ -240,6 +202,9 @@
             out.append((hf, lf, hb, pb, lb))
         return tuple(out)
 
+    half_rate = [
+        (-0.5 * FADING_FACTOR) * speed_ref[d : d + 1, 0:1] * rate_ref[d : d + 1, :] for d in range(2)
+    ]
     zero = jnp.zeros((SEG, 128), F32)
     one = jnp.ones((SEG, 128), F32)
     totals = tuple((zero, zero, zero, one, zero) for _ in range(2))
@@ -279,18 +244,56 @@
     seg_copy.start()
     packed = send.astype(BF16)
     send_ref[...] = jnp.broadcast_to(packed[None], send_ref.shape)
-    for copy in (gate_copy, pool_copy, seg_copy, *kd_copies):
+    send_copy = pltpu.make_async_copy(send_ref, send_out, send_sem)
+    send_copy.start()
+    for copy in (xn_copy, seg_copy, *kd_copies, send_copy):
         copy.wait()
 
 
-def pooling_kernel(at_ref, pool_ref, cluster_ref, factor_ref, mix_ref, p_ref):
-    place, column = at_ref[0], at_ref[1]
+def pooling_kernel(
+    at_ref, xn_hbm, wg_hbm, wp_hbm, cluster_ref, factor_ref,
+    gate_ref, mix_ref,
+    xn_ref, wg_ref, wp_ref, y_ref, pool_ref, p_ref, sem,
+):
+    loads = [
+        pltpu.make_async_copy(source, target, sem.at[n])
+        for n, (source, target) in enumerate(((xn_hbm, xn_ref), (wp_hbm, wp_ref), (wg_hbm, wg_ref)))
+    ]
+    for load in loads:
+        load.start()
+    place, take = placing(at_ref)
+    position_of, column = at_ref[0], at_ref[1]
     total = at_ref[2]
     code = lax.rem(column, 4)
+    loads[0].wait()
+    loads[1].wait()
+    xn = xn_ref[...]
+    place(y_ref, 2, dot(xn, wp_ref[...]).astype(BF16).astype(F32), True)
+    loads[2].wait()
+    value = dot(xn, wg_ref[...]).astype(BF16).astype(F32)
+    for k in range(2):
+        place(y_ref, k, value[:, k * 128 : (k + 1) * 128], False)
+
+    def gates(i, _):
+        rows = pl.ds(pl.multiple_of(i * 64, 64), 64)
+        for lt in range(2):
+            tiles = [take(y_ref, lt, i * 8 + j) for j in range(8)]
+            gate_ref[rows, lt * 128 : lt * 128 + 128] = jnp.concatenate(tiles, axis=0).astype(BF16)
+        return 0
+
+    lax.fori_loop(0, STEP // 8, gates, 0)
+
+    def pools(i, _):
+        rows = pl.ds(pl.multiple_of(i * 64, 64), 64)
+        tiles = [take(y_ref, 2, i * 8 + j - EDGE) for j in range(8)]
+        pool_ref[rows, :] = jnp.concatenate(tiles, axis=0)
+        return 0
+
+    lax.fori_loop(0, (STEP + 2 * EDGE) // 8, pools, 0)
 
     def windows(i, _):
         base = pl.multiple_of(i * 64, 64)
-        level = pool_ref[pl.ds(base, 64 + 2 * EDGE * SEG), :].astype(F32)
+        level = pool_ref[pl.ds(base, 64 + 2 * EDGE * SEG), :]
         centre = level[EDGE * SEG : EDGE * SEG + 64]
         chosen = jnp.zeros((64, PC), F32)
         for k in range(4):
@@ -300,7 +303,7 @@
             begin = (EDGE - (1 << k)) * SEG
             chosen = jnp.where(code == k, level[begin : begin + 64], chosen)
         row = base + lax.broadcasted_iota(jnp.int32, (64, PC), 0)
-        position = place * ROWS + (row & 7) * STEP + (row >> 3)
+        position = position_of * ROWS + (row & 7) * STEP + (row >> 3)
         reach = jnp.left_shift(1, code)
         count = jnp.minimum(position + reach, total) - jnp.maximum(position - reach, 0)
         p_ref[pl.ds(base, 64), :] = (chosen / count.astype(F32) - centre).astype(BF16)
@@ -448,23 +451,34 @@
                     pairs.append((sp * 8 + tp, to * 8 + (tp ^ cross)))
         return pairs
 
-    spread = pl.pallas_call(
-        spread_kernel,
-        out_shape=HBM((4, STEP, WIDE), BF16),
-        in_specs=hspecs(1),
-        out_specs=pl.BlockSpec(memory_space=HBM),
-        scratch_shapes=[VMEM((STEP, WIDE), BF16), DMA, DMA((4,))],
-        compiler_params=params(2),
-        cost_estimate=cost(0, 1_300_000),
-        name="spread",
-    )(*kept(incoming_activity))
-    spread, *later = lax.optimization_barrier(
-        (spread, switch_tiled_matrices, recursive_final_matrix, averaging_final_matrix)
-    )
-    x_own = exchange(spread)
+    def to_chip(v, offset):
+        return lax.ppermute(v, "tp", [(k, (k + 2 * offset) % 8) for k in range(8)])
+
+    def to_sibling(v):
+        return lax.ppermute(v, "tp", sibling)
+
+    x = incoming_activity
+    edge_row = (STEP - EDGE) * core
+    x_before = to_chip(x, 1)
+    x_after = to_chip(x, 3)
+    edge_own = lax.dynamic_slice(x, (edge_row, 0), (EDGE, WIDE))
+    edge_far = to_chip(edge_own, 2)
+    x_far = to_chip(x, 2)
+    x_sibling = [to_sibling(x)]
+    chip = column // 2
+    holder = jnp.where(core == 1, 3 - chip, (4 - chip) % 4)
+    edge = jnp.where(holder == 0, edge_own, edge_far)
+    edge = jnp.where(holder == 3, lax.dynamic_slice(x_before, (edge_row, 0), (EDGE, WIDE)), edge)
+    edge = jnp.where(holder == 1, lax.dynamic_slice(x_after, (edge_row, 0), (EDGE, WIDE)), edge)
+    edge_same = lax.ppermute(edge, ("sp", "tp"), edge_pairs(0))
+    edge_cross = lax.ppermute(edge, ("sp", "tp"), edge_pairs(1))
+    x_sibling.append(to_sibling(x_before))
+    x_sibling.append(to_sibling(x_after))
+    x_sibling.append(to_sibling(x_far))
+
     at = jnp.stack([place, column, jnp.asarray(blocks * ROWS)]).astype(jnp.int32)
-    half_rate = (-0.5 * FADING_FACTOR) * speed_factors[:, :1] * jax.nn.softplus(-prior_fading_odds)
     gain = entry_standardize_factor.reshape(1, WIDE)
+    rate = jax.nn.softplus(-prior_fading_odds)
     smem = pl.BlockSpec(memory_space=pltpu.SMEM)
     maps, extra = pl.pallas_call(
         tables_kernel,
@@ -477,54 +491,34 @@
         compiler_params=params(4),
         cost_estimate=cost(1_000_000, 2_000_000),
         name="tables",
-    )(later[0], extra_fading_amounts.reshape(2, SEG, STEP))
-    sibling_recursive = lax.ppermute(later[1], "tp", sibling)
-    sibling_averaging = lax.ppermute(later[2], "tp", sibling)
-    x_own, maps, extra, half_rate, gain, at, sibling_recursive, sibling_averaging = (
-        lax.optimization_barrier(
-            (x_own, maps, extra, half_rate, gain, at, sibling_recursive, sibling_averaging)
-        )
-    )
-    edge = lax.dynamic_slice(
-        x_own, (3 * core, (STEP - EDGE) * core, 0), (1, EDGE, WIDE)
-    ).reshape(EDGE, WIDE)
-    edge_same = lax.ppermute(edge, ("sp", "tp"), edge_pairs(0))
-    edge_cross = lax.ppermute(edge, ("sp", "tp"), edge_pairs(1))
-    x_sibling = lax.ppermute(x_own, "tp", sibling)
-    entry_weights = (recursive_entry_matrix, final_switch_matrix, averaging_entry_matrix)
-
-    y_own = pl.pallas_call(
-        project_kernel,
-        out_shape=jax.ShapeDtypeStruct((256, 640), BF16),
-        in_specs=vspecs(5),
-        out_specs=pl.BlockSpec(memory_space=VMEM),
-        scratch_shapes=[VMEM((256, WIDE), BF16)],
-        compiler_params=params(8),
-        cost_estimate=cost(2 * 256 * WIDE * 640, 4_000_000),
-        name="project",
-    )(x_own, gain, *entry_weights)
-
-    kd, gate, pool, seg, send = pl.pallas_call(
+    )(switch_tiled_matrices, extra_fading_amounts.reshape(2, SEG, STEP))
+
+    kd, xn, seg, send = pl.pallas_call(
         gates_kernel,
         out_shape=(
             HBM((4, ROWS, CH), F32),
-            HBM((ROWS, CH), BF16),
-            HBM((ROWS + 2 * EDGE * SEG, PC), BF16),
+            HBM((ROWS + 2 * EDGE, WIDE), BF16),
             HBM((4, SEG, CH), F32),
-            jax.ShapeDtypeStruct((blocks, SEG, 128), BF16),
+            HBM((blocks, SEG, 128), BF16),
         ),
-        in_specs=[smem, *hspecs(1), *vspecs(11)],
-        out_specs=(*hspecs(4), *vspecs(1)),
+        in_specs=[smem, *hspecs(1), *vspecs(11), *hspecs(5)],
+        out_specs=tuple(hspecs(4)),
         scratch_shapes=[
-            VMEM((4, STEP, WIDE), BF16),
-            VMEM((272, WIDE), BF16),
-            VMEM((5, SEG * PITCH, 128), F32),
+            VMEM((STEP, WIDE), BF16),
+            VMEM((WIDE, CH), BF16),
+            VMEM((4, CH), BF16),
+            VMEM((CH, 4 * CH), BF16),
+            VMEM((2, ROWS), F32),
+            VMEM((2, ROWS, 128), F32),
+            VMEM((ROWS + 2 * EDGE, WIDE), BF16),
+            VMEM((2, SEG * PITCH, 128), F32),
             VMEM((ROWS, CH), BF16),
             VMEM((ROWS, 4 * CH), F32),
             VMEM((4, ROWS, CH), F32),
-            VMEM((ROWS, CH), BF16),
-            VMEM((ROWS + 2 * EDGE * SEG, PC), BF16),
             VMEM((4, SEG, CH), F32),
+            VMEM((blocks, SEG, 128), BF16),
+            DMA,
+            DMA,
             DMA((4,)),
             DMA((4,)),
             DMA,
@@ -532,27 +526,41 @@
             DMA,
         ],
         compiler_params=params(20),
-        cost_estimate=cost(4 * 272 * WIDE * 640, 8_000_000, 1_000_000),
+        cost_estimate=cost(2 * 528 * WIDE * 256, 8_000_000, 1_000_000),
         name="gates",
     )(
-        at, *kept(x_sibling), edge_same, edge_cross, y_own, gain, *entry_weights,
-        percolumn_filter_coefficients, maps, half_rate, extra,
+        at, *kept(x), x_before, x_after, x_far, *x_sibling, edge_same, edge_cross, gain, rate,
+        *kept(recursive_entry_matrix, percolumn_filter_coefficients, maps, speed_factors, extra),
     )
 
+    send, *later = lax.optimization_barrier((send, recursive_final_matrix, averaging_final_matrix))
     got = lax.all_to_all(send, "sp", split_axis=0, concat_axis=0, tiled=True)
-
-    pool_mix = pl.pallas_call(
+    sibling_recursive = lax.ppermute(later[0], "tp", sibling)
+    sibling_averaging = lax.ppermute(later[1], "tp", sibling)
+
+    gate, pool_mix = pl.pallas_call(
         pooling_kernel,
-        out_shape=jax.ShapeDtypeStruct((ROWS, PC), BF16),
-        in_specs=[smem, *vspecs(3)],
-        out_specs=pl.BlockSpec(memory_space=VMEM),
-        scratch_shapes=[VMEM((ROWS, PC), BF16)],
-        compiler_params=params(4),
-        cost_estimate=cost(1_000_000_000, 2_000_000, 200_000),
+        out_shape=(
+            jax.ShapeDtypeStruct((ROWS, CH), BF16),
+            jax.ShapeDtypeStruct((ROWS, PC), BF16),
+        ),
+        in_specs=[smem, *hspecs(3), *vspecs(2)],
+        out_specs=tuple(vspecs(2)),
+        scratch_shapes=[
+            VMEM((ROWS + 2 * EDGE, WIDE), BF16),
+            VMEM((WIDE, CH), BF16),
+            VMEM((WIDE, PC), BF16),
+            VMEM((3, SEG * PITCH, 128), F32),
+            VMEM((ROWS + 2 * EDGE * SEG, PC), F32),
+            VMEM((ROWS, PC), BF16),
+            DMA((3,)),
+        ],
+        compiler_params=params(16),
+        cost_estimate=cost(2 * 528 * WIDE * 384, 6_000_000, 200_000),
         name="pooling",
     )(
-        at, pool, averaging_cluster_matrices.reshape(PC, PC),
-        averaging_feature_factor.reshape(1, PC),
+        at, *kept(xn, final_switch_matrix, averaging_entry_matrix),
+        averaging_cluster_matrices.reshape(PC, PC), averaging_feature_factor.reshape(1, PC),
     )
 
     mix_send, mix_own = pl.pallas_call(

time: 107 us -> 112 us (1.047)
  starting transfers between devices: 42.1 us -> 58 us
  waiting for transfers between devices: 24.9 us -> 9.05 us
  local copies, waits for them, and re-layouts: 2.11 us -> 5.81 us
    ppermute x3 -> x10, starting transfers between devices: 13.4 us -> 33.1 us  [the longest x4 16.1 us: to_sibling(): return lax.ppermute(v, 'tp', sibling)]
    all_to_all x1 -> x0, waiting for transfers between devices: 10.9 us -> none  [exchange(): lax.all_to_all(v, 'tp', split_axis=0, concat_axis=0, tiled=True, axis_ind...]
    all_to_all x1, waiting for transfers between devices: 13 us -> 7.98 us  [local(): got = lax.all_to_all(send, 'sp', split_axis=0, concat_axis=0, tiled=True)]
    all_to_all x1 -> x0, starting transfers between devices: 3.53 us -> none  [exchange(): lax.all_to_all(v, 'tp', split_axis=0, concat_axis=0, tiled=True, axis_ind...]
    unnamed x34 -> x16, local copies, waits for them, and re-layouts: 2.01 us -> 3.56 us
    select_n x0 -> x2, other arithmetic: none -> 1.48 us  [the longest x1 0.79 us: local(): jnp.where(holder == 1, lax.dynamic_slice(x_after, (edge_row, 0), (EDGE, W...]
    pallas_call x3 -> x1, Pallas kernels: 4.87 us -> 5.54 us  [local(): pl.pallas_call(pooling_kernel, out_shape=(jax.ShapeDtypeStruct((ROWS, CH)...]
  transfers between devices with their start and end apart: 8 -> 14, of which waited for: 3 -> 2; matrix products, arithmetic and copies ran while one was open for 1% -> 3% of each run, Pallas kernels for 4% -> 7%
where the time goes in v3:
time: 112 us; the launch traced here: 111 us
  starting transfers between devices  58 us (52%)
  blocking collectives  17.7 us (16%)
  Pallas kernels  17.4 us (16%)
  waiting for transfers between devices  9.05 us (8%)
  local copies, waits for them, and re-layouts  5.81 us (5%)
  other arithmetic  2.48 us (2%)
    all_to_all x1, blocking collectives, exchange(): lax.all_to_all(v, 'tp', split_axis=0, concat_axis=0, tiled=True, axis_ind...  17.7 us
    all_to_all x1, starting transfers between devices, local(): got = lax.all_to_all(send, 'sp', split_axis=0, concat_axis=0, tiled=True)  17 us
    ppermute x4, starting transfers between devices, to_sibling(): return lax.ppermute(v, 'tp', sibling)  16.1 us
    ppermute x4, starting transfers between devices, to_chip(): return lax.ppermute(v, 'tp', [(k, (k + 2 * offset) % 8) for k in range(8)])  12.1 us
    all_to_all x1, waiting for transfers between devices, local(): got = lax.all_to_all(send, 'sp', split_axis=0, concat_axis=0, tiled=True)  7.98 us
    pallas_call x1, Pallas kernels, local(): pl.pallas_call(gates_kernel, out_shape=(HBM((4, ROWS, CH), F32), HBM((ROW...  6.05 us
    pallas_call x1, Pallas kernels, local(): pl.pallas_call(pooling_kernel, out_shape=(jax.ShapeDtypeStruct((ROWS, CH)...  5.54 us
    ppermute x1, starting transfers between devices, local(): mix_got = lax.ppermute(mix_send, 'tp', sibling)  4.74 us
  transfers between devices with their start and end apart: 14, of which 2 were waited for; matrix products, arithmetic and copies ran while one was open for 3% of the time, Pallas kernels for 7%

profile of v3, /device:TPU:1, one launch (start us, length us, event | category | flops | bytes accessed | tf_op | source)
XLA Modules:
  0.0 110.8 jit_solution(3225448894413652234)
XLA Ops:
  0.0 8.7 %collective-permute-start.3 = (bf16[64,2048]{1,0:T(8,128)(2,1)}, bf16[64,2048]{1,0:T(8,128)(2,1)S(1)}, u32[]{:S(2)}, u32[]{:S(2)}) collective-permute-start(bf16[64,2048]{1,0:T(8,128)(2,1)} %x_hbm.1), channel_id=1, source_target_pairs={{0,1},{1,0},{2,3},{3,2},{4,5},{5,4},{6,7},{7,6},{8,9},{9,8},{10,11... | collective-permute-start | bytes 786440 | tf_op jit(solution)/shard_map/ppermute | solution.py:458
  8.7 1.9 %collective-permute-start.2 = (bf16[64,2048]{1,0:T(8,128)(2,1)}, bf16[64,2048]{1,0:T(8,128)(2,1)S(1)}, u32[]{:S(2)}, u32[]{:S(2)}) collective-permute-start(bf16[64,2048]{1,0:T(8,128)(2,1)} %x_hbm.1), channel_id=1, source_target_pairs={{0,4},{1,5},{2,6},{3,7},{4,0},{5,1},{6,2},{7,3},{8,12},{9,13},{10,... | collective-permute-start | bytes 786440 | tf_op jit(solution)/shard_map/ppermute | solution.py:455
  10.7 1.9 %collective-permute-start.1 = (bf16[64,2048]{1,0:T(8,128)(2,1)}, bf16[64,2048]{1,0:T(8,128)(2,1)S(1)}, u32[]{:S(2)}, u32[]{:S(2)}) collective-permute-start(bf16[64,2048]{1,0:T(8,128)(2,1)} %x_hbm.1), channel_id=1, source_target_pairs={{0,6},{1,7},{2,0},{3,1},{4,2},{5,3},{6,4},{7,5},{8,14},{9,15},{10,... | collective-permute-start | bytes 786440 | tf_op jit(solution)/shard_map/ppermute | solution.py:455
  12.6 3.4 %collective-permute-start = (bf16[64,2048]{1,0:T(8,128)(2,1)}, bf16[64,2048]{1,0:T(8,128)(2,1)S(1)}, u32[]{:S(2)}, u32[]{:S(2)}) collective-permute-start(bf16[64,2048]{1,0:T(8,128)(2,1)} %x_hbm.1), channel_id=1, source_target_pairs={{0,2},{1,3},{2,4},{3,5},{4,6},{5,7},{6,0},{7,1},{8,10},{9,11},{10,... | collective-permute-start | bytes 786440 | tf_op jit(solution)/shard_map/ppermute | solution.py:455
  16.0 0.8 constant_dynamic-slice_fusion
  16.8 4.9 %collective-permute-start.7 = (bf16[8,2048]{1,0:T(8,128)(2,1)S(1)}, bf16[8,2048]{1,0:T(8,128)(2,1)S(1)}, u32[]{:S(2)}, u32[]{:S(2)}) collective-permute-start(bf16[8,2048]{1,0:T(8,128)(2,1)S(1)} %constant_dynamic-slice_fusion), channel_id=1, source_target_pairs={{0,4},{1,5},{2,6},{3,7},{4,0},{5,1},{6,2},{7,3},{8,12},{9,13},{10,... | collective-permute-start | bytes 98312 | tf_op jit(solution)/shard_map/ppermute | solution.py:455
  21.7 0.7 compare_select_fusion.rate_ref
  22.4 3.0 %collective-permute-start.6 = (bf16[64,2048]{1,0:T(8,128)(2,1)S(1)}, bf16[64,2048]{1,0:T(8,128)(2,1)S(1)}, u32[]{:S(2)}, u32[]{:S(2)}) collective-permute-start(bf16[64,2048]{1,0:T(8,128)(2,1)S(1)} %collective-permute-done.2.xd_ref), channel_id=1, source_target_pairs={{0,1},{1,0},{2,3},{3,2},{4,5},{5,4},{6,7},{7,6},{8,9},{9,8},{10,11... | collective-permute-start | bytes 786440 | tf_op jit(solution)/shard_map/ppermute | solution.py:458
  25.5 1.9 %collective-permute-start.5 = (bf16[64,2048]{1,0:T(8,128)(2,1)S(1)}, bf16[64,2048]{1,0:T(8,128)(2,1)S(1)}, u32[]{:S(2)}, u32[]{:S(2)}) collective-permute-start(bf16[64,2048]{1,0:T(8,128)(2,1)S(1)} %collective-permute-done.1.xc_ref), channel_id=1, source_target_pairs={{0,1},{1,0},{2,3},{3,2},{4,5},{5,4},{6,7},{7,6},{8,9},{9,8},{10,11... | collective-permute-start | bytes 786440 | tf_op jit(solution)/shard_map/ppermute | solution.py:458
  27.4 2.4 %collective-permute-start.4 = (bf16[64,2048]{1,0:T(8,128)(2,1)S(1)}, bf16[64,2048]{1,0:T(8,128)(2,1)S(1)}, u32[]{:S(2)}, u32[]{:S(2)}) collective-permute-start(bf16[64,2048]{1,0:T(8,128)(2,1)S(1)} %collective-permute-done.xb_ref), channel_id=1, source_target_pairs={{0,1},{1,0},{2,3},{3,2},{4,5},{5,4},{6,7},{7,6},{8,9},{9,8},{10,11... | collective-permute-start | bytes 786440 | tf_op jit(solution)/shard_map/ppermute | solution.py:458
  29.8 0.8 select_select_fusion
  30.6 1.9 %collective-permute-start.9 = (bf16[8,2048]{1,0:T(8,128)(2,1)S(1)}, bf16[8,2048]{1,0:T(8,128)(2,1)S(1)}, u32[]{:S(2)}, u32[]{:S(2)}) collective-permute-start(bf16[8,2048]{1,0:T(8,128)(2,1)S(1)} %select_select_fusion), channel_id=1, source_target_pairs={{1,8},{3,10},{5,12},{7,14},{8,1},{9,16},{10,3},{11,18},{12,5},{13,... | collective-permute-start | bytes 98312 | tf_op jit(solution)/shard_map/ppermute | solution.py:474
  32.6 1.3 %collective-permute-start.8 = (bf16[8,2048]{1,0:T(8,128)(2,1)S(1)}, bf16[8,2048]{1,0:T(8,128)(2,1)S(1)}, u32[]{:S(2)}, u32[]{:S(2)}) collective-permute-start(bf16[8,2048]{1,0:T(8,128)(2,1)S(1)} %select_select_fusion), channel_id=1, source_target_pairs={{1,9},{3,11},{5,13},{7,15},{8,0},{9,17},{10,2},{11,19},{12,4},{13,... | collective-permute-start | bytes 98312 | tf_op jit(solution)/shard_map/ppermute | solution.py:473
  33.9 0.1 pad_add_fusion.at_ref
  33.9 0.7 reshape.12.gain_ref
  34.6 0.8 reshape.13.extra_ref
  35.4 0.9 copy-done
  36.3 1.3 %tables.1 = (bf16[256,1024]{1,0:T(8,128)(2,1)}, f32[2,512,128]{2,1,0:T(8,128)}) custom-call(bf16[2,2,4,64,64]{4,3,2,1,0:T(8,128)(2,1)S(1)} %copy-done, f32[2,8,64]{2,1,0:T(8,128)S(1)} %reshape.13.extra_ref), custom_call_target="tpu_custom_call" | custom-call | flops 1000000 | bytes 2000000 | tf_op jit(solution)/shard_map/tables/pallas_call | solution.py:483
  37.7 6.1 %gates.1 = (f32[4,512,256]{2,1,0:T(8,128)}, bf16[528,2048]{1,0:T(8,128)(2,1)}, f32[4,8,256]{2,1,0:T(8,128)}, bf16[64,8,128]{2,1,0:T(8,128)(2,1)}) custom-call(s32[3]{0:T(128)S(1)} %pad_add_fusion.at_ref, bf16[64,2048]{1,0:T(8,128)(2,1)} %x_hbm.1, bf16[64,2048]{1,0:T(8,128)(2,1)S(1)} %collective-permute-done.xb_ref, ...), custom_call_target="tpu_custom_call" | custom-call | flops 553648128 | bytes 8000000 | tf_op jit(solution)/shard_map/gates/pallas_call | solution.py:496
  43.8 2.7 %collective-permute-start.11 = (bf16[256,2048]{1,0:T(8,128)(2,1)S(1)}, bf16[256,2048]{1,0:T(8,128)(2,1)S(1)}, u32[]{:S(2)}, u32[]{:S(2)}) collective-permute-start(bf16[256,2048]{1,0:T(8,128)(2,1)S(1)} %copy-done.5), channel_id=1, source_target_pairs={{0,1},{1,0},{2,3},{3,2},{4,5},{5,4},{6,7},{7,6},{8,9},{9,8},{10,11... | collective-permute-start | bytes 3145736 | tf_op jit(solution)/shard_map/ppermute | solution.py:538
  46.5 17.0 %all-to-all-start = ((bf16[64,8,128]{2,1,0:T(8,128)(2,1)}), bf16[64,8,128]{2,1,0:T(8,128)(2,1)S(1)}, u32[]{:S(2)}, u32[]{:S(2)}) async-start(bf16[64,8,128]{2,1,0:T(8,128)(2,1)} %get-tuple-element.21), calls=%async_computation | async-start | bytes 262144 | tf_op jit(solution)/shard_map/all_to_all | solution.py:537
  63.5 2.2 %collective-permute-start.12 = (bf16[128,2048]{1,0:T(8,128)(2,1)S(1)}, bf16[128,2048]{1,0:T(8,128)(2,1)}, u32[]{:S(2)}, u32[]{:S(2)}) collective-permute-start(bf16[128,2048]{1,0:T(8,128)(2,1)S(1)} %copy-done.7), channel_id=1, source_target_pairs={{0,1},{1,0},{2,3},{3,2},{4,5},{5,4},{6,7},{7,6},{8,9},{9,8},{10,11... | collective-permute-start | bytes 1572872 | tf_op jit(solution)/shard_map/ppermute | solution.py:539
  65.8 5.5 %pooling.1 = (bf16[512,256]{1,0:T(8,128)(2,1)S(1)}, bf16[512,128]{1,0:T(8,128)(2,1)S(1)}) custom-call(s32[3]{0:T(128)S(1)} %pad_add_fusion.at_ref, bf16[528,2048]{1,0:T(8,128)(2,1)} %get-tuple-element.24.xn_hbm, bf16[2048,256]{1,0:T(8,128)(2,1)} %wg_hbm.1, bf16[2048,128]{1,0:T(8,128)(2,1)} %wp_hbm.2, bf16[128,128]{1,0:T(8,128)(2,1)S(1)} %bitcast.4, ...), custom_call_target="tpu_custom_call" | custom-call | flops 830472192 | bytes 6000000 | tf_op jit(solution)/shard_map/pooling/pallas_call | solution.py:541
  71.3 8.0 %all-to-all-done.got_ref = bf16[64,8,128]{2,1,0:T(8,128)(2,1)S(1)} async-done(((bf16[64,8,128]{2,1,0:T(8,128)(2,1)}), bf16[64,8,128]{2,1,0:T(8,128)(2,1)S(1)}, u32[]{:S(2)}, u32[]{:S(2)}) %all-to-all-start) | async-done | bytes 131104 | tf_op jit(solution)/shard_map/all_to_all | solution.py:537
  79.3 1.6 %copy-done.3 = f32[4,512,256]{2,1,0:T(8,128)S(1)} copy-done((f32[4,512,256]{2,1,0:T(8,128)S(1)}, f32[4,512,256]{2,1,0:T(8,128)}, u32[]{:S(2)}) %copy-start.3) | copy-done | bytes 2097176
  80.9 1.5 %states.1 = (bf16[256,384]{1,0:T(8,128)(2,1)S(1)}, bf16[256,384]{1,0:T(8,128)(2,1)S(1)}) custom-call(s32[3]{0:T(128)S(1)} %pad_add_fusion.at_ref, bf16[64,8,128]{2,1,0:T(8,128)(2,1)S(1)} %all-to-all-done.got_ref, f32[4,8,256]{2,1,0:T(8,128)S(1)} %copy-done.4, f32[4,512,256]{2,1,0:T(8,128)S(1)} %copy-done.3, bf16[512,256]{1,0:T(8,128)(2,1)S(1)} %get-tuple-element.25.gate_ref, ...), custom_call_target="tpu_custom_call" | custom-call | flops 1000000000 | bytes 4000000 | tf_op jit(solution)/shard_map/states/pallas_call | solution.py:566
  82.4 4.7 %collective-permute-start.10 = (bf16[256,384]{1,0:T(8,128)(2,1)S(1)}, bf16[256,384]{1,0:T(8,128)(2,1)S(1)}, u32[]{:S(2)}, u32[]{:S(2)}) collective-permute-start(bf16[256,384]{1,0:T(8,128)(2,1)S(1)} %get-tuple-element.28), channel_id=1, source_target_pairs={{0,1},{1,0},{2,3},{3,2},{4,5},{5,4},{6,7},{7,6},{8,9},{9,8},{10,11... | collective-permute-start | bytes 589832 | tf_op jit(solution)/shard_map/ppermute | solution.py:584
  87.1 1.0 collective-permute-done.10.got_ref
  88.2 1.0 copy-done.6
  89.1 3.1 %output.1 = bf16[4,64,2048]{2,1,0:T(8,128)(2,1)S(1)} custom-call(bf16[256,384]{1,0:T(8,128)(2,1)S(1)} %get-tuple-element.27.own_ref, bf16[256,384]{1,0:T(8,128)(2,1)S(1)} %collective-permute-done.10.got_ref, bf16[256,2048]{1,0:T(8,128)(2,1)} %wr_hbm.1, bf16[128,2048]{1,0:T(8,128)(2,1)} %wp_hbm.3, bf16[256,2048]{1,0:T(8,128)(2,1)} %copy-done.6, ...), custom_call_target="tpu_custom_call" | custom-call | flops 805306368 | bytes 5000000 | tf_op jit(solution)/shard_map/output/pallas_call | solution.py:586
  92.2 17.7 %all_to_all.10 = bf16[4,64,2048]{2,1,0:T(8,128)(2,1)S(1)} all-to-all(bf16[4,64,2048]{2,1,0:T(8,128)(2,1)S(1)} %output.1), channel_id=1, replica_groups={{0,2,4,6},{1,3,5,7},{8,10,12,14},{9,11,13,15},{16,18,20,22},{17,19,21,2..., dimensions={0} | all-to-all | bytes 2097152 | tf_op jit(solution)/shard_map/all_to_all | solution.py:441
  109.9 0.9 reduce_sum.12
  (25 shorter events, 0.1 us)
Async XLA Ops:
  0.0 32.6 %collective-permute-start.3 = (bf16[64,2048]{1,0:T(8,128)(2,1)}, bf16[64,2048]{1,0:T(8,128)(2,1)S(1)}, u32[]{:S(2)}, u32[]{:S(2)}) collective-permute-start(bf16[64,2048]{1,0:T(8,128)(2,1)} %x_hbm.1), channel_id=1, source_target_pairs={{0,1},{1,0},{2,3},{3,2},{4,5},{5,4},{6,7},{7,6},{8,9},{9,8},{10,11... | collective-permute-start | bytes 786440 | tf_op jit(solution)/shard_map/ppermute | solution.py:458
  8.7 13.7 %collective-permute-start.2 = (bf16[64,2048]{1,0:T(8,128)(2,1)}, bf16[64,2048]{1,0:T(8,128)(2,1)S(1)}, u32[]{:S(2)}, u32[]{:S(2)}) collective-permute-start(bf16[64,2048]{1,0:T(8,128)(2,1)} %x_hbm.1), channel_id=1, source_target_pairs={{0,4},{1,5},{2,6},{3,7},{4,0},{5,1},{6,2},{7,3},{8,12},{9,13},{10,... | collective-permute-start | bytes 786440 | tf_op jit(solution)/shard_map/ppermute | solution.py:455
  10.7 14.8 %collective-permute-start.1 = (bf16[64,2048]{1,0:T(8,128)(2,1)}, bf16[64,2048]{1,0:T(8,128)(2,1)S(1)}, u32[]{:S(2)}, u32[]{:S(2)}) collective-permute-start(bf16[64,2048]{1,0:T(8,128)(2,1)} %x_hbm.1), channel_id=1, source_target_pairs={{0,6},{1,7},{2,0},{3,1},{4,2},{5,3},{6,4},{7,5},{8,14},{9,15},{10,... | collective-permute-start | bytes 786440 | tf_op jit(solution)/shard_map/ppermute | solution.py:455
  12.6 14.8 %collective-permute-start = (bf16[64,2048]{1,0:T(8,128)(2,1)}, bf16[64,2048]{1,0:T(8,128)(2,1)S(1)}, u32[]{:S(2)}, u32[]{:S(2)}) collective-permute-start(bf16[64,2048]{1,0:T(8,128)(2,1)} %x_hbm.1), channel_id=1, source_target_pairs={{0,2},{1,3},{2,4},{3,5},{4,6},{5,7},{6,0},{7,1},{8,10},{9,11},{10,... | collective-permute-start | bytes 786440 | tf_op jit(solution)/shard_map/ppermute | solution.py:455
  16.8 13.0 %collective-permute-start.7 = (bf16[8,2048]{1,0:T(8,128)(2,1)S(1)}, bf16[8,2048]{1,0:T(8,128)(2,1)S(1)}, u32[]{:S(2)}, u32[]{:S(2)}) collective-permute-start(bf16[8,2048]{1,0:T(8,128)(2,1)S(1)} %constant_dynamic-slice_fusion), channel_id=1, source_target_pairs={{0,4},{1,5},{2,6},{3,7},{4,0},{5,1},{6,2},{7,3},{8,12},{9,13},{10,... | collective-permute-start | bytes 98312 | tf_op jit(solution)/shard_map/ppermute | solution.py:455
  22.4 15.2 %collective-permute-start.6 = (bf16[64,2048]{1,0:T(8,128)(2,1)S(1)}, bf16[64,2048]{1,0:T(8,128)(2,1)S(1)}, u32[]{:S(2)}, u32[]{:S(2)}) collective-permute-start(bf16[64,2048]{1,0:T(8,128)(2,1)S(1)} %collective-permute-done.2.xd_ref), channel_id=1, source_target_pairs={{0,1},{1,0},{2,3},{3,2},{4,5},{5,4},{6,7},{7,6},{8,9},{9,8},{10,11... | collective-permute-start | bytes 786440 | tf_op jit(solution)/shard_map/ppermute | solution.py:458
  25.5 12.2 %collective-permute-start.5 = (bf16[64,2048]{1,0:T(8,128)(2,1)S(1)}, bf16[64,2048]{1,0:T(8,128)(2,1)S(1)}, u32[]{:S(2)}, u32[]{:S(2)}) collective-permute-start(bf16[64,2048]{1,0:T(8,128)(2,1)S(1)} %collective-permute-done.1.xc_ref), channel_id=1, source_target_pairs={{0,1},{1,0},{2,3},{3,2},{4,5},{5,4},{6,7},{7,6},{8,9},{9,8},{10,11... | collective-permute-start | bytes 786440 | tf_op jit(solution)/shard_map/ppermute | solution.py:458
  27.4 10.3 %collective-permute-start.4 = (bf16[64,2048]{1,0:T(8,128)(2,1)S(1)}, bf16[64,2048]{1,0:T(8,128)(2,1)S(1)}, u32[]{:S(2)}, u32[]{:S(2)}) collective-permute-start(bf16[64,2048]{1,0:T(8,128)(2,1)S(1)} %collective-permute-done.xb_ref), channel_id=1, source_target_pairs={{0,1},{1,0},{2,3},{3,2},{4,5},{5,4},{6,7},{7,6},{8,9},{9,8},{10,11... | collective-permute-start | bytes 786440 | tf_op jit(solution)/shard_map/ppermute | solution.py:458
  30.6 7.0 %collective-permute-start.9 = (bf16[8,2048]{1,0:T(8,128)(2,1)S(1)}, bf16[8,2048]{1,0:T(8,128)(2,1)S(1)}, u32[]{:S(2)}, u32[]{:S(2)}) collective-permute-start(bf16[8,2048]{1,0:T(8,128)(2,1)S(1)} %select_select_fusion), channel_id=1, source_target_pairs={{1,8},{3,10},{5,12},{7,14},{8,1},{9,16},{10,3},{11,18},{12,5},{13,... | collective-permute-start | bytes 98312 | tf_op jit(solution)/shard_map/ppermute | solution.py:474
  32.6 5.1 %collective-permute-start.8 = (bf16[8,2048]{1,0:T(8,128)(2,1)S(1)}, bf16[8,2048]{1,0:T(8,128)(2,1)S(1)}, u32[]{:S(2)}, u32[]{:S(2)}) collective-permute-start(bf16[8,2048]{1,0:T(8,128)(2,1)S(1)} %select_select_fusion), channel_id=1, source_target_pairs={{1,9},{3,11},{5,13},{7,15},{8,0},{9,17},{10,2},{11,19},{12,4},{13,... | collective-permute-start | bytes 98312 | tf_op jit(solution)/shard_map/ppermute | solution.py:473
  35.4 0.9 copy-start
  37.6 6.2 %copy-start.5 = (bf16[256,2048]{1,0:T(8,128)(2,1)S(1)}, bf16[256,2048]{1,0:T(8,128)(2,1)}, u32[]{:S(2)}) copy-start(bf16[256,2048]{1,0:T(8,128)(2,1)} %wr_hbm.1) | copy-start | bytes 3145732
  37.7 25.8 %copy-start.7 = (bf16[128,2048]{1,0:T(8,128)(2,1)S(1)}, bf16[128,2048]{1,0:T(8,128)(2,1)}, u32[]{:S(2)}) copy-start(bf16[128,2048]{1,0:T(8,128)(2,1)} %wp_hbm.3) | copy-start | bytes 1572868
  37.7 28.1 %copy-start.1 = (bf16[1,128,128]{2,1,0:T(8,128)(2,1)S(1)}, bf16[1,128,128]{2,1,0:T(8,128)(2,1)}, u32[]{:S(2)}) copy-start(bf16[1,128,128]{2,1,0:T(8,128)(2,1)} %param.24) | copy-start | bytes 98308
  37.7 28.0 %copy-start.2 = (bf16[128]{0:T(256)(128)(2,1)S(1)}, bf16[128]{0:T(256)(128)(2,1)}, u32[]{:S(2)}) copy-start(bf16[128]{0:T(256)(128)(2,1)} %param.25) | copy-start | bytes 772
  43.8 35.5 %copy-start.4 = (f32[4,8,256]{2,1,0:T(8,128)S(1)}, f32[4,8,256]{2,1,0:T(8,128)}, u32[]{:S(2)}) copy-start(f32[4,8,256]{2,1,0:T(8,128)} %get-tuple-element.22.seg_ref) | copy-start | bytes 98308
  43.8 44.4 %collective-permute-start.11 = (bf16[256,2048]{1,0:T(8,128)(2,1)S(1)}, bf16[256,2048]{1,0:T(8,128)(2,1)S(1)}, u32[]{:S(2)}, u32[]{:S(2)}) collective-permute-start(bf16[256,2048]{1,0:T(8,128)(2,1)S(1)} %copy-done.5), channel_id=1, source_target_pairs={{0,1},{1,0},{2,3},{3,2},{4,5},{5,4},{6,7},{7,6},{8,9},{9,8},{10,11... | collective-permute-start | bytes 3145736 | tf_op jit(solution)/shard_map/ppermute | solution.py:538
  46.5 32.7 %all-to-all-start = ((bf16[64,8,128]{2,1,0:T(8,128)(2,1)}), bf16[64,8,128]{2,1,0:T(8,128)(2,1)S(1)}, u32[]{:S(2)}, u32[]{:S(2)}) async-start(bf16[64,8,128]{2,1,0:T(8,128)(2,1)} %get-tuple-element.21), calls=%async_computation | async-start | bytes 262144 | tf_op jit(solution)/shard_map/all_to_all | solution.py:537
  63.5 23.6 %collective-permute-start.12 = (bf16[128,2048]{1,0:T(8,128)(2,1)S(1)}, bf16[128,2048]{1,0:T(8,128)(2,1)}, u32[]{:S(2)}, u32[]{:S(2)}) collective-permute-start(bf16[128,2048]{1,0:T(8,128)(2,1)S(1)} %copy-done.7), channel_id=1, source_target_pairs={{0,1},{1,0},{2,3},{3,2},{4,5},{5,4},{6,7},{7,6},{8,9},{9,8},{10,11... | collective-permute-start | bytes 1572872 | tf_op jit(solution)/shard_map/ppermute | solution.py:539
  79.3 1.6 %copy-start.3 = (f32[4,512,256]{2,1,0:T(8,128)S(1)}, f32[4,512,256]{2,1,0:T(8,128)}, u32[]{:S(2)}) copy-start(f32[4,512,256]{2,1,0:T(8,128)} %get-tuple-element.23.kd_ref) | copy-start | bytes 6291460
  82.4 5.8 %collective-permute-start.10 = (bf16[256,384]{1,0:T(8,128)(2,1)S(1)}, bf16[256,384]{1,0:T(8,128)(2,1)S(1)}, u32[]{:S(2)}, u32[]{:S(2)}) collective-permute-start(bf16[256,384]{1,0:T(8,128)(2,1)S(1)} %get-tuple-element.28), channel_id=1, source_target_pairs={{0,1},{1,0},{2,3},{3,2},{4,5},{5,4},{6,7},{7,6},{8,9},{9,8},{10,11... | collective-permute-start | bytes 589832 | tf_op jit(solution)/shard_map/ppermute | solution.py:584
  88.2 1.0 copy-start.6

commit v4 on v3

--- a/solution.py
+++ b/solution.py
@@ -67,6 +67,17 @@
         out_ref[base : base + x_ref.shape[0], lane : lane + 128] = v
 
     normalize(read, write, gain_ref, x_ref.shape[0])
+
+
+def spread_kernel(x_ref, out_ref, held_ref, in_sem, out_sem):
+    load = pltpu.make_async_copy(x_ref, held_ref, in_sem)
+    load.start()
+    load.wait()
+    copies = [pltpu.make_async_copy(held_ref, out_ref.at[k], out_sem.at[k]) for k in range(4)]
+    for copy in copies:
+        copy.start()
+    for copy in copies:
+        copy.wait()
 
 
 def tables_kernel(maps_ref, extra_ref, bd_ref, spread_ref):
@@ -88,14 +99,12 @@
 
 def placing(at_ref):
     core = lax.rem(at_ref[1], 2)
-    chip = lax.div(at_ref[1], 2)
 
     def place(y_ref, k, tile, edges):
         for n in range(8):
             parity = core if n < 4 else 1 - core
-            segment = 2 * lax.rem(chip + (0, 3, 1, 2)[n % 4], 4) + parity
-            rows = pl.ds(pl.multiple_of(segment * PITCH + EDGE, 8), STEP)
-            y_ref[k, rows, :] = tile[n * STEP : (n + 1) * STEP]
+            base = pl.multiple_of((2 * (n % 4) + parity) * PITCH + EDGE, 8)
+            y_ref[k, pl.ds(base, STEP), :] = tile[n * STEP : (n + 1) * STEP]
         if edges:
             one, two = tile[ROWS : ROWS + EDGE], tile[ROWS + EDGE : ROWS + 2 * EDGE]
             y_ref[k, 0:EDGE, :] = jnp.where(core == 1, one, two)
@@ -115,16 +124,14 @@
 
 
 def gates_kernel(
-    at_ref, x_hbm, xb_ref, xc_ref, xd_ref, sa_ref, sb_ref, sc_ref, sd_ref, h1_ref, h2_ref, gain_ref,
+    at_ref, own_ref, other_ref, h1_ref, h2_ref, gain_ref,
     rate_ref, ws_hbm, conv_hbm, bd_hbm, speed_hbm, extra_hbm,
     kd_out, xn_out, seg_out, send_out,
-    x_ref, ws_ref, conv_ref, bd_ref, speed_ref, extra_ref,
+    ws_ref, conv_ref, bd_ref, speed_ref, extra_ref,
     xn_ref, y_ref, f_ref, g_ref, kd_ref, seg_ref, send_ref,
-    x_sem, ws_sem, table_sem, kd_sem, xn_sem, seg_sem, send_sem,
+    ws_sem, table_sem, kd_sem, xn_sem, seg_sem, send_sem,
 ):
     place, take = placing(at_ref)
-    x_load = pltpu.make_async_copy(x_hbm, x_ref, x_sem)
-    x_load.start()
     ws_load = pltpu.make_async_copy(ws_hbm, ws_ref, ws_sem)
     ws_load.start()
     tables = ((conv_hbm, conv_ref), (bd_hbm, bd_ref), (speed_hbm, speed_ref), (extra_hbm, extra_ref))
@@ -134,13 +141,12 @@
     ]
     for load in table_loads:
         load.start()
-    shards = (xb_ref, xc_ref, xd_ref, sa_ref, sb_ref, sc_ref, sd_ref)
-    for n, ref in enumerate(shards):
-        normalize_shard(ref, gain_ref, xn_ref, (n + 1) * STEP)
+    for n in range(4):
+        normalize_shard(own_ref.at[n], gain_ref, xn_ref, n * STEP)
     for n, ref in enumerate((h1_ref, h2_ref)):
         normalize_shard(ref, gain_ref, xn_ref, ROWS + n * EDGE)
-    x_load.wait()
-    normalize_shard(x_ref, gain_ref, xn_ref, 0)
+    for n in range(4):
+        normalize_shard(other_ref.at[n], gain_ref, xn_ref, (n + 4) * STEP)
     xn_copy = pltpu.make_async_copy(xn_ref, xn_out, xn_sem)
     xn_copy.start()
     ws_load.wait()
@@ -218,7 +224,7 @@
         copy.start()
         kd_copies.append(copy)
     row = lax.broadcasted_iota(jnp.int32, (SEG, 128), 0)
-    send = jnp.zeros((SEG, 128), F32)
+    sends = [jnp.zeros((SEG, 128), F32), jnp.zeros((SEG, 128), F32)]
     for lt in range(2):
         hf, lf, hb, _, lb = totals[lt]
         lanes = slice(lt * 128, lt * 128 + 128)
@@ -238,12 +244,15 @@
             end = SEG - 1 if d == 0 else 0
             whole_log = jnp.sum(log_total, axis=0, keepdims=True)
             whole_state = jnp.sum(jnp.where(row == end, state, 0.0), axis=0, keepdims=True)
-            send = jnp.where(row == 4 * d + lt, whole_log, send)
-            send = jnp.where(row == 4 * d + 2 + lt, whole_state, send)
+            sends[d] = jnp.where(row == lt, whole_log, sends[d])
+            sends[d] = jnp.where(row == 2 + lt, whole_state, sends[d])
     seg_copy = pltpu.make_async_copy(seg_ref, seg_out, seg_sem)
     seg_copy.start()
-    packed = send.astype(BF16)
-    send_ref[...] = jnp.broadcast_to(packed[None], send_ref.shape)
+    shape = (1, 4, 128)
+    forward, backward = (v[0:4].astype(BF16).reshape(shape) for v in sends)
+    place_of = at_ref[0]
+    for p in range(send_ref.shape[0]):
+        send_ref[p : p + 1] = jnp.where(p > place_of, forward, backward)
     send_copy = pltpu.make_async_copy(send_ref, send_out, send_sem)
     send_copy.start()
     for copy in (xn_copy, seg_copy, *kd_copies, send_copy):
@@ -315,10 +324,18 @@
 
 
 def states_kernel(
-    at_ref, got_ref, seg_ref, kd_ref, gate_ref, pool_mix_ref,
+    at_ref, got_ref, seg_ref, kd_hbm, gate_ref, pool_mix_ref,
     send_ref, own_ref,
-    hf_ref, hb_ref, mix_ref,
+    kd_ref, hf_ref, hb_ref, mix_ref, kd_sem,
 ):
+    loads = []
+    for part in range(4):
+        for n, at in enumerate((part, 3 - part)):
+            there = (slice(2 * n, 2 * n + 2), slice(at * 128, at * 128 + 128), slice(None))
+            loads.append(
+                pltpu.make_async_copy(kd_hbm.at[there], kd_ref.at[there], kd_sem.at[2 * part + n])
+            )
+            loads[-1].start()
     place = at_ref[0]
     core = lax.rem(at_ref[1], 2)
     blocks = got_ref.shape[0]
@@ -328,21 +345,20 @@
         for k in range(2):
             p = i * 2 + k
             v = got_ref[p].astype(F32)
-            ahead = jnp.where(p < place, jnp.exp(pltpu.roll(v, 2, 0)) * ahead + v, ahead)
+            ahead = jnp.where(p < place, jnp.exp(v[0:2]) * ahead + v[2:4], ahead)
             p = blocks - 1 - p
             v = got_ref[p].astype(F32)
-            behind = jnp.where(p > place, jnp.exp(pltpu.roll(v, 2, 0)) * behind + v, behind)
+            behind = jnp.where(p > place, jnp.exp(v[0:2]) * behind + v[2:4], behind)
         return ahead, behind
 
-    zero = jnp.zeros((SEG, 128), F32)
+    zero = jnp.zeros((2, 128), F32)
     carry = lax.fori_loop(0, blocks // 2, arriving, (zero, zero), unroll=min(8, blocks // 2))
     begin = []
     for lt in range(2):
         lanes = slice(lt * 128, lt * 128 + 128)
         for d in range(2):
-            r = 4 * d + 2 + lt
             begin.append(
-                seg_ref[2 * d, :, lanes] * carry[d][r : r + 1] + seg_ref[2 * d + 1, :, lanes]
+                seg_ref[2 * d, :, lanes] * carry[d][lt : lt + 1] + seg_ref[2 * d + 1, :, lanes]
             )
 
     def walk(i, carry):
@@ -360,7 +376,11 @@
             hb_ref[b, 128:256] = hb1
         return hf0, hb0, hf1, hb1
 
-    lax.fori_loop(0, STEP // 8, walk, tuple(begin))
+    states = tuple(begin)
+    for part in range(4):
+        loads[2 * part].wait()
+        loads[2 * part + 1].wait()
+        states = lax.fori_loop(2 * part, 2 * part + 2, walk, states)
 
     def mixing(i, _):
         rows = pl.ds(pl.multiple_of(i * 64, 64), 64)
@@ -451,35 +471,34 @@
                     pairs.append((sp * 8 + tp, to * 8 + (tp ^ cross)))
         return pairs
 
-    def to_chip(v, offset):
-        return lax.ppermute(v, "tp", [(k, (k + 2 * offset) % 8) for k in range(8)])
-
     def to_sibling(v):
         return lax.ppermute(v, "tp", sibling)
 
-    x = incoming_activity
-    edge_row = (STEP - EDGE) * core
-    x_before = to_chip(x, 1)
-    x_after = to_chip(x, 3)
-    edge_own = lax.dynamic_slice(x, (edge_row, 0), (EDGE, WIDE))
-    edge_far = to_chip(edge_own, 2)
-    x_far = to_chip(x, 2)
-    x_sibling = [to_sibling(x)]
-    chip = column // 2
-    holder = jnp.where(core == 1, 3 - chip, (4 - chip) % 4)
-    edge = jnp.where(holder == 0, edge_own, edge_far)
-    edge = jnp.where(holder == 3, lax.dynamic_slice(x_before, (edge_row, 0), (EDGE, WIDE)), edge)
-    edge = jnp.where(holder == 1, lax.dynamic_slice(x_after, (edge_row, 0), (EDGE, WIDE)), edge)
+    smem = pl.BlockSpec(memory_space=pltpu.SMEM)
+    at = jnp.stack([place, column, jnp.asarray(blocks * ROWS)]).astype(jnp.int32)
+    spread = pl.pallas_call(
+        spread_kernel,
+        out_shape=HBM((4, STEP, WIDE), BF16),
+        in_specs=hspecs(1),
+        out_specs=pl.BlockSpec(memory_space=HBM),
+        scratch_shapes=[VMEM((STEP, WIDE), BF16), DMA, DMA((4,))],
+        compiler_params=params(2),
+        cost_estimate=cost(0, 1_300_000),
+        name="spread",
+    )(*kept(incoming_activity))
+    x_own = exchange(spread)
+    sibling_recursive = lax.ppermute(recursive_final_matrix, "tp", sibling)
+    sibling_averaging = lax.ppermute(averaging_final_matrix, "tp", sibling)
+    x_other = to_sibling(x_own)
+    edge = lax.dynamic_slice(
+        x_own, (3 * core, (STEP - EDGE) * core, 0), (1, EDGE, WIDE)
+    ).reshape(EDGE, WIDE)
     edge_same = lax.ppermute(edge, ("sp", "tp"), edge_pairs(0))
     edge_cross = lax.ppermute(edge, ("sp", "tp"), edge_pairs(1))
-    x_sibling.append(to_sibling(x_before))
-    x_sibling.append(to_sibling(x_after))
-    x_sibling.append(to_sibling(x_far))
 
     at = jnp.stack([place, column, jnp.asarray(blocks * ROWS)]).astype(jnp.int32)
     gain = entry_standardize_factor.reshape(1, WIDE)
     rate = jax.nn.softplus(-prior_fading_odds)
-    smem = pl.BlockSpec(memory_space=pltpu.SMEM)
     maps, extra = pl.pallas_call(
         tables_kernel,
         out_shape=(
@@ -499,12 +518,11 @@
             HBM((4, ROWS, CH), F32),
             HBM((ROWS + 2 * EDGE, WIDE), BF16),
             HBM((4, SEG, CH), F32),
-            HBM((blocks, SEG, 128), BF16),
+            HBM((blocks, 4, 128), BF16),
         ),
-        in_specs=[smem, *hspecs(1), *vspecs(11), *hspecs(5)],
+        in_specs=[smem, *vspecs(6), *hspecs(5)],
         out_specs=tuple(hspecs(4)),
         scratch_shapes=[
-            VMEM((STEP, WIDE), BF16),
             VMEM((WIDE, CH), BF16),
             VMEM((4, CH), BF16),
             VMEM((CH, 4 * CH), BF16),
@@ -516,8 +534,7 @@
             VMEM((ROWS, 4 * CH), F32),
             VMEM((4, ROWS, CH), F32),
             VMEM((4, SEG, CH), F32),
-            VMEM((blocks, SEG, 128), BF16),
-            DMA,
+            VMEM((blocks, 4, 128), BF16),
             DMA,
             DMA((4,)),
             DMA((4,)),
@@ -529,14 +546,11 @@
         cost_estimate=cost(2 * 528 * WIDE * 256, 8_000_000, 1_000_000),
         name="gates",
     )(
-        at, *kept(x), x_before, x_after, x_far, *x_sibling, edge_same, edge_cross, gain, rate,
+        at, x_own, x_other, edge_same, edge_cross, gain, rate,
         *kept(recursive_entry_matrix, percolumn_filter_coefficients, maps, speed_factors, extra),
     )
 
-    send, *later = lax.optimization_barrier((send, recursive_final_matrix, averaging_final_matrix))
     got = lax.all_to_all(send, "sp", split_axis=0, concat_axis=0, tiled=True)
-    sibling_recursive = lax.ppermute(later[0], "tp", sibling)
-    sibling_averaging = lax.ppermute(later[1], "tp", sibling)
 
     gate, pool_mix = pl.pallas_call(
         pooling_kernel,
@@ -556,7 +570,7 @@
             DMA((3,)),
         ],
         compiler_params=params(16),
-        cost_estimate=cost(2 * 528 * WIDE * 384, 6_000_000, 200_000),
+        cost_estimate=cost(8 * 528 * WIDE * 384, 8_000_000, 200_000),
         name="pooling",
     )(
         at, *kept(xn, final_switch_matrix, averaging_entry_matrix),
@@ -569,17 +583,19 @@
             jax.ShapeDtypeStruct((256, CH + PC), BF16),
             jax.ShapeDtypeStruct((256, CH + PC), BF16),
         ),
-        in_specs=[smem, *vspecs(5)],
+        in_specs=[smem, *vspecs(2), *hspecs(1), *vspecs(2)],
         out_specs=tuple(vspecs(2)),
         scratch_shapes=[
+            VMEM((4, ROWS, CH), F32),
             VMEM((ROWS, CH), F32),
             VMEM((ROWS, CH), F32),
             VMEM((3, ROWS, 128), F32),
+            DMA((8,)),
         ],
         compiler_params=params(8),
         cost_estimate=cost(1_000_000_000, 4_000_000, 100_000),
         name="states",
-    )(at, got, seg, kd, gate, pool_mix)
+    )(at, got, seg, *kept(kd), gate, pool_mix)
 
     mix_got = lax.ppermute(mix_send, "tp", sibling)
 

time: 112 us -> 107 us (0.955)
  starting transfers between devices: 58 us -> 42.3 us
  blocking collectives: 17.7 us -> 31.8 us
  local copies, waits for them, and re-layouts: 5.81 us -> 0.13 us
  Pallas kernels: 17.4 us -> 20.3 us
  waiting for transfers between devices: 9.05 us -> 10.8 us
  other arithmetic: 2.48 us -> 1.01 us
    all_to_all x1 -> x2, blocking collectives: 17.7 us -> 31.8 us  [exchange(): lax.all_to_all(v, 'tp', split_axis=0, concat_axis=0, tiled=True, axis_ind...]
    ppermute x6 -> x2, starting transfers between devices: 17 us -> 4.33 us  [the longest x1 2.41 us: local(): sibling_averaging = lax.ppermute(averaging_final_matrix, 'tp', sibling)]
    ppermute x4 -> x1, starting transfers between devices: 16.1 us -> 8.52 us  [to_sibling(): return lax.ppermute(v, 'tp', sibling)]
    unnamed x16, local copies, waits for them, and re-layouts: 3.56 us -> 0.03 us
    all_to_all x1, starting transfers between devices: 17 us -> 20.3 us  [local(): got = lax.all_to_all(send, 'sp', split_axis=0, concat_axis=0, tiled=True)]
    pallas_call x0 -> x1, Pallas kernels: none -> 2.08 us  [local(): pl.pallas_call(spread_kernel, out_shape=HBM((4, STEP, WIDE), BF16), in_sp...]
    ppermute x1, starting transfers between devices: 1.29 us -> 2.88 us  [local(): edge_same = lax.ppermute(edge, ('sp', 'tp'), edge_pairs(0))]
    ppermute x1, waiting for transfers between devices: 0.01 us -> 1.2 us  [local(): edge_cross = lax.ppermute(edge, ('sp', 'tp'), edge_pairs(1))]
  transfers between devices with their start and end apart: 14 -> 7, of which waited for: 2 -> 3; matrix products, arithmetic and copies ran while one was open for 3% -> 0% of each run, Pallas kernels for 7% -> 14%
where the time goes in v4:
time: 107 us
  starting transfers between devices  42.3 us (40%)
  blocking collectives  31.8 us (30%)
  Pallas kernels  20.3 us (19%)
  waiting for transfers between devices  10.8 us (10%)
    all_to_all x2, blocking collectives, exchange(): lax.all_to_all(v, 'tp', split_axis=0, concat_axis=0, tiled=True, axis_ind...  31.8 us
    all_to_all x1, starting transfers between devices, local(): got = lax.all_to_all(send, 'sp', split_axis=0, concat_axis=0, tiled=True)  20.3 us
    all_to_all x1, waiting for transfers between devices, local(): got = lax.all_to_all(send, 'sp', split_axis=0, concat_axis=0, tiled=True)  8.58 us
    ppermute x1, starting transfers between devices, to_sibling(): return lax.ppermute(v, 'tp', sibling)  8.52 us
    pallas_call x1, Pallas kernels, local(): pl.pallas_call(gates_kernel, out_shape=(HBM((4, ROWS, CH), F32), HBM((ROW...  5.8 us
    pallas_call x1, Pallas kernels, local(): pl.pallas_call(pooling_kernel, out_shape=(jax.ShapeDtypeStruct((ROWS, CH)...  5.54 us
    ppermute x1, starting transfers between devices, local(): mix_got = lax.ppermute(mix_send, 'tp', sibling)  3.75 us
    pallas_call x1, Pallas kernels, local(): pl.pallas_call(output_kernel, out_shape=jax.ShapeDtypeStruct((4, STEP, WI...  3.05 us
  transfers between devices with their start and end apart: 7, of which 3 were waited for; matrix products, arithmetic and copies ran while one was open for 0% of the time, Pallas kernels for 14%

profile of v4, /device:TPU:1, one launch (start us, length us, event | category | flops | bytes accessed | tf_op | source)
XLA Modules:
  0.0 106.7 jit_solution(10821745069082155224)
XLA Ops:
  0.0 0.0 copy-start.6
  0.0 0.0 copy-start
  0.0 2.1 %spread.1 = bf16[4,64,2048]{2,1,0:T(8,128)(2,1)} custom-call(bf16[64,2048]{1,0:T(8,128)(2,1)} %x_ref.1), custom_call_target="tpu_custom_call" | custom-call | bytes 1300000 | tf_op jit(solution)/shard_map/spread/pallas_call | solution.py:479
  2.1 14.6 %all_to_all.15.own_ref = bf16[4,64,2048]{2,1,0:T(8,128)(2,1)S(1)} all-to-all(bf16[4,64,2048]{2,1,0:T(8,128)(2,1)} %spread.1), channel_id=1, replica_groups={{0,2,4,6},{1,3,5,7},{8,10,12,14},{9,11,13,15},{16,18,20,22},{17,19,21,2..., dimensions={0} | all-to-all | bytes 2097152 | tf_op jit(solution)/shard_map/all_to_all | solution.py:461
  16.7 8.5 %collective-permute-start = (bf16[4,64,2048]{2,1,0:T(8,128)(2,1)S(1)}, bf16[4,64,2048]{2,1,0:T(8,128)(2,1)S(1)}, u32[]{:S(2)}, u32[]{:S(2)}) collective-permute-start(bf16[4,64,2048]{2,1,0:T(8,128)(2,1)S(1)} %all_to_all.15.own_ref), channel_id=1, source_target_pairs={{0,1},{1,0},{2,3},{3,2},{4,5},{5,4},{6,7},{7,6},{8,9},{9,8},{10,11... | collective-permute-start | bytes 3145736 | tf_op jit(solution)/shard_map/ppermute | solution.py:475
  25.2 1.9 %collective-permute-start.4 = (bf16[256,2048]{1,0:T(8,128)(2,1)S(1)}, bf16[256,2048]{1,0:T(8,128)(2,1)}, u32[]{:S(2)}, u32[]{:S(2)}) collective-permute-start(bf16[256,2048]{1,0:T(8,128)(2,1)S(1)} %copy-done.4), channel_id=1, source_target_pairs={{0,1},{1,0},{2,3},{3,2},{4,5},{5,4},{6,7},{7,6},{8,9},{9,8},{10,11... | collective-permute-start | bytes 3145736 | tf_op jit(solution)/shard_map/ppermute | solution.py:490
  27.2 2.4 %collective-permute-start.5 = (bf16[128,2048]{1,0:T(8,128)(2,1)}, bf16[128,2048]{1,0:T(8,128)(2,1)}, u32[]{:S(2)}, u32[]{:S(2)}) collective-permute-start(bf16[128,2048]{1,0:T(8,128)(2,1)} %wp_hbm.3), channel_id=1, source_target_pairs={{0,1},{1,0},{2,3},{3,2},{4,5},{5,4},{6,7},{7,6},{8,9},{9,8},{10,11... | collective-permute-start | bytes 1572872 | tf_op jit(solution)/shard_map/ppermute | solution.py:491
  29.7 2.9 %collective-permute-start.1 = (bf16[8,2048]{1,0:T(8,128)(2,1)S(1)}, bf16[8,2048]{1,0:T(8,128)(2,1)S(1)}, u32[]{:S(2)}, u32[]{:S(2)}) collective-permute-start(bf16[8,2048]{1,0:T(8,128)(2,1)S(1)} %dynamic-slice_bitcast_fusion), channel_id=1, source_target_pairs={{1,9},{3,11},{5,13},{7,15},{8,0},{9,17},{10,2},{11,19},{12,4},{13,... | collective-permute-start | bytes 98312 | tf_op jit(solution)/shard_map/ppermute | solution.py:496
  32.6 2.6 %collective-permute-start.2 = (bf16[8,2048]{1,0:T(8,128)(2,1)S(1)}, bf16[8,2048]{1,0:T(8,128)(2,1)S(1)}, u32[]{:S(2)}, u32[]{:S(2)}) collective-permute-start(bf16[8,2048]{1,0:T(8,128)(2,1)S(1)} %dynamic-slice_bitcast_fusion), channel_id=1, source_target_pairs={{1,8},{3,10},{5,12},{7,14},{8,1},{9,16},{10,3},{11,18},{12,5},{13,... | collective-permute-start | bytes 98312 | tf_op jit(solution)/shard_map/ppermute | solution.py:497
  35.1 0.1 pad_add_fusion.at_ref
  35.2 0.0 copy-done.5
  35.2 0.1 reshape.17.extra_ref
  35.3 0.0 copy-done.6
  35.3 1.3 %tables.1 = (bf16[256,1024]{1,0:T(8,128)(2,1)}, f32[2,512,128]{2,1,0:T(8,128)}) custom-call(bf16[2,2,4,64,64]{4,3,2,1,0:T(8,128)(2,1)S(1)} %copy-done, f32[2,8,64]{2,1,0:T(8,128)S(1)} %reshape.17.extra_ref), custom_call_target="tpu_custom_call" | custom-call | flops 1000000 | bytes 2000000 | tf_op jit(solution)/shard_map/tables/pallas_call | solution.py:502
  36.6 0.0 collective-permute-done.1.h1_ref
  36.6 1.2 %collective-permute-done.2.h2_ref = bf16[8,2048]{1,0:T(8,128)(2,1)S(1)} collective-permute-done((bf16[8,2048]{1,0:T(8,128)(2,1)S(1)}, bf16[8,2048]{1,0:T(8,128)(2,1)S(1)}, u32[]{:S(2)}, u32[]{:S(2)}) %collective-permute-start.2) | collective-permute-done | bytes 32800 | tf_op jit(solution)/shard_map/ppermute | solution.py:497
  37.8 0.0 collective-permute-done.other_ref
  37.8 5.8 %gates.1 = (f32[4,512,256]{2,1,0:T(8,128)}, bf16[528,2048]{1,0:T(8,128)(2,1)}, f32[4,8,256]{2,1,0:T(8,128)}, bf16[64,4,128]{2,1,0:T(4,128)(2,1)}) custom-call(s32[3]{0:T(128)S(1)} %pad_add_fusion.at_ref, bf16[4,64,2048]{2,1,0:T(8,128)(2,1)S(1)} %all_to_all.15.own_ref, bf16[4,64,2048]{2,1,0:T(8,128)(2,1)S(1)} %collective-permute-done.other_ref, ...), custom_call_target="tpu_custom_call" | custom-call | flops 553648128 | bytes 8000000 | tf_op jit(solution)/shard_map/gates/pallas_call | solution.py:515
  43.6 20.3 %all-to-all-start.1 = ((bf16[64,4,128]{2,1,0:T(4,128)(2,1)}), bf16[64,4,128]{2,1,0:T(4,128)(2,1)S(1)}, u32[]{:S(2)}, u32[]{:S(2)}) async-start(bf16[64,4,128]{2,1,0:T(4,128)(2,1)} %get-tuple-element.17), calls=%async_computation.1 | async-start | bytes 131072 | tf_op jit(solution)/shard_map/all_to_all | solution.py:553
  63.9 0.0 copy-done.1
  63.9 0.0 copy-done.3
  63.9 0.0 copy-start.2
  63.9 5.5 %pooling.1 = (bf16[512,256]{1,0:T(8,128)(2,1)S(1)}, bf16[512,128]{1,0:T(8,128)(2,1)S(1)}) custom-call(s32[3]{0:T(128)S(1)} %pad_add_fusion.at_ref, bf16[528,2048]{1,0:T(8,128)(2,1)} %get-tuple-element.20.xn_hbm, bf16[2048,256]{1,0:T(8,128)(2,1)} %wg_hbm.1, bf16[2048,128]{1,0:T(8,128)(2,1)} %wp_hbm.2, bf16[128,128]{1,0:T(8,128)(2,1)S(1)} %bitcast.6, ...), custom_call_target="tpu_custom_call" | custom-call | flops 3321888768 | bytes 8000000 | tf_op jit(solution)/shard_map/pooling/pallas_call | solution.py:555
  69.4 8.6 %all-to-all-done.1.got_ref = bf16[64,4,128]{2,1,0:T(4,128)(2,1)S(1)} async-done(((bf16[64,4,128]{2,1,0:T(4,128)(2,1)}), bf16[64,4,128]{2,1,0:T(4,128)(2,1)S(1)}, u32[]{:S(2)}, u32[]{:S(2)}) %all-to-all-start.1) | async-done | bytes 65568 | tf_op jit(solution)/shard_map/all_to_all | solution.py:553
  78.0 2.6 %states.1 = (bf16[256,384]{1,0:T(8,128)(2,1)S(1)}, bf16[256,384]{1,0:T(8,128)(2,1)S(1)}) custom-call(s32[3]{0:T(128)S(1)} %pad_add_fusion.at_ref, bf16[64,4,128]{2,1,0:T(4,128)(2,1)S(1)} %all-to-all-done.1.got_ref, f32[4,8,256]{2,1,0:T(8,128)S(1)} %copy-done.2, f32[4,512,256]{2,1,0:T(8,128)} %get-tuple-element.19.kd_hbm, ...), custom_call_target="tpu_custom_call" | custom-call | flops 1000000000 | bytes 4000000 | tf_op jit(solution)/shard_map/states/pallas_call | solution.py:580
  80.7 3.8 %collective-permute-start.3 = (bf16[256,384]{1,0:T(8,128)(2,1)S(1)}, bf16[256,384]{1,0:T(8,128)(2,1)S(1)}, u32[]{:S(2)}, u32[]{:S(2)}) collective-permute-start(bf16[256,384]{1,0:T(8,128)(2,1)S(1)} %get-tuple-element.24), channel_id=1, source_target_pairs={{0,1},{1,0},{2,3},{3,2},{4,5},{5,4},{6,7},{7,6},{8,9},{9,8},{10,11... | collective-permute-start | bytes 589832 | tf_op jit(solution)/shard_map/ppermute | solution.py:600
  84.4 0.0 collective-permute-done.5.vp_hbm
  84.4 0.0 collective-permute-done.4.vr_hbm
  84.4 1.0 collective-permute-done.3.got_ref
  85.5 3.0 %output.1 = bf16[4,64,2048]{2,1,0:T(8,128)(2,1)S(1)} custom-call(bf16[256,384]{1,0:T(8,128)(2,1)S(1)} %get-tuple-element.23.own_ref, bf16[256,384]{1,0:T(8,128)(2,1)S(1)} %collective-permute-done.3.got_ref, bf16[256,2048]{1,0:T(8,128)(2,1)} %wr_hbm.1, bf16[128,2048]{1,0:T(8,128)(2,1)} %wp_hbm.3, bf16[256,2048]{1,0:T(8,128)(2,1)} %collective-permute-done.4.vr_hbm, ...), custom_call_target="tpu_custom_call" | custom-call | flops 805306368 | bytes 5000000 | tf_op jit(solution)/shard_map/output/pallas_call | solution.py:602
  88.5 17.2 %all_to_all.16 = bf16[4,64,2048]{2,1,0:T(8,128)(2,1)S(1)} all-to-all(bf16[4,64,2048]{2,1,0:T(8,128)(2,1)S(1)} %output.1), channel_id=1, replica_groups={{0,2,4,6},{1,3,5,7},{8,10,12,14},{9,11,13,15},{16,18,20,22},{17,19,21,2..., dimensions={0} | all-to-all | bytes 2097152 | tf_op jit(solution)/shard_map/all_to_all | solution.py:461
  105.8 0.9 reduce_sum.12
  (12 shorter events, 0.0 us)
Async XLA Ops:
  0.0 25.2 %copy-start.4 = (bf16[256,2048]{1,0:T(8,128)(2,1)S(1)}, bf16[256,2048]{1,0:T(8,128)(2,1)}, u32[]{:S(2)}) copy-start(bf16[256,2048]{1,0:T(8,128)(2,1)} %wr_hbm.1) | copy-start | bytes 3145732
  0.0 29.6 %copy-start.7 = (f32[2,256]{1,0:T(2,128)S(1)}, f32[2,256]{1,0:T(2,128)}, u32[]{:S(2)}) copy-start(f32[2,256]{1,0:T(2,128)} %param.21) | copy-start | bytes 6148
  0.0 35.2 %copy-start.5 = (f32[2,512]{1,0:T(2,128)S(1)}, f32[2,512]{1,0:T(2,128)}, u32[]{:S(2)}) copy-start(f32[2,512]{1,0:T(2,128)} %param.23) | copy-start | bytes 12292
  0.0 35.3 %copy-start.6 = (bf16[2048]{0:T(1024)(128)(2,1)S(1)}, bf16[2048]{0:T(1024)(128)(2,1)}, u32[]{:S(2)}) copy-start(bf16[2048]{0:T(1024)(128)(2,1)} %param.15) | copy-start | bytes 12292
  0.0 35.3 %copy-start = (bf16[2,2,4,64,64]{4,3,2,1,0:T(8,128)(2,1)S(1)}, bf16[2,2,4,64,64]{4,3,2,1,0:T(8,128)(2,1)}, u32[]{:S(2)}) copy-start(bf16[2,2,4,64,64]{4,3,2,1,0:T(8,128)(2,1)} %maps_ref.1) | copy-start | bytes 393220
  16.7 21.1 %collective-permute-start = (bf16[4,64,2048]{2,1,0:T(8,128)(2,1)S(1)}, bf16[4,64,2048]{2,1,0:T(8,128)(2,1)S(1)}, u32[]{:S(2)}, u32[]{:S(2)}) collective-permute-start(bf16[4,64,2048]{2,1,0:T(8,128)(2,1)S(1)} %all_to_all.15.own_ref), channel_id=1, source_target_pairs={{0,1},{1,0},{2,3},{3,2},{4,5},{5,4},{6,7},{7,6},{8,9},{9,8},{10,11... | collective-permute-start | bytes 3145736 | tf_op jit(solution)/shard_map/ppermute | solution.py:475
  25.2 59.2 %collective-permute-start.4 = (bf16[256,2048]{1,0:T(8,128)(2,1)S(1)}, bf16[256,2048]{1,0:T(8,128)(2,1)}, u32[]{:S(2)}, u32[]{:S(2)}) collective-permute-start(bf16[256,2048]{1,0:T(8,128)(2,1)S(1)} %copy-done.4), channel_id=1, source_target_pairs={{0,1},{1,0},{2,3},{3,2},{4,5},{5,4},{6,7},{7,6},{8,9},{9,8},{10,11... | collective-permute-start | bytes 3145736 | tf_op jit(solution)/shard_map/ppermute | solution.py:490
  27.2 57.2 %collective-permute-start.5 = (bf16[128,2048]{1,0:T(8,128)(2,1)}, bf16[128,2048]{1,0:T(8,128)(2,1)}, u32[]{:S(2)}, u32[]{:S(2)}) collective-permute-start(bf16[128,2048]{1,0:T(8,128)(2,1)} %wp_hbm.3), channel_id=1, source_target_pairs={{0,1},{1,0},{2,3},{3,2},{4,5},{5,4},{6,7},{7,6},{8,9},{9,8},{10,11... | collective-permute-start | bytes 1572872 | tf_op jit(solution)/shard_map/ppermute | solution.py:491
  29.7 6.9 %collective-permute-start.1 = (bf16[8,2048]{1,0:T(8,128)(2,1)S(1)}, bf16[8,2048]{1,0:T(8,128)(2,1)S(1)}, u32[]{:S(2)}, u32[]{:S(2)}) collective-permute-start(bf16[8,2048]{1,0:T(8,128)(2,1)S(1)} %dynamic-slice_bitcast_fusion), channel_id=1, source_target_pairs={{1,9},{3,11},{5,13},{7,15},{8,0},{9,17},{10,2},{11,19},{12,4},{13,... | collective-permute-start | bytes 98312 | tf_op jit(solution)/shard_map/ppermute | solution.py:496
  32.6 5.2 %collective-permute-start.2 = (bf16[8,2048]{1,0:T(8,128)(2,1)S(1)}, bf16[8,2048]{1,0:T(8,128)(2,1)S(1)}, u32[]{:S(2)}, u32[]{:S(2)}) collective-permute-start(bf16[8,2048]{1,0:T(8,128)(2,1)S(1)} %dynamic-slice_bitcast_fusion), channel_id=1, source_target_pairs={{1,8},{3,10},{5,12},{7,14},{8,1},{9,16},{10,3},{11,18},{12,5},{13,... | collective-permute-start | bytes 98312 | tf_op jit(solution)/shard_map/ppermute | solution.py:497
  37.8 26.1 %copy-start.1 = (bf16[1,128,128]{2,1,0:T(8,128)(2,1)S(1)}, bf16[1,128,128]{2,1,0:T(8,128)(2,1)}, u32[]{:S(2)}) copy-start(bf16[1,128,128]{2,1,0:T(8,128)(2,1)} %param.24) | copy-start | bytes 98308
  37.8 26.1 %copy-start.3 = (bf16[128]{0:T(256)(128)(2,1)S(1)}, bf16[128]{0:T(256)(128)(2,1)}, u32[]{:S(2)}) copy-start(bf16[128]{0:T(256)(128)(2,1)} %param.25) | copy-start | bytes 772
  43.6 34.4 %all-to-all-start.1 = ((bf16[64,4,128]{2,1,0:T(4,128)(2,1)}), bf16[64,4,128]{2,1,0:T(4,128)(2,1)S(1)}, u32[]{:S(2)}, u32[]{:S(2)}) async-start(bf16[64,4,128]{2,1,0:T(4,128)(2,1)} %get-tuple-element.17), calls=%async_computation.1 | async-start | bytes 131072 | tf_op jit(solution)/shard_map/all_to_all | solution.py:553
  63.9 14.1 %copy-start.2 = (f32[4,8,256]{2,1,0:T(8,128)S(1)}, f32[4,8,256]{2,1,0:T(8,128)}, u32[]{:S(2)}) copy-start(f32[4,8,256]{2,1,0:T(8,128)} %get-tuple-element.18.seg_ref) | copy-start | bytes 98308
  80.7 4.8 %collective-permute-start.3 = (bf16[256,384]{1,0:T(8,128)(2,1)S(1)}, bf16[256,384]{1,0:T(8,128)(2,1)S(1)}, u32[]{:S(2)}, u32[]{:S(2)}) collective-permute-start(bf16[256,384]{1,0:T(8,128)(2,1)S(1)} %get-tuple-element.24), channel_id=1, source_target_pairs={{0,1},{1,0},{2,3},{3,2},{4,5},{5,4},{6,7},{7,6},{8,9},{9,8},{10,11... | collective-permute-start | bytes 589832 | tf_op jit(solution)/shard_map/ppermute | solution.py:600

commit v5 on v4

--- a/solution.py
+++ b/solution.py
@@ -404,32 +404,37 @@
             own_ref[rows, lanes] = here.astype(BF16)
 
 
-def output_kernel(
-    own_ref, got_ref, wr_hbm, wp_hbm, vr_hbm, vp_hbm, out_ref, wr_ref, wp_ref, vr_ref, vp_ref, sem
-):
-    pairs = ((wr_hbm, wr_ref), (wp_hbm, wp_ref), (vr_hbm, vr_ref), (vp_hbm, vp_ref))
-    copies = []
+def weights_in_parts(pairs, sem):
+    waits = []
     for k in range(4):
         lanes = slice(k * 512, k * 512 + 512)
-        copies.append(
-            [
-                pltpu.make_async_copy(source.at[:, lanes], target.at[:, lanes], sem.at[k, n])
-                for n, (source, target) in enumerate(pairs)
-            ]
-        )
-        for copy in copies[k]:
+        copies = [
+            pltpu.make_async_copy(source.at[:, lanes], target.at[:, lanes], sem.at[k, n])
+            for n, (source, target) in enumerate(pairs)
+        ]
+        for copy in copies:
             copy.start()
-    own_state = own_ref[:, 0:CH]
-    own_pool = own_ref[:, CH : CH + PC]
-    got_state = got_ref[:, 0:CH]
-    got_pool = got_ref[:, CH : CH + PC]
+        waits.append(copies)
+    return waits
+
+
+def own_output_kernel(own_ref, wr_hbm, wp_hbm, out_ref, wr_ref, wp_ref, sem):
+    waits = weights_in_parts(((wr_hbm, wr_ref), (wp_hbm, wp_ref)), sem)
     for k in range(4):
         lanes = slice(k * 512, k * 512 + 512)
-        for copy in copies[k]:
+        for copy in waits[k]:
             copy.wait()
-        value = dot(own_state, wr_ref[:, lanes]) + dot(got_state, vr_ref[:, lanes])
-        value = value + dot(own_pool, wp_ref[:, lanes]) + dot(got_pool, vp_ref[:, lanes])
-        value = value.astype(BF16)
+        out_ref[:, lanes] = dot(own_ref[:, 0:CH], wr_ref[:, lanes]) + dot(
+            own_ref[:, CH : CH + PC], wp_ref[:, lanes]
+        )
+
+
+def output_kernel(own_ref, got_ref, vr_ref, vp_ref, out_ref):
+    for k in range(4):
+        lanes = slice(k * 512, k * 512 + 512)
+        value = dot(got_ref[:, 0:CH], vr_ref[:, lanes])
+        value = value + dot(got_ref[:, CH : CH + PC], vp_ref[:, lanes])
+        value = (value + own_ref[:, lanes]).astype(BF16)
         for x in range(4):
             out_ref[x, :, lanes] = value[x * STEP : (x + 1) * STEP]
 
@@ -597,28 +602,26 @@
         name="states",
     )(at, got, seg, *kept(kd), gate, pool_mix)
 
-    mix_got = lax.ppermute(mix_send, "tp", sibling)
-
+    mix_got = to_sibling(mix_send)
+    own_part = pl.pallas_call(
+        own_output_kernel,
+        out_shape=jax.ShapeDtypeStruct((256, WIDE), F32),
+        in_specs=[*vspecs(1), *hspecs(2)],
+        out_specs=pl.BlockSpec(memory_space=VMEM),
+        scratch_shapes=[VMEM((CH, WIDE), BF16), VMEM((PC, WIDE), BF16), DMA((4, 2))],
+        compiler_params=params(6),
+        cost_estimate=cost(2 * 256 * 384 * WIDE, 2_500_000),
+        name="own_output",
+    )(mix_own, *kept(recursive_final_matrix, averaging_final_matrix))
     partial = pl.pallas_call(
         output_kernel,
         out_shape=jax.ShapeDtypeStruct((4, STEP, WIDE), BF16),
-        in_specs=[*vspecs(2), *hspecs(4)],
+        in_specs=vspecs(4),
         out_specs=pl.BlockSpec(memory_space=VMEM),
-        scratch_shapes=[
-            VMEM((CH, WIDE), BF16),
-            VMEM((PC, WIDE), BF16),
-            VMEM((CH, WIDE), BF16),
-            VMEM((PC, WIDE), BF16),
-            DMA((4, 4)),
-        ],
-        compiler_params=params(10),
-        cost_estimate=cost(4 * 256 * 384 * WIDE, 5_000_000),
+        compiler_params=params(8),
+        cost_estimate=cost(2 * 256 * 384 * WIDE, 2_500_000),
         name="output",
-    )(
-        mix_own,
-        mix_got,
-        *kept(recursive_final_matrix, averaging_final_matrix, sibling_recursive, sibling_averaging),
-    )
+    )(own_part, mix_got, sibling_recursive, sibling_averaging)
     moved = exchange(partial)
     return jnp.sum(moved.astype(F32), axis=0).astype(BF16)
 

time: 107 us -> 107 us (level)
    ppermute x1 -> x0, starting transfers between devices: 3.75 us -> none  [local(): mix_got = lax.ppermute(mix_send, 'tp', sibling)]
    ppermute x1 -> x2, starting transfers between devices: 8.52 us -> 12.3 us  [to_sibling(): return lax.ppermute(v, 'tp', sibling)]
    pallas_call x0 -> x1, Pallas kernels: none -> 2.21 us  [local(): pl.pallas_call(own_output_kernel, out_shape=jax.ShapeDtypeStruct((256, WI...]
    pallas_call x1, Pallas kernels: 3.05 us -> 1.74 us  [local(): pl.pallas_call(output_kernel, out_shape=jax.ShapeDtypeStruct((4, STEP, WI...]
  transfers between devices with their start and end apart: 7 -> 7, of which waited for: 3 -> 2; matrix products, arithmetic and copies ran while one was open for 0% -> 0% of each run, Pallas kernels for 14% -> 16%
where the time goes in v5:
time: 107 us
  starting transfers between devices  42.3 us (40%)
  blocking collectives  31.9 us (30%)
  Pallas kernels  21.2 us (20%)
  waiting for transfers between devices  9.78 us (9%)
    all_to_all x2, blocking collectives, exchange(): lax.all_to_all(v, 'tp', split_axis=0, concat_axis=0, tiled=True, axis_ind...  31.9 us
    all_to_all x1, starting transfers between devices, local(): got = lax.all_to_all(send, 'sp', split_axis=0, concat_axis=0, tiled=True)  20.3 us
    ppermute x2, starting transfers between devices, to_sibling(): return lax.ppermute(v, 'tp', sibling)  12.3 us
    all_to_all x1, waiting for transfers between devices, local(): got = lax.all_to_all(send, 'sp', split_axis=0, concat_axis=0, tiled=True)  8.58 us
    pallas_call x1, Pallas kernels, local(): pl.pallas_call(gates_kernel, out_shape=(HBM((4, ROWS, CH), F32), HBM((ROW...  5.82 us
    pallas_call x1, Pallas kernels, local(): pl.pallas_call(pooling_kernel, out_shape=(jax.ShapeDtypeStruct((ROWS, CH)...  5.54 us
    ppermute x1, starting transfers between devices, local(): edge_same = lax.ppermute(edge, ('sp', 'tp'), edge_pairs(0))  2.88 us
    pallas_call x1, Pallas kernels, local(): pl.pallas_call(states_kernel, out_shape=(jax.ShapeDtypeStruct((256, CH +...  2.63 us
  transfers between devices with their start and end apart: 7, of which 2 were waited for; matrix products, arithmetic and copies ran while one was open for 0% of the time, Pallas kernels for 16%

profile of v5, /device:TPU:1, one launch (start us, length us, event | category | flops | bytes accessed | tf_op | source)
XLA Modules:
  0.0 106.6 jit_solution(7383501849653256578)
XLA Ops:
  0.0 0.0 copy-start
  0.0 2.0 %spread.1 = bf16[4,64,2048]{2,1,0:T(8,128)(2,1)} custom-call(bf16[64,2048]{1,0:T(8,128)(2,1)} %x_ref.1), custom_call_target="tpu_custom_call" | custom-call | bytes 1300000 | tf_op jit(solution)/shard_map/spread/pallas_call | solution.py:484
  2.0 14.6 %all_to_all.15.own_ref = bf16[4,64,2048]{2,1,0:T(8,128)(2,1)S(1)} all-to-all(bf16[4,64,2048]{2,1,0:T(8,128)(2,1)} %spread.1), channel_id=1, replica_groups={{0,2,4,6},{1,3,5,7},{8,10,12,14},{9,11,13,15},{16,18,20,22},{17,19,21,2..., dimensions={0} | all-to-all | bytes 2097152 | tf_op jit(solution)/shard_map/all_to_all | solution.py:466
  16.6 8.5 %collective-permute-start = (bf16[4,64,2048]{2,1,0:T(8,128)(2,1)S(1)}, bf16[4,64,2048]{2,1,0:T(8,128)(2,1)S(1)}, u32[]{:S(2)}, u32[]{:S(2)}) collective-permute-start(bf16[4,64,2048]{2,1,0:T(8,128)(2,1)S(1)} %all_to_all.15.own_ref), channel_id=1, source_target_pairs={{0,1},{1,0},{2,3},{3,2},{4,5},{5,4},{6,7},{7,6},{8,9},{9,8},{10,11... | collective-permute-start | bytes 3145736 | tf_op jit(solution)/shard_map/ppermute | solution.py:480
  25.2 1.9 %collective-permute-start.4 = (bf16[256,2048]{1,0:T(8,128)(2,1)}, bf16[256,2048]{1,0:T(8,128)(2,1)S(1)}, u32[]{:S(2)}, u32[]{:S(2)}) collective-permute-start(bf16[256,2048]{1,0:T(8,128)(2,1)} %wr_hbm.1), channel_id=1, source_target_pairs={{0,1},{1,0},{2,3},{3,2},{4,5},{5,4},{6,7},{7,6},{8,9},{9,8},{10,11... | collective-permute-start | bytes 3145736 | tf_op jit(solution)/shard_map/ppermute | solution.py:495
  27.1 2.4 %collective-permute-start.5 = (bf16[128,2048]{1,0:T(8,128)(2,1)}, bf16[128,2048]{1,0:T(8,128)(2,1)}, u32[]{:S(2)}, u32[]{:S(2)}) collective-permute-start(bf16[128,2048]{1,0:T(8,128)(2,1)} %wp_hbm.3), channel_id=1, source_target_pairs={{0,1},{1,0},{2,3},{3,2},{4,5},{5,4},{6,7},{7,6},{8,9},{9,8},{10,11... | collective-permute-start | bytes 1572872 | tf_op jit(solution)/shard_map/ppermute | solution.py:496
  29.5 0.0 copy-done.6
  29.6 2.9 %collective-permute-start.1 = (bf16[8,2048]{1,0:T(8,128)(2,1)S(1)}, bf16[8,2048]{1,0:T(8,128)(2,1)S(1)}, u32[]{:S(2)}, u32[]{:S(2)}) collective-permute-start(bf16[8,2048]{1,0:T(8,128)(2,1)S(1)} %dynamic-slice_bitcast_fusion), channel_id=1, source_target_pairs={{1,9},{3,11},{5,13},{7,15},{8,0},{9,17},{10,2},{11,19},{12,4},{13,... | collective-permute-start | bytes 98312 | tf_op jit(solution)/shard_map/ppermute | solution.py:501
  32.5 2.6 %collective-permute-start.2 = (bf16[8,2048]{1,0:T(8,128)(2,1)S(1)}, bf16[8,2048]{1,0:T(8,128)(2,1)S(1)}, u32[]{:S(2)}, u32[]{:S(2)}) collective-permute-start(bf16[8,2048]{1,0:T(8,128)(2,1)S(1)} %dynamic-slice_bitcast_fusion), channel_id=1, source_target_pairs={{1,8},{3,10},{5,12},{7,14},{8,1},{9,16},{10,3},{11,18},{12,5},{13,... | collective-permute-start | bytes 98312 | tf_op jit(solution)/shard_map/ppermute | solution.py:502
  35.1 0.1 pad_add_fusion.at_ref
  35.1 0.0 copy-done.4
  35.1 0.1 reshape.17.extra_ref
  35.2 0.0 copy-done.5
  35.2 0.0 copy-done
  35.2 1.3 %tables.1 = (bf16[256,1024]{1,0:T(8,128)(2,1)}, f32[2,512,128]{2,1,0:T(8,128)}) custom-call(bf16[2,2,4,64,64]{4,3,2,1,0:T(8,128)(2,1)S(1)} %copy-done, f32[2,8,64]{2,1,0:T(8,128)S(1)} %reshape.17.extra_ref), custom_call_target="tpu_custom_call" | custom-call | flops 1000000 | bytes 2000000 | tf_op jit(solution)/shard_map/tables/pallas_call | solution.py:507
  36.5 0.0 collective-permute-done.1.h1_ref
  36.5 1.2 %collective-permute-done.2.h2_ref = bf16[8,2048]{1,0:T(8,128)(2,1)S(1)} collective-permute-done((bf16[8,2048]{1,0:T(8,128)(2,1)S(1)}, bf16[8,2048]{1,0:T(8,128)(2,1)S(1)}, u32[]{:S(2)}, u32[]{:S(2)}) %collective-permute-start.2) | collective-permute-done | bytes 32800 | tf_op jit(solution)/shard_map/ppermute | solution.py:502
  37.7 0.0 collective-permute-done.other_ref
  37.7 5.8 %gates.1 = (f32[4,512,256]{2,1,0:T(8,128)}, bf16[528,2048]{1,0:T(8,128)(2,1)}, f32[4,8,256]{2,1,0:T(8,128)}, bf16[64,4,128]{2,1,0:T(4,128)(2,1)}) custom-call(s32[3]{0:T(128)S(1)} %pad_add_fusion.at_ref, bf16[4,64,2048]{2,1,0:T(8,128)(2,1)S(1)} %all_to_all.15.own_ref, bf16[4,64,2048]{2,1,0:T(8,128)(2,1)S(1)} %collective-permute-done.other_ref, ...), custom_call_target="tpu_custom_call" | custom-call | flops 553648128 | bytes 8000000 | tf_op jit(solution)/shard_map/gates/pallas_call | solution.py:520
  43.5 20.3 %all-to-all-start.1 = ((bf16[64,4,128]{2,1,0:T(4,128)(2,1)}), bf16[64,4,128]{2,1,0:T(4,128)(2,1)S(1)}, u32[]{:S(2)}, u32[]{:S(2)}) async-start(bf16[64,4,128]{2,1,0:T(4,128)(2,1)} %get-tuple-element.17), calls=%async_computation.1 | async-start | bytes 131072 | tf_op jit(solution)/shard_map/all_to_all | solution.py:558
  63.8 0.0 copy-done.1
  63.8 5.5 %pooling.1 = (bf16[512,256]{1,0:T(8,128)(2,1)S(1)}, bf16[512,128]{1,0:T(8,128)(2,1)S(1)}) custom-call(s32[3]{0:T(128)S(1)} %pad_add_fusion.at_ref, bf16[528,2048]{1,0:T(8,128)(2,1)} %get-tuple-element.20.xn_hbm, bf16[2048,256]{1,0:T(8,128)(2,1)} %wg_hbm.1, bf16[2048,128]{1,0:T(8,128)(2,1)} %wp_hbm.2, bf16[128,128]{1,0:T(8,128)(2,1)S(1)} %bitcast.6, ...), custom_call_target="tpu_custom_call" | custom-call | flops 3321888768 | bytes 8000000 | tf_op jit(solution)/shard_map/pooling/pallas_call | solution.py:560
  69.4 8.6 %all-to-all-done.1.got_ref = bf16[64,4,128]{2,1,0:T(4,128)(2,1)S(1)} async-done(((bf16[64,4,128]{2,1,0:T(4,128)(2,1)}), bf16[64,4,128]{2,1,0:T(4,128)(2,1)S(1)}, u32[]{:S(2)}, u32[]{:S(2)}) %all-to-all-start.1) | async-done | bytes 65568 | tf_op jit(solution)/shard_map/all_to_all | solution.py:558
  78.0 2.6 %states.1 = (bf16[256,384]{1,0:T(8,128)(2,1)S(1)}, bf16[256,384]{1,0:T(8,128)(2,1)S(1)}) custom-call(s32[3]{0:T(128)S(1)} %pad_add_fusion.at_ref, bf16[64,4,128]{2,1,0:T(4,128)(2,1)S(1)} %all-to-all-done.1.got_ref, f32[4,8,256]{2,1,0:T(8,128)S(1)} %copy-done.2, f32[4,512,256]{2,1,0:T(8,128)} %get-tuple-element.19.kd_hbm, ...), custom_call_target="tpu_custom_call" | custom-call | flops 1000000000 | bytes 4000000 | tf_op jit(solution)/shard_map/states/pallas_call | solution.py:585
  80.6 3.8 %collective-permute-start.3 = (bf16[256,384]{1,0:T(8,128)(2,1)S(1)}, bf16[256,384]{1,0:T(8,128)(2,1)S(1)}, u32[]{:S(2)}, u32[]{:S(2)}) collective-permute-start(bf16[256,384]{1,0:T(8,128)(2,1)S(1)} %get-tuple-element.24), channel_id=1, source_target_pairs={{0,1},{1,0},{2,3},{3,2},{4,5},{5,4},{6,7},{7,6},{8,9},{9,8},{10,11... | collective-permute-start | bytes 589832 | tf_op jit(solution)/shard_map/ppermute | solution.py:480
  84.3 2.2 %own_output.1.own_ref = f32[256,2048]{1,0:T(8,128)S(1)} custom-call(bf16[256,384]{1,0:T(8,128)(2,1)S(1)} %get-tuple-element.23.own_ref, bf16[256,2048]{1,0:T(8,128)(2,1)} %wr_hbm.1, bf16[128,2048]{1,0:T(8,128)(2,1)} %wp_hbm.3), custom_call_target="tpu_custom_call" | custom-call | flops 402653184 | bytes 2500000 | tf_op jit(solution)/shard_map/own_output/pallas_call | solution.py:606
  86.6 0.0 collective-permute-done.5.vp_ref
  86.6 0.0 collective-permute-done.4.vr_ref
  86.6 0.0 collective-permute-done.3.got_ref
  86.6 1.7 %output.1 = bf16[4,64,2048]{2,1,0:T(8,128)(2,1)S(1)} custom-call(f32[256,2048]{1,0:T(8,128)S(1)} %own_output.1.own_ref, bf16[256,384]{1,0:T(8,128)(2,1)S(1)} %collective-permute-done.3.got_ref, bf16[256,2048]{1,0:T(8,128)(2,1)S(1)} %collective-permute-done.4.vr_ref, bf16[128,2048]{1,0:T(8,128)(2,1)} %collective-permute-done.5.vp_ref), custom_call_target="tpu_custom_call" | custom-call | flops 402653184 | bytes 2500000 | tf_op jit(solution)/shard_map/output/pallas_call | solution.py:616
  88.3 17.3 %all_to_all.16 = bf16[4,64,2048]{2,1,0:T(8,128)(2,1)S(1)} all-to-all(bf16[4,64,2048]{2,1,0:T(8,128)(2,1)S(1)} %output.1), channel_id=1, replica_groups={{0,2,4,6},{1,3,5,7},{8,10,12,14},{9,11,13,15},{16,18,20,22},{17,19,21,2..., dimensions={0} | all-to-all | bytes 2097152 | tf_op jit(solution)/shard_map/all_to_all | solution.py:466
  105.6 0.9 reduce_sum.12
  (11 shorter events, 0.0 us)
Async XLA Ops:
  0.0 29.5 %copy-start.6 = (f32[2,256]{1,0:T(2,128)S(1)}, f32[2,256]{1,0:T(2,128)}, u32[]{:S(2)}) copy-start(f32[2,256]{1,0:T(2,128)} %param.21) | copy-start | bytes 6148
  0.0 35.1 %copy-start.4 = (f32[2,512]{1,0:T(2,128)S(1)}, f32[2,512]{1,0:T(2,128)}, u32[]{:S(2)}) copy-start(f32[2,512]{1,0:T(2,128)} %param.23) | copy-start | bytes 12292
  0.0 35.2 %copy-start.5 = (bf16[2048]{0:T(1024)(128)(2,1)S(1)}, bf16[2048]{0:T(1024)(128)(2,1)}, u32[]{:S(2)}) copy-start(bf16[2048]{0:T(1024)(128)(2,1)} %param.15) | copy-start | bytes 12292
  0.0 35.2 %copy-start = (bf16[2,2,4,64,64]{4,3,2,1,0:T(8,128)(2,1)S(1)}, bf16[2,2,4,64,64]{4,3,2,1,0:T(8,128)(2,1)}, u32[]{:S(2)}) copy-start(bf16[2,2,4,64,64]{4,3,2,1,0:T(8,128)(2,1)} %maps_ref.1) | copy-start | bytes 393220
  16.6 21.1 %collective-permute-start = (bf16[4,64,2048]{2,1,0:T(8,128)(2,1)S(1)}, bf16[4,64,2048]{2,1,0:T(8,128)(2,1)S(1)}, u32[]{:S(2)}, u32[]{:S(2)}) collective-permute-start(bf16[4,64,2048]{2,1,0:T(8,128)(2,1)S(1)} %all_to_all.15.own_ref), channel_id=1, source_target_pairs={{0,1},{1,0},{2,3},{3,2},{4,5},{5,4},{6,7},{7,6},{8,9},{9,8},{10,11... | collective-permute-start | bytes 3145736 | tf_op jit(solution)/shard_map/ppermute | solution.py:480
  25.2 61.4 %collective-permute-start.4 = (bf16[256,2048]{1,0:T(8,128)(2,1)}, bf16[256,2048]{1,0:T(8,128)(2,1)S(1)}, u32[]{:S(2)}, u32[]{:S(2)}) collective-permute-start(bf16[256,2048]{1,0:T(8,128)(2,1)} %wr_hbm.1), channel_id=1, source_target_pairs={{0,1},{1,0},{2,3},{3,2},{4,5},{5,4},{6,7},{7,6},{8,9},{9,8},{10,11... | collective-permute-start | bytes 3145736 | tf_op jit(solution)/shard_map/ppermute | solution.py:495
  27.1 59.5 %collective-permute-start.5 = (bf16[128,2048]{1,0:T(8,128)(2,1)}, bf16[128,2048]{1,0:T(8,128)(2,1)}, u32[]{:S(2)}, u32[]{:S(2)}) collective-permute-start(bf16[128,2048]{1,0:T(8,128)(2,1)} %wp_hbm.3), channel_id=1, source_target_pairs={{0,1},{1,0},{2,3},{3,2},{4,5},{5,4},{6,7},{7,6},{8,9},{9,8},{10,11... | collective-permute-start | bytes 1572872 | tf_op jit(solution)/shard_map/ppermute | solution.py:496
  29.6 6.9 %collective-permute-start.1 = (bf16[8,2048]{1,0:T(8,128)(2,1)S(1)}, bf16[8,2048]{1,0:T(8,128)(2,1)S(1)}, u32[]{:S(2)}, u32[]{:S(2)}) collective-permute-start(bf16[8,2048]{1,0:T(8,128)(2,1)S(1)} %dynamic-slice_bitcast_fusion), channel_id=1, source_target_pairs={{1,9},{3,11},{5,13},{7,15},{8,0},{9,17},{10,2},{11,19},{12,4},{13,... | collective-permute-start | bytes 98312 | tf_op jit(solution)/shard_map/ppermute | solution.py:501
  32.5 5.2 %collective-permute-start.2 = (bf16[8,2048]{1,0:T(8,128)(2,1)S(1)}, bf16[8,2048]{1,0:T(8,128)(2,1)S(1)}, u32[]{:S(2)}, u32[]{:S(2)}) collective-permute-start(bf16[8,2048]{1,0:T(8,128)(2,1)S(1)} %dynamic-slice_bitcast_fusion), channel_id=1, source_target_pairs={{1,8},{3,10},{5,12},{7,14},{8,1},{9,16},{10,3},{11,18},{12,5},{13,... | collective-permute-start | bytes 98312 | tf_op jit(solution)/shard_map/ppermute | solution.py:502
  37.7 26.1 %copy-start.1 = (bf16[1,128,128]{2,1,0:T(8,128)(2,1)S(1)}, bf16[1,128,128]{2,1,0:T(8,128)(2,1)}, u32[]{:S(2)}) copy-start(bf16[1,128,128]{2,1,0:T(8,128)(2,1)} %param.24) | copy-start | bytes 98308
  37.7 26.1 %copy-start.3 = (bf16[128]{0:T(256)(128)(2,1)S(1)}, bf16[128]{0:T(256)(128)(2,1)}, u32[]{:S(2)}) copy-start(bf16[128]{0:T(256)(128)(2,1)} %param.25) | copy-start | bytes 772
  43.5 34.4 %all-to-all-start.1 = ((bf16[64,4,128]{2,1,0:T(4,128)(2,1)}), bf16[64,4,128]{2,1,0:T(4,128)(2,1)S(1)}, u32[]{:S(2)}, u32[]{:S(2)}) async-start(bf16[64,4,128]{2,1,0:T(4,128)(2,1)} %get-tuple-element.17), calls=%async_computation.1 | async-start | bytes 131072 | tf_op jit(solution)/shard_map/all_to_all | solution.py:558
  63.8 14.1 %copy-start.2 = (f32[4,8,256]{2,1,0:T(8,128)S(1)}, f32[4,8,256]{2,1,0:T(8,128)}, u32[]{:S(2)}) copy-start(f32[4,8,256]{2,1,0:T(8,128)} %get-tuple-element.18.seg_ref) | copy-start | bytes 98308
  80.6 6.0 %collective-permute-start.3 = (bf16[256,384]{1,0:T(8,128)(2,1)S(1)}, bf16[256,384]{1,0:T(8,128)(2,1)S(1)}, u32[]{:S(2)}, u32[]{:S(2)}) collective-permute-start(bf16[256,384]{1,0:T(8,128)(2,1)S(1)} %get-tuple-element.24), channel_id=1, source_target_pairs={{0,1},{1,0},{2,3},{3,2},{4,5},{5,4},{6,7},{7,6},{8,9},{9,8},{10,11... | collective-permute-start | bytes 589832 | tf_op jit(solution)/shard_map/ppermute | solution.py:480

commit v6 on v5

--- a/solution.py
+++ b/solution.py
@@ -534,7 +534,7 @@
             VMEM((2, ROWS), F32),
             VMEM((2, ROWS, 128), F32),
             VMEM((ROWS + 2 * EDGE, WIDE), BF16),
-            VMEM((2, SEG * PITCH, 128), F32),
+            VMEM((2, (SEG + 1) * PITCH, 128), F32),
             VMEM((ROWS, CH), BF16),
             VMEM((ROWS, 4 * CH), F32),
             VMEM((4, ROWS, CH), F32),
@@ -569,7 +569,7 @@
             VMEM((ROWS + 2 * EDGE, WIDE), BF16),
             VMEM((WIDE, CH), BF16),
             VMEM((WIDE, PC), BF16),
-            VMEM((3, SEG * PITCH, 128), F32),
+            VMEM((3, (SEG + 1) * PITCH, 128), F32),
             VMEM((ROWS + 2 * EDGE * SEG, PC), F32),
             VMEM((ROWS, PC), BF16),
             DMA((3,)),
@@ -594,7 +594,7 @@
             VMEM((4, ROWS, CH), F32),
             VMEM((ROWS, CH), F32),
             VMEM((ROWS, CH), F32),
-            VMEM((3, ROWS, 128), F32),
+            VMEM((3, ROWS + SEG, 128), F32),
             DMA((8,)),
         ],
         compiler_params=params(8),

time: 107 us -> 107 us (level)
  no operation moved by 1% of the time
where the time goes in v6:
time: 107 us
  starting transfers between devices  42.3 us (40%)
  blocking collectives  31.9 us (30%)
  Pallas kernels  21.2 us (20%)
  waiting for transfers between devices  9.79 us (9%)
    all_to_all x2, blocking collectives, exchange(): lax.all_to_all(v, 'tp', split_axis=0, concat_axis=0, tiled=True, axis_ind...  31.9 us
    all_to_all x1, starting transfers between devices, local(): got = lax.all_to_all(send, 'sp', split_axis=0, concat_axis=0, tiled=True)  20.3 us
    ppermute x2, starting transfers between devices, to_sibling(): return lax.ppermute(v, 'tp', sibling)  12.3 us
    all_to_all x1, waiting for transfers between devices, local(): got = lax.all_to_all(send, 'sp', split_axis=0, concat_axis=0, tiled=True)  8.58 us
    pallas_call x1, Pallas kernels, local(): pl.pallas_call(gates_kernel, out_shape=(HBM((4, ROWS, CH), F32), HBM((ROW...  5.82 us
    pallas_call x1, Pallas kernels, local(): pl.pallas_call(pooling_kernel, out_shape=(jax.ShapeDtypeStruct((ROWS, CH)...  5.53 us
    ppermute x1, starting transfers between devices, local(): edge_same = lax.ppermute(edge, ('sp', 'tp'), edge_pairs(0))  2.88 us
    pallas_call x1, Pallas kernels, local(): pl.pallas_call(states_kernel, out_shape=(jax.ShapeDtypeStruct((256, CH +...  2.63 us
  transfers between devices with their start and end apart: 7, of which 2 were waited for; matrix products, arithmetic and copies ran while one was open for 0% of the time, Pallas kernels for 16%

profile of v6, /device:TPU:1, one launch (start us, length us, event | category | flops | bytes accessed | tf_op | source)
XLA Modules:
  0.0 106.6 jit_solution(10200699786560341101)
XLA Ops:
  0.0 0.0 copy-start
  0.0 2.0 %spread.1 = bf16[4,64,2048]{2,1,0:T(8,128)(2,1)} custom-call(bf16[64,2048]{1,0:T(8,128)(2,1)} %x_ref.1), custom_call_target="tpu_custom_call" | custom-call | bytes 1300000 | tf_op jit(solution)/shard_map/spread/pallas_call | solution.py:484
  2.0 14.6 %all_to_all.15.own_ref = bf16[4,64,2048]{2,1,0:T(8,128)(2,1)S(1)} all-to-all(bf16[4,64,2048]{2,1,0:T(8,128)(2,1)} %spread.1), channel_id=1, replica_groups={{0,2,4,6},{1,3,5,7},{8,10,12,14},{9,11,13,15},{16,18,20,22},{17,19,21,2..., dimensions={0} | all-to-all | bytes 2097152 | tf_op jit(solution)/shard_map/all_to_all | solution.py:466
  16.6 8.5 %collective-permute-start = (bf16[4,64,2048]{2,1,0:T(8,128)(2,1)S(1)}, bf16[4,64,2048]{2,1,0:T(8,128)(2,1)S(1)}, u32[]{:S(2)}, u32[]{:S(2)}) collective-permute-start(bf16[4,64,2048]{2,1,0:T(8,128)(2,1)S(1)} %all_to_all.15.own_ref), channel_id=1, source_target_pairs={{0,1},{1,0},{2,3},{3,2},{4,5},{5,4},{6,7},{7,6},{8,9},{9,8},{10,11... | collective-permute-start | bytes 3145736 | tf_op jit(solution)/shard_map/ppermute | solution.py:480
  25.2 1.9 %collective-permute-start.4 = (bf16[256,2048]{1,0:T(8,128)(2,1)}, bf16[256,2048]{1,0:T(8,128)(2,1)S(1)}, u32[]{:S(2)}, u32[]{:S(2)}) collective-permute-start(bf16[256,2048]{1,0:T(8,128)(2,1)} %wr_hbm.1), channel_id=1, source_target_pairs={{0,1},{1,0},{2,3},{3,2},{4,5},{5,4},{6,7},{7,6},{8,9},{9,8},{10,11... | collective-permute-start | bytes 3145736 | tf_op jit(solution)/shard_map/ppermute | solution.py:495
  27.1 2.4 %collective-permute-start.5 = (bf16[128,2048]{1,0:T(8,128)(2,1)}, bf16[128,2048]{1,0:T(8,128)(2,1)}, u32[]{:S(2)}, u32[]{:S(2)}) collective-permute-start(bf16[128,2048]{1,0:T(8,128)(2,1)} %wp_hbm.3), channel_id=1, source_target_pairs={{0,1},{1,0},{2,3},{3,2},{4,5},{5,4},{6,7},{7,6},{8,9},{9,8},{10,11... | collective-permute-start | bytes 1572872 | tf_op jit(solution)/shard_map/ppermute | solution.py:496
  29.6 2.9 %collective-permute-start.1 = (bf16[8,2048]{1,0:T(8,128)(2,1)S(1)}, bf16[8,2048]{1,0:T(8,128)(2,1)S(1)}, u32[]{:S(2)}, u32[]{:S(2)}) collective-permute-start(bf16[8,2048]{1,0:T(8,128)(2,1)S(1)} %dynamic-slice_bitcast_fusion), channel_id=1, source_target_pairs={{1,9},{3,11},{5,13},{7,15},{8,0},{9,17},{10,2},{11,19},{12,4},{13,... | collective-permute-start | bytes 98312 | tf_op jit(solution)/shard_map/ppermute | solution.py:501
  32.5 2.6 %collective-permute-start.2 = (bf16[8,2048]{1,0:T(8,128)(2,1)S(1)}, bf16[8,2048]{1,0:T(8,128)(2,1)S(1)}, u32[]{:S(2)}, u32[]{:S(2)}) collective-permute-start(bf16[8,2048]{1,0:T(8,128)(2,1)S(1)} %dynamic-slice_bitcast_fusion), channel_id=1, source_target_pairs={{1,8},{3,10},{5,12},{7,14},{8,1},{9,16},{10,3},{11,18},{12,5},{13,... | collective-permute-start | bytes 98312 | tf_op jit(solution)/shard_map/ppermute | solution.py:502
  35.1 0.1 pad_add_fusion.at_ref
  35.1 0.0 copy-done.4
  35.1 0.1 reshape.17.extra_ref
  35.2 0.0 copy-done.5
  35.2 0.0 copy-done
  35.2 1.3 %tables.1 = (bf16[256,1024]{1,0:T(8,128)(2,1)}, f32[2,512,128]{2,1,0:T(8,128)}) custom-call(bf16[2,2,4,64,64]{4,3,2,1,0:T(8,128)(2,1)S(1)} %copy-done, f32[2,8,64]{2,1,0:T(8,128)S(1)} %reshape.17.extra_ref), custom_call_target="tpu_custom_call" | custom-call | flops 1000000 | bytes 2000000 | tf_op jit(solution)/shard_map/tables/pallas_call | solution.py:507
  36.5 0.0 collective-permute-done.1.h1_ref
  36.5 1.2 %collective-permute-done.2.h2_ref = bf16[8,2048]{1,0:T(8,128)(2,1)S(1)} collective-permute-done((bf16[8,2048]{1,0:T(8,128)(2,1)S(1)}, bf16[8,2048]{1,0:T(8,128)(2,1)S(1)}, u32[]{:S(2)}, u32[]{:S(2)}) %collective-permute-start.2) | collective-permute-done | bytes 32800 | tf_op jit(solution)/shard_map/ppermute | solution.py:502
  37.7 0.0 collective-permute-done.other_ref
  37.7 5.8 %gates.1 = (f32[4,512,256]{2,1,0:T(8,128)}, bf16[528,2048]{1,0:T(8,128)(2,1)}, f32[4,8,256]{2,1,0:T(8,128)}, bf16[64,4,128]{2,1,0:T(4,128)(2,1)}) custom-call(s32[3]{0:T(128)S(1)} %pad_add_fusion.at_ref, bf16[4,64,2048]{2,1,0:T(8,128)(2,1)S(1)} %all_to_all.15.own_ref, bf16[4,64,2048]{2,1,0:T(8,128)(2,1)S(1)} %collective-permute-done.other_ref, ...), custom_call_target="tpu_custom_call" | custom-call | flops 553648128 | bytes 8000000 | tf_op jit(solution)/shard_map/gates/pallas_call | solution.py:520
  43.5 20.3 %all-to-all-start.1 = ((bf16[64,4,128]{2,1,0:T(4,128)(2,1)}), bf16[64,4,128]{2,1,0:T(4,128)(2,1)S(1)}, u32[]{:S(2)}, u32[]{:S(2)}) async-start(bf16[64,4,128]{2,1,0:T(4,128)(2,1)} %get-tuple-element.17), calls=%async_computation.1 | async-start | bytes 131072 | tf_op jit(solution)/shard_map/all_to_all | solution.py:558
  63.8 0.0 copy-done.1
  63.8 0.0 copy-done.3
  63.8 5.5 %pooling.1 = (bf16[512,256]{1,0:T(8,128)(2,1)S(1)}, bf16[512,128]{1,0:T(8,128)(2,1)S(1)}) custom-call(s32[3]{0:T(128)S(1)} %pad_add_fusion.at_ref, bf16[528,2048]{1,0:T(8,128)(2,1)} %get-tuple-element.20.xn_hbm, bf16[2048,256]{1,0:T(8,128)(2,1)} %wg_hbm.1, bf16[2048,128]{1,0:T(8,128)(2,1)} %wp_hbm.2, bf16[128,128]{1,0:T(8,128)(2,1)S(1)} %bitcast.6, ...), custom_call_target="tpu_custom_call" | custom-call | flops 3321888768 | bytes 8000000 | tf_op jit(solution)/shard_map/pooling/pallas_call | solution.py:560
  69.4 8.6 %all-to-all-done.1.got_ref = bf16[64,4,128]{2,1,0:T(4,128)(2,1)S(1)} async-done(((bf16[64,4,128]{2,1,0:T(4,128)(2,1)}), bf16[64,4,128]{2,1,0:T(4,128)(2,1)S(1)}, u32[]{:S(2)}, u32[]{:S(2)}) %all-to-all-start.1) | async-done | bytes 65568 | tf_op jit(solution)/shard_map/all_to_all | solution.py:558
  78.0 2.6 %states.1 = (bf16[256,384]{1,0:T(8,128)(2,1)S(1)}, bf16[256,384]{1,0:T(8,128)(2,1)S(1)}) custom-call(s32[3]{0:T(128)S(1)} %pad_add_fusion.at_ref, bf16[64,4,128]{2,1,0:T(4,128)(2,1)S(1)} %all-to-all-done.1.got_ref, f32[4,8,256]{2,1,0:T(8,128)S(1)} %copy-done.2, f32[4,512,256]{2,1,0:T(8,128)} %get-tuple-element.19.kd_hbm, ...), custom_call_target="tpu_custom_call" | custom-call | flops 1000000000 | bytes 4000000 | tf_op jit(solution)/shard_map/states/pallas_call | solution.py:585
  80.6 3.8 %collective-permute-start.3 = (bf16[256,384]{1,0:T(8,128)(2,1)S(1)}, bf16[256,384]{1,0:T(8,128)(2,1)S(1)}, u32[]{:S(2)}, u32[]{:S(2)}) collective-permute-start(bf16[256,384]{1,0:T(8,128)(2,1)S(1)} %get-tuple-element.24), channel_id=1, source_target_pairs={{0,1},{1,0},{2,3},{3,2},{4,5},{5,4},{6,7},{7,6},{8,9},{9,8},{10,11... | collective-permute-start | bytes 589832 | tf_op jit(solution)/shard_map/ppermute | solution.py:480
  84.4 2.2 %own_output.1.own_ref = f32[256,2048]{1,0:T(8,128)S(1)} custom-call(bf16[256,384]{1,0:T(8,128)(2,1)S(1)} %get-tuple-element.23.own_ref, bf16[256,2048]{1,0:T(8,128)(2,1)} %wr_hbm.1, bf16[128,2048]{1,0:T(8,128)(2,1)} %wp_hbm.3), custom_call_target="tpu_custom_call" | custom-call | flops 402653184 | bytes 2500000 | tf_op jit(solution)/shard_map/own_output/pallas_call | solution.py:606
  86.6 0.0 collective-permute-done.5.vp_ref
  86.6 0.0 collective-permute-done.4.vr_ref
  86.6 0.0 collective-permute-done.3.got_ref
  86.6 1.7 %output.1 = bf16[4,64,2048]{2,1,0:T(8,128)(2,1)S(1)} custom-call(f32[256,2048]{1,0:T(8,128)S(1)} %own_output.1.own_ref, bf16[256,384]{1,0:T(8,128)(2,1)S(1)} %collective-permute-done.3.got_ref, bf16[256,2048]{1,0:T(8,128)(2,1)S(1)} %collective-permute-done.4.vr_ref, bf16[128,2048]{1,0:T(8,128)(2,1)} %collective-permute-done.5.vp_ref), custom_call_target="tpu_custom_call" | custom-call | flops 402653184 | bytes 2500000 | tf_op jit(solution)/shard_map/output/pallas_call | solution.py:616
  88.3 17.3 %all_to_all.16 = bf16[4,64,2048]{2,1,0:T(8,128)(2,1)S(1)} all-to-all(bf16[4,64,2048]{2,1,0:T(8,128)(2,1)S(1)} %output.1), channel_id=1, replica_groups={{0,2,4,6},{1,3,5,7},{8,10,12,14},{9,11,13,15},{16,18,20,22},{17,19,21,2..., dimensions={0} | all-to-all | bytes 2097152 | tf_op jit(solution)/shard_map/all_to_all | solution.py:466
  105.7 0.9 reduce_sum.12
  (11 shorter events, 0.0 us)
Async XLA Ops:
  0.0 29.5 %copy-start.6 = (f32[2,256]{1,0:T(2,128)S(1)}, f32[2,256]{1,0:T(2,128)}, u32[]{:S(2)}) copy-start(f32[2,256]{1,0:T(2,128)} %param.21) | copy-start | bytes 6148
  0.0 35.1 %copy-start.4 = (f32[2,512]{1,0:T(2,128)S(1)}, f32[2,512]{1,0:T(2,128)}, u32[]{:S(2)}) copy-start(f32[2,512]{1,0:T(2,128)} %param.23) | copy-start | bytes 12292
  0.0 35.2 %copy-start.5 = (bf16[2048]{0:T(1024)(128)(2,1)S(1)}, bf16[2048]{0:T(1024)(128)(2,1)}, u32[]{:S(2)}) copy-start(bf16[2048]{0:T(1024)(128)(2,1)} %param.15) | copy-start | bytes 12292
  0.0 35.2 %copy-start = (bf16[2,2,4,64,64]{4,3,2,1,0:T(8,128)(2,1)S(1)}, bf16[2,2,4,64,64]{4,3,2,1,0:T(8,128)(2,1)}, u32[]{:S(2)}) copy-start(bf16[2,2,4,64,64]{4,3,2,1,0:T(8,128)(2,1)} %maps_ref.1) | copy-start | bytes 393220
  16.6 21.1 %collective-permute-start = (bf16[4,64,2048]{2,1,0:T(8,128)(2,1)S(1)}, bf16[4,64,2048]{2,1,0:T(8,128)(2,1)S(1)}, u32[]{:S(2)}, u32[]{:S(2)}) collective-permute-start(bf16[4,64,2048]{2,1,0:T(8,128)(2,1)S(1)} %all_to_all.15.own_ref), channel_id=1, source_target_pairs={{0,1},{1,0},{2,3},{3,2},{4,5},{5,4},{6,7},{7,6},{8,9},{9,8},{10,11... | collective-permute-start | bytes 3145736 | tf_op jit(solution)/shard_map/ppermute | solution.py:480
  25.2 61.4 %collective-permute-start.4 = (bf16[256,2048]{1,0:T(8,128)(2,1)}, bf16[256,2048]{1,0:T(8,128)(2,1)S(1)}, u32[]{:S(2)}, u32[]{:S(2)}) collective-permute-start(bf16[256,2048]{1,0:T(8,128)(2,1)} %wr_hbm.1), channel_id=1, source_target_pairs={{0,1},{1,0},{2,3},{3,2},{4,5},{5,4},{6,7},{7,6},{8,9},{9,8},{10,11... | collective-permute-start | bytes 3145736 | tf_op jit(solution)/shard_map/ppermute | solution.py:495
  27.1 59.5 %collective-permute-start.5 = (bf16[128,2048]{1,0:T(8,128)(2,1)}, bf16[128,2048]{1,0:T(8,128)(2,1)}, u32[]{:S(2)}, u32[]{:S(2)}) collective-permute-start(bf16[128,2048]{1,0:T(8,128)(2,1)} %wp_hbm.3), channel_id=1, source_target_pairs={{0,1},{1,0},{2,3},{3,2},{4,5},{5,4},{6,7},{7,6},{8,9},{9,8},{10,11... | collective-permute-start | bytes 1572872 | tf_op jit(solution)/shard_map/ppermute | solution.py:496
  29.6 6.9 %collective-permute-start.1 = (bf16[8,2048]{1,0:T(8,128)(2,1)S(1)}, bf16[8,2048]{1,0:T(8,128)(2,1)S(1)}, u32[]{:S(2)}, u32[]{:S(2)}) collective-permute-start(bf16[8,2048]{1,0:T(8,128)(2,1)S(1)} %dynamic-slice_bitcast_fusion), channel_id=1, source_target_pairs={{1,9},{3,11},{5,13},{7,15},{8,0},{9,17},{10,2},{11,19},{12,4},{13,... | collective-permute-start | bytes 98312 | tf_op jit(solution)/shard_map/ppermute | solution.py:501
  32.5 5.2 %collective-permute-start.2 = (bf16[8,2048]{1,0:T(8,128)(2,1)S(1)}, bf16[8,2048]{1,0:T(8,128)(2,1)S(1)}, u32[]{:S(2)}, u32[]{:S(2)}) collective-permute-start(bf16[8,2048]{1,0:T(8,128)(2,1)S(1)} %dynamic-slice_bitcast_fusion), channel_id=1, source_target_pairs={{1,8},{3,10},{5,12},{7,14},{8,1},{9,16},{10,3},{11,18},{12,5},{13,... | collective-permute-start | bytes 98312 | tf_op jit(solution)/shard_map/ppermute | solution.py:502
  37.7 26.1 %copy-start.1 = (bf16[1,128,128]{2,1,0:T(8,128)(2,1)S(1)}, bf16[1,128,128]{2,1,0:T(8,128)(2,1)}, u32[]{:S(2)}) copy-start(bf16[1,128,128]{2,1,0:T(8,128)(2,1)} %param.24) | copy-start | bytes 98308
  37.7 26.1 %copy-start.3 = (bf16[128]{0:T(256)(128)(2,1)S(1)}, bf16[128]{0:T(256)(128)(2,1)}, u32[]{:S(2)}) copy-start(bf16[128]{0:T(256)(128)(2,1)} %param.25) | copy-start | bytes 772
  43.5 34.4 %all-to-all-start.1 = ((bf16[64,4,128]{2,1,0:T(4,128)(2,1)}), bf16[64,4,128]{2,1,0:T(4,128)(2,1)S(1)}, u32[]{:S(2)}, u32[]{:S(2)}) async-start(bf16[64,4,128]{2,1,0:T(4,128)(2,1)} %get-tuple-element.17), calls=%async_computation.1 | async-start | bytes 131072 | tf_op jit(solution)/shard_map/all_to_all | solution.py:558
  63.8 14.1 %copy-start.2 = (f32[4,8,256]{2,1,0:T(8,128)S(1)}, f32[4,8,256]{2,1,0:T(8,128)}, u32[]{:S(2)}) copy-start(f32[4,8,256]{2,1,0:T(8,128)} %get-tuple-element.18.seg_ref) | copy-start | bytes 98308
  80.6 6.0 %collective-permute-start.3 = (bf16[256,384]{1,0:T(8,128)(2,1)S(1)}, bf16[256,384]{1,0:T(8,128)(2,1)S(1)}, u32[]{:S(2)}, u32[]{:S(2)}) collective-permute-start(bf16[256,384]{1,0:T(8,128)(2,1)S(1)} %get-tuple-element.24), channel_id=1, source_target_pairs={{0,1},{1,0},{2,3},{3,2},{4,5},{5,4},{6,7},{7,6},{8,9},{9,8},{10,11... | collective-permute-start | bytes 589832 | tf_op jit(solution)/shard_map/ppermute | solution.py:480
